TPU v7x, 512 devices: a whole 4x4x16 slice. The times are simulated.
512 devices in a mesh: sp: 128 (over z, x, core), tp: 4 (over y).
Axes of the slice: x: 4, y: 4, z: 16, core: 2. Of those that a mesh axis runs over, the one named last changes fastest.
Arguments:
- tokens: bfloat16 [81920, 2048], P(('sp', 'tp')), may hold values from -44 to 44
- in_gain: float32 [2048], replicated, may hold values from 0.1 to 1.9
- w_x: bfloat16 [2048, 2048], P('sp', 'tp'), may hold values from -0.125 to 0.125
- w_z: bfloat16 [2048, 2048], P('sp', 'tp'), may hold values from -0.125 to 0.125
- w_b: bfloat16 [2048, 1024], P('sp', 'tp'), may hold values from -0.125 to 0.125
- w_c: bfloat16 [2048, 1024], P('sp', 'tp'), may hold values from -0.125 to 0.125
- w_dt: bfloat16 [2048, 32], replicated, may hold values from -0.125 to 0.125
- conv_x: float32 [4, 2048], replicated, may hold values from -3 to 3
- conv_b: float32 [4, 1024], replicated, may hold values from -3 to 3
- conv_c: float32 [4, 1024], replicated, may hold values from -3 to 3
- dt_bias: float32 [32], replicated, may hold values from -15 to -3.5
- a_log: float32 [32], replicated, may hold values from -0.5 to 0.5
- out_gain: float32 [2048], replicated, may hold values from 0.1 to 1.9
- w_out: bfloat16 [2048, 2048], P('tp', 'sp'), may hold values from -0.125 to 0.125
Outputs:
- mixer_out: bfloat16 [81920, 2048], P(('sp', 'tp'))
All inputs are finite; a program needn't handle non-finite values.
Results may differ from a plain program's by a relative error of at most 0.015.
Values may be sent and summed in bfloat16 or wider, within the bound.
No kernel may reach another device: no remote copies, remote signals or barrier semaphores. Data moves between devices by JAX's collectives and lax.ppermute only.
A program may use at most 128 MiB of HBM per device.

v0:
```python
import jax
import jax.numpy as jnp
from jax import lax
from jax.sharding import Mesh
from jax.sharding import PartitionSpec as P

HEAD_DIM = 64
STATE = 128
CONV = 4
BLOCK = 128
SP = ("sp_0", "sp_1", "sp_2")
SP_TP = ("sp_0", "sp_1", "sp_2", "tp")


EPS = 1e-06


def filled_with(shard, identity):
    return jax.tree.map(
        lambda part, zero: jnp.zeros_like(part) + jnp.asarray(zero, part.dtype), shard, identity
    )


def prefix_by_axis(shard, axes, combine, identity):
    before = start = filled_with(shard, identity)
    subtotal = shard
    for axis in reversed(axes):
        devices, here = (lax.axis_size(axis), lax.axis_index(axis))
        pieces = jax.tree.map(lambda part: lax.all_gather(part, axis), subtotal)
        inside, subtotal = (start, start)
        for k in range(devices):
            passed = k < here
            subtotal = combine(subtotal, jax.tree.map(lambda part: part[k], pieces))
            inside = jax.tree.map(lambda new, old: jnp.where(passed, new, old), subtotal, inside)
        before = combine(inside, before)
    return before


def from_everyone(shard, axis):
    copies = jnp.broadcast_to(shard, (lax.axis_size(axis), *shard.shape))
    return lax.all_to_all(copies, axis, split_axis=0, concat_axis=0, tiled=True)


def joined_along(tiles, dim):
    shape = list(tiles.shape[1:])
    shape[dim] *= tiles.shape[0]
    return jnp.moveaxis(tiles, 0, dim).reshape(shape)


def collect(shard, axis, dim):
    tiles = from_everyone(shard, axis)
    return joined_along(tiles, dim)


def sent_together(arrays, axis, dim, along):
    both = jnp.concatenate(arrays, axis=along)
    whole, at, outs = (lax.all_gather(both, axis, axis=dim, tiled=True), 0, [])
    for a in arrays:
        outs.append(lax.slice_in_dim(whole, at, at + a.shape[along], axis=along))
        at += a.shape[along]
    return tuple(outs)


def from_behind(value, axis, steps):
    count = lax.axis_size(axis)
    first, last = (max(0, -steps), min(count, count - steps))
    return lax.ppermute(value, axis, [(source, source + steps) for source in range(first, last)])


def stacked_from(shard, axes, sequence):
    tiles = shard[None]
    for k in sequence:
        tiles = lax.all_gather(tiles, axes[k], axis=0, tiled=True)
    current = [lax.axis_size(axes[k]) for k in reversed(sequence)]
    tiles = tiles.reshape(*current, *shard.shape)
    turned = sorted(range(len(sequence)), key=lambda place: sequence[len(sequence) - 1 - place])
    return tiles.transpose(*turned, *range(len(sequence), tiles.ndim)).reshape(-1, *shard.shape)


def gathered_by_axis(shard, axes, sequence, dim):
    return joined_along(stacked_from(shard, axes, sequence), dim)


def in_blocks(shard, dim, devices):
    before, after = (shard.shape[:dim], shard.shape[dim + 1 :])
    return jnp.moveaxis(shard.reshape(*before, devices, -1, *after), dim, 0)


def sent_and_summed(shard, axis, dim):
    devices = lax.axis_size(axis)
    tiles = lax.all_to_all(in_blocks(shard, dim, devices), axis, 0, 0, tiled=True)
    return jnp.sum(tiles.astype(jnp.float32), axis=0)


def inverse_rms(values):
    return lax.rsqrt(jnp.mean(values * values, axis=-1, keepdims=True) + EPS)


def causal_conv(prev_rows, new_rows, kernel):
    joined = jnp.concatenate([prev_rows, new_rows], axis=0).astype(jnp.float32)
    row_count = new_rows.shape[0]
    summed = jnp.zeros(new_rows.shape, jnp.float32)
    for offset in range(kernel.shape[0]):
        summed = summed + kernel[offset] * joined[offset : offset + row_count]
    return jax.nn.silu(summed)


def fold_single(gathered):

    def fold_step(total_part, rows_part, first_row):
        return jnp.dot(gathered, rows_part, preferred_element_type=jnp.float32)

    return fold_step


def fold_products(gathered, totals, weight_rows, first_row):
    single = fold_single(gathered)
    return tuple(
        (
            single(total_part, rows_part, first_row)
            for total_part, rows_part in zip(totals, weight_rows)
        )
    )


def inner_part(cum_decay, b_rows, c_rows, scaled_x, causal):
    scores = jnp.einsum("blgn,bsgn->bgls", c_rows, b_rows)
    decay_gap = cum_decay[:, :, None] - cum_decay[:, None, :]
    causal_mask = causal[None, :, :, None, None]
    within = jnp.where(causal_mask, jnp.exp(jnp.where(causal_mask, decay_gap, 0.0)), 0.0)
    return jnp.einsum("bgls,blsgh,bsghp->blghp", scores, within, scaled_x)


def carried_part(c_rows, states, cum_decay):
    return jnp.einsum("blgn,bghpn,blgh->blghp", c_rows, states, jnp.exp(cum_decay))


def run_blocks(block_states, block_decay, start_state):

    def advance(run_state, inputs):
        fresh_state, factor = inputs
        return (run_state * factor[:, :, None, None] + fresh_state, run_state)

    final_state, entering = lax.scan(advance, start_state, (block_states, block_decay))
    return (entering, final_state)


def chain(earlier, later):
    return (earlier[0] * later[0], earlier[1] * later[0][:, :, None, None] + later[1])


def carry_in(total_decay, final_state):
    identity = (jnp.ones_like(total_decay), jnp.zeros_like(final_state))
    before = prefix_by_axis((total_decay, final_state), SP, chain, identity)
    return before[1]


def body(
    tokens,
    in_gain,
    w_x,
    w_z,
    w_b,
    w_c,
    w_dt,
    conv_x,
    conv_b,
    conv_c,
    dt_bias,
    a_log,
    out_gain,
    w_out,
):
    share_index = lax.axis_index("tp")
    width_x = w_x.shape[1]
    width_b = w_b.shape[1]
    heads_here = width_x // HEAD_DIM
    groups_here = width_b // STATE
    group_heads = heads_here // groups_here
    kernel_x = lax.dynamic_slice_in_dim(conv_x, share_index * width_x, width_x, 1)
    kernel_b = lax.dynamic_slice_in_dim(conv_b, share_index * width_b, width_b, 1)
    kernel_c = lax.dynamic_slice_in_dim(conv_c, share_index * width_b, width_b, 1)
    bias_here = lax.dynamic_slice_in_dim(dt_bias, share_index * heads_here, heads_here, 0)
    rate_here = jnp.exp(lax.dynamic_slice_in_dim(a_log, share_index * heads_here, heads_here, 0))
    gain_here = lax.dynamic_slice_in_dim(out_gain, share_index * width_x, width_x, 0)
    dt_weight = lax.dynamic_slice_in_dim(w_dt, share_index * heads_here, heads_here, 1)
    values = tokens.astype(jnp.float32)
    normed = (values * inverse_rms(values) * in_gain).astype(jnp.bfloat16)
    gathered = collect(normed, "tp", 0)
    seg_rows = gathered.shape[0]
    blocks = seg_rows // BLOCK
    empty_x = jnp.zeros((seg_rows, width_x), jnp.float32)
    empty_b = jnp.zeros((seg_rows, width_b), jnp.float32)
    projected = fold_products(
        gathered,
        (empty_x, empty_x, empty_b, empty_b),
        sent_together((w_x, w_z, w_b, w_c), SP, 0, 1),
        jnp.int32(0),
    )
    proj_x, gate_rows, proj_b, proj_c = [
        summed_part.astype(jnp.bfloat16) for summed_part in projected
    ]
    dt_raw = jnp.dot(gathered, dt_weight, preferred_element_type=jnp.float32)
    conv_keep = CONV - 1
    tail_start = seg_rows - conv_keep
    prev_x, prev_b, prev_c = from_behind(
        (proj_x[tail_start:], proj_b[tail_start:], proj_c[tail_start:]), SP, 1
    )
    conv_xs = causal_conv(prev_x, proj_x, kernel_x)
    conv_bs = causal_conv(prev_b, proj_b, kernel_b)
    conv_cs = causal_conv(prev_c, proj_c, kernel_c)
    step_size = jax.nn.softplus(dt_raw + bias_here)
    log_decay = (-step_size * rate_here).reshape(blocks, BLOCK, groups_here, group_heads)
    causal = lax.broadcasted_iota(jnp.int32, (BLOCK, BLOCK), 0) >= lax.broadcasted_iota(
        jnp.int32, (BLOCK, BLOCK), 1
    )
    cum_decay = jnp.einsum("ls,bsgh->blgh", causal.astype(jnp.float32), log_decay)
    scaled_x = (conv_xs.reshape(seg_rows, heads_here, HEAD_DIM) * step_size[:, :, None]).reshape(
        blocks, BLOCK, groups_here, group_heads, HEAD_DIM
    )
    b_rows = conv_bs.reshape(blocks, BLOCK, groups_here, STATE)
    c_rows = conv_cs.reshape(blocks, BLOCK, groups_here, STATE)
    block_total = cum_decay[:, BLOCK - 1]
    tail_weight = jnp.exp(block_total[:, None] - cum_decay)
    block_states = jnp.einsum("blgn,blgh,blghp->bghpn", b_rows, tail_weight, scaled_x)
    block_decay = jnp.exp(block_total)
    total_decay = jnp.exp(jnp.sum(block_total, axis=0))
    start_state = jnp.zeros(block_states.shape[1:], jnp.float32)
    entering, final_state = run_blocks(block_states, block_decay, start_state)
    local_out = inner_part(cum_decay, b_rows, c_rows, scaled_x, causal) + carried_part(
        c_rows, entering, cum_decay
    )
    incoming = carry_in(total_decay, final_state)
    offset = jnp.cumsum(block_total, axis=0) - block_total
    reach_decay = jnp.exp(cum_decay + offset[:, None])
    heads_out = local_out + jnp.einsum("blgn,ghpn,blgh->blghp", c_rows, incoming, reach_decay)
    gated_out = heads_out.reshape(seg_rows, width_x) * jax.nn.silu(gate_rows.astype(jnp.float32))
    grouped = gated_out.reshape(seg_rows, groups_here, width_x // groups_here)
    mixed_rows = ((grouped * inverse_rms(grouped)).reshape(seg_rows, width_x) * gain_here).astype(
        jnp.bfloat16
    )
    partial_sum = jnp.dot(
        mixed_rows, gathered_by_axis(w_out, SP, (1, 0, 2), 1), preferred_element_type=jnp.float32
    )
    return sent_and_summed(partial_sum.astype(jnp.bfloat16), "tp", 0).astype(jnp.bfloat16)


def solution(mesh):
    split = Mesh(mesh.devices.reshape(16, 4, 2, mesh.shape["tp"]), ("sp_0", "sp_1", "sp_2", "tp"))
    in_specs = (
        P(SP_TP, None),
        P(),
        P(SP, "tp"),
        P(SP, "tp"),
        P(SP, "tp"),
        P(SP, "tp"),
        P(),
        P(),
        P(),
        P(),
        P(),
        P(),
        P(),
        P("tp", SP),
    )
    out_specs = P(SP_TP, None)
    return jax.shard_map(body, mesh=split, in_specs=in_specs, out_specs=out_specs, check_vma=False)
```

profile of v0, /device:TPU:4, one launch (start us, length us, event | category | flops | bytes accessed | tf_op | source)
XLA Modules:
  0.0 423.4 jit_solution(15064805402565436030)
XLA Ops:
  12.5 4.6 %all-to-all-start = ((bf16[4,160,2048]{2,1,0:T(8,128)(2,1)}), bf16[4,160,2048]{2,1,0:T(8,128)(2,1)S(1)}, u32[]{:S(2)}, u32[]{:S(2)}) async-start(bf16[4,160,2048]{2,1,0:T(8,128)(2,1)} %broadcast_in_dim.45), calls=%async_computation | async-start | bytes 5242880 | tf_op jit(solution)/shard_map/all_to_all | solution.py:41
  17.1 14.9 %all-gather.2 = bf16[2048,16]{0,1:T(8,128)(2,1)S(1)} all-gather(bf16[512,16]{0,1:T(8,128)(2,1)S(1)} %copy-done.9), channel_id=4, replica_groups=mesh['sp_0'=16,'sp_1'=4,'sp_2'=2,'tp'=4] {'sp_1'}, dimensions={0}, use_global_device_ids=true | all-gather | bytes 81920 | tf_op jit(solution)/shard_map/all_gather | solution.py:73
  34.8 14.3 %all-to-all-done = bf16[4,160,2048]{2,1,0:T(8,128)(2,1)S(1)} async-done(((bf16[4,160,2048]{2,1,0:T(8,128)(2,1)}), bf16[4,160,2048]{2,1,0:T(8,128)(2,1)S(1)}, u32[]{:S(2)}, u32[]{:S(2)}) %all-to-all-start) | async-done | bytes 2621472 | tf_op jit(solution)/shard_map/all_to_all | solution.py:41
  52.4 7.6 %all-gather.5 = f32[4,2,4]{2,1,0:T(2,128)S(1)} all-gather(f32[1,2,4]{2,1,0:T(2,128)S(1)} %fusion.203), channel_id=5, replica_groups=mesh['sp_0'=16,'sp_1'=4,'sp_2'=2,'tp'=4] {'sp_1'}, dimensions={0}, use_global_device_ids=true | all-gather | bytes 160 | tf_op jit(solution)/shard_map/all_gather | solution.py:29
  60.6 96.9 %all-gather.12.cloned.1.call-done = bf16[2048,1536]{1,0:T(8,128)(2,1)} async-done(((bf16[16,1536]{1,0:T(8,128)(2,1)}), bf16[2048,1536]{1,0:T(8,128)(2,1)}) %all-gather.12.cloned.1.call-update) | async-done | bytes 6291472 | tf_op jit(solution)/shard_map/all_gather | solution.py:57
  159.5 2.1 collective-permute-start.1
  161.7 3.1 fusion.17
  164.8 2.8 collective-permute-start.2
  173.0 2.8 copy.151
  175.8 2.7 reshape.158
  178.5 2.9 broadcast_multiply_fusion
  182.8 8.7 %while.13 = (s32[]{:T(128)}, f32[2,4,64,128]{3,2,1,0:T(8,128)S(1)}, bf16[5,2,4,64,128]{4,3,2,1,0:T(8,128)(2,1)}, f32[5,2,4]{2,1,0:T(2,128)S(1)}, f32[5,2,4,64,128]{4,3,2,1,0:T(8,128)}, /*index=5*/s32[]{:T(128)}, s32[]{:T(128)}) while((s32[]{:T(128)}, f32[2,4,64,128]{3,2,1,0:T(8,128)S(1)}, bf16[5,2,4,64,128]{4,3,2,1,0:T(8,128)(2,1)}, ...), condition=%wide.region_2.3_spmd.clone, body=%wide.region_1.2_spmd.clone.sunk | while | flops 262147 | bytes 1180352 | solution.py:144
  191.5 2.2 all-gather.1
  195.4 31.6 %all-gather.18.cloned.1.call-done = bf16[64,512,16]{1,2,0:T(8,128)(2,1)} async-done(((bf16[4,512,16]{1,2,0:T(8,128)(2,1)}), bf16[64,512,16]{1,2,0:T(8,128)(2,1)}) %all-gather.18.cloned.1.call-update) | async-done | bytes 1048592 | tf_op jit(solution)/shard_map/all_gather | solution.py:73
  227.0 30.1 %all-gather.14.cloned.1.call-done = f32[4,2,4,64,128]{4,3,2,1,0:T(8,128)} async-done(((f32[1,2,4,64,128]{4,3,2,1,0:T(8,128)}), f32[4,2,4,64,128]{4,3,2,1,0:T(8,128)}) %all-gather.14.cloned.1.call-update) | async-done | bytes 1048592 | tf_op jit(solution)/shard_map/all_gather | solution.py:29
  262.1 30.2 %all_gather.41 = f32[16,2,4]{2,1,0:T(2,128)S(1)} all-gather(f32[1,2,4]{2,1,0:T(2,128)S(1)} %get-tuple-element.141), channel_id=1, replica_groups=mesh['sp_0'=16,'sp_1'=4,'sp_2'=2,'tp'=4] {'sp_0'}, dimensions={0}, use_global_device_ids=true | all-gather | bytes 544 | tf_op jit(solution)/shard_map/all_gather | solution.py:29
  297.2 3.3 copy.167
  304.3 2.2 fusion.13
  306.4 56.2 %all-gather.16.cloned.1.call-done = f32[16,2,4,64,128]{4,3,2,1,0:T(8,128)} async-done(((f32[1,2,4,64,128]{4,3,2,1,0:T(8,128)}), f32[16,2,4,64,128]{4,3,2,1,0:T(8,128)}) %all-gather.16.cloned.1.call-update) | async-done | bytes 4194320 | tf_op jit(solution)/shard_map/all_gather | solution.py:29
  362.8 3.8 fusion.16
  368.1 3.7 copy.179
  371.8 3.9 reshape.203
  375.6 5.2 %fusion.207 = (f32[640,512]{1,0:T(8,128)}, f32[640,512]{1,0:T(8,128)}) fusion(f32[640,512]{1,0:T(8,128)} %reshape.203, bf16[640,2048]{1,0:T(8,128)(2,1)S(1)} %bitcast.322, bf16[2048,1536]{1,0:T(8,128)(2,1)} %all-gather.12.cloned.1.call-done), kind=kOutput, calls=%fused_computation.281 | convolution fusion | flops 1344798720 | bytes 8650752 | tf_op jit(solution)/shard_map/dot_general | solution.py:111
  387.9 27.4 %all_to_all.10 = bf16[4,160,2048]{2,1,0:T(8,128)(2,1)S(1)} all-to-all(bf16[4,160,2048]{2,1,0:T(8,128)(2,1)S(1)} %bitcast.327), channel_id=1, replica_groups=mesh['sp_0'=16,'sp_1'=4,'sp_2'=2,'tp'=4] {'tp'}, dimensions={0} | all-to-all | bytes 5242880 | tf_op jit(solution)/shard_map/all_to_all | solution.py:91
  (171 shorter events, 55.1 us)
Async XLA Ops:
  6.5 150.9 %all-gather.12.cloned.1.call-start = ((), (), s32[]{:S(2)}) async-start(), calls=%async_computation.2 | async-start | bytes 6340608 | tf_op jit(solution)/shard_map/all_gather | solution.py:57
  12.5 36.5 %all-to-all-start = ((bf16[4,160,2048]{2,1,0:T(8,128)(2,1)}), bf16[4,160,2048]{2,1,0:T(8,128)(2,1)S(1)}, u32[]{:S(2)}, u32[]{:S(2)}) async-start(bf16[4,160,2048]{2,1,0:T(8,128)(2,1)} %broadcast_in_dim.45), calls=%async_computation | async-start | bytes 5242880 | tf_op jit(solution)/shard_map/all_to_all | solution.py:41
  17.1 209.8 %all-gather.18.cloned.1.call-start = ((), (), s32[]{:S(2)}) async-start(), calls=%async_computation.5 | async-start | bytes 1114112 | tf_op jit(solution)/shard_map/all_gather | solution.py:73
  32.7 224.4 %all-gather.14.cloned.1.call-start = ((), (), s32[]{:S(2)}) async-start(), calls=%async_computation.3 | async-start | bytes 1310720 | tf_op jit(solution)/shard_map/all_gather | solution.py:29
  60.6 133.1 %copy-start.11 = (f32[2,4]{1,0:T(2,128)}, f32[2,4]{1,0:T(2,128)S(1)}, u32[]{:S(2)}) copy-start(f32[2,4]{1,0:T(2,128)S(1)} %get-tuple-element.146) | copy-start | bytes 100
  159.5 8.1 %collective-permute-start.1 = (bf16[3,256]{1,0:T(4,128)(2,1)S(1)}, bf16[3,256]{1,0:T(4,128)(2,1)S(1)}, u32[]{:S(2)}, u32[]{:S(2)}) collective-permute-start(bf16[3,256]{1,0:T(4,128)(2,1)S(1)} %slice.325), channel_id=1, source_target_pairs={{0,4},{4,8},{8,12},{12,16},{16,20},{20,24},{24,28},{28,32},{32,36}... | collective-permute-start | bytes 4616 | tf_op jit(solution)/shard_map/ppermute | solution.py:67
  164.8 5.1 %collective-permute-start.2 = (bf16[3,512]{1,0:T(4,128)(2,1)S(1)}, bf16[3,512]{1,0:T(4,128)(2,1)S(1)}, u32[]{:S(2)}, u32[]{:S(2)}) collective-permute-start(bf16[3,512]{1,0:T(4,128)(2,1)S(1)} %slice.331), channel_id=1, source_target_pairs={{0,4},{4,8},{8,12},{12,16},{16,20},{20,24},{24,28},{28,32},{32,36}... | collective-permute-start | bytes 9224 | tf_op jit(solution)/shard_map/ppermute | solution.py:67
  195.3 101.9 %all-gather.20.cloned.1.call-start = ((), (), s32[]{:S(2)}) async-start(), calls=%async_computation.6 | async-start | bytes 3145728 | tf_op jit(solution)/shard_map/all_gather | solution.py:73
  227.0 135.6 %all-gather.16.cloned.1.call-start = ((), (), s32[]{:S(2)}) async-start(), calls=%async_computation.4 | async-start | bytes 4456448 | tf_op jit(solution)/shard_map/all_gather | solution.py:29
  294.4 6.2 %collective-permute-start = (bf16[3,256]{1,0:T(4,128)(2,1)S(1)}, bf16[3,256]{1,0:T(4,128)(2,1)S(1)}, u32[]{:S(2)}, u32[]{:S(2)}) collective-permute-start(bf16[3,256]{1,0:T(4,128)(2,1)S(1)} %slice.319), channel_id=1, source_target_pairs={{0,4},{4,8},{8,12},{12,16},{16,20},{20,24},{24,28},{28,32},{32,36}... | collective-permute-start | bytes 4616 | tf_op jit(solution)/shard_map/ppermute | solution.py:67
  304.1 58.5 %copy-start.20 = (f32[2,4]{1,0:T(2,128)S(1)}, f32[2,4]{1,0:T(2,128)}, u32[]{:S(2)}) copy-start(f32[2,4]{1,0:T(2,128)} %get-tuple-element.117) | copy-start | bytes 100
  304.1 58.5 %copy-start.21 = (f32[2,4]{1,0:T(2,128)S(1)}, f32[2,4]{1,0:T(2,128)}, u32[]{:S(2)}) copy-start(f32[2,4]{1,0:T(2,128)} %get-tuple-element.118) | copy-start | bytes 100
  304.1 58.5 %copy-start.22 = (f32[2,4]{1,0:T(2,128)S(1)}, f32[2,4]{1,0:T(2,128)}, u32[]{:S(2)}) copy-start(f32[2,4]{1,0:T(2,128)} %get-tuple-element.119) | copy-start | bytes 100
  304.1 58.5 %copy-start.23 = (f32[2,4]{1,0:T(2,128)S(1)}, f32[2,4]{1,0:T(2,128)}, u32[]{:S(2)}) copy-start(f32[2,4]{1,0:T(2,128)} %get-tuple-element.120) | copy-start | bytes 100
  304.1 58.5 %copy-start.24 = (f32[2,4]{1,0:T(2,128)S(1)}, f32[2,4]{1,0:T(2,128)}, u32[]{:S(2)}) copy-start(f32[2,4]{1,0:T(2,128)} %get-tuple-element.121) | copy-start | bytes 100
  304.1 58.5 %copy-start.25 = (f32[2,4]{1,0:T(2,128)S(1)}, f32[2,4]{1,0:T(2,128)}, u32[]{:S(2)}) copy-start(f32[2,4]{1,0:T(2,128)} %get-tuple-element.122) | copy-start | bytes 100
  304.2 58.5 %copy-start.26 = (f32[2,4]{1,0:T(2,128)S(1)}, f32[2,4]{1,0:T(2,128)}, u32[]{:S(2)}) copy-start(f32[2,4]{1,0:T(2,128)} %get-tuple-element.123) | copy-start | bytes 100
  304.2 58.5 %copy-start.27 = (f32[2,4]{1,0:T(2,128)S(1)}, f32[2,4]{1,0:T(2,128)}, u32[]{:S(2)}) copy-start(f32[2,4]{1,0:T(2,128)} %get-tuple-element.124) | copy-start | bytes 100
  304.2 58.5 %copy-start.28 = (f32[2,4]{1,0:T(2,128)S(1)}, f32[2,4]{1,0:T(2,128)}, u32[]{:S(2)}) copy-start(f32[2,4]{1,0:T(2,128)} %get-tuple-element.125) | copy-start | bytes 100
  304.2 58.5 %copy-start.29 = (f32[2,4]{1,0:T(2,128)S(1)}, f32[2,4]{1,0:T(2,128)}, u32[]{:S(2)}) copy-start(f32[2,4]{1,0:T(2,128)} %get-tuple-element.126) | copy-start | bytes 100
  304.2 58.5 %copy-start.30 = (f32[2,4]{1,0:T(2,128)S(1)}, f32[2,4]{1,0:T(2,128)}, u32[]{:S(2)}) copy-start(f32[2,4]{1,0:T(2,128)} %get-tuple-element.127) | copy-start | bytes 100
  304.2 58.5 %copy-start.31 = (f32[2,4]{1,0:T(2,128)S(1)}, f32[2,4]{1,0:T(2,128)}, u32[]{:S(2)}) copy-start(f32[2,4]{1,0:T(2,128)} %get-tuple-element.128) | copy-start | bytes 100
  304.2 58.5 %copy-start.32 = (f32[2,4]{1,0:T(2,128)S(1)}, f32[2,4]{1,0:T(2,128)}, u32[]{:S(2)}) copy-start(f32[2,4]{1,0:T(2,128)} %get-tuple-element.129) | copy-start | bytes 100
  304.2 58.5 %copy-start.33 = (f32[2,4]{1,0:T(2,128)S(1)}, f32[2,4]{1,0:T(2,128)}, u32[]{:S(2)}) copy-start(f32[2,4]{1,0:T(2,128)} %get-tuple-element.130) | copy-start | bytes 100
  (26 other events, 685.8 us)
Sparse Core Ops, SparseCore 0:
  10.5 146.9 all-gather.11
  159.5 67.3 all-gather.17
  229.0 28.0 all-gather.13
  259.0 22.3 all-gather.19
  283.4 79.1 all-gather.15
where the time goes:
time: 425 us; the launch traced here: 423 us
  waiting for transfers between devices  229 us (54%)
  blocking collectives  84.1 us (20%)
  local copies, waits for them, and re-layouts  31.8 us (7%)
  other arithmetic  28.5 us (7%)
  matrix products  24.2 us (6%)
  between operations  13.9 us (3%)
  starting transfers between devices  11.7 us (3%)
    all_gather x1, waiting for transfers between devices, sent_together(): whole, at, outs = (lax.all_gather(both, axis, axis=dim, tiled=True), 0, [])  96.9 us
    all_gather x2, waiting for transfers between devices, prefix_by_axis(): pieces = jax.tree.map(lambda part: lax.all_gather(part, axis), subtotal)  86.2 us
    all_gather x4, blocking collectives, prefix_by_axis(): pieces = jax.tree.map(lambda part: lax.all_gather(part, axis), subtotal)  41.8 us
    all_gather x2, waiting for transfers between devices, stacked_from(): tiles = lax.all_gather(tiles, axes[k], axis=0, tiled=True)  31.6 us
    all_to_all x1, blocking collectives, sent_and_summed(): lax.all_to_all(in_blocks(shard, dim, devices), axis, 0, 0, tiled=True)  27.4 us
    all_gather x1, blocking collectives, stacked_from(): tiles = lax.all_gather(tiles, axes[k], axis=0, tiled=True)  14.9 us
    all_to_all x1, waiting for transfers between devices, from_everyone(): return lax.all_to_all(copies, axis, split_axis=0, concat_axis=0, tiled=True)  14.3 us
    dot_general x4, matrix products, fold_step(): return jnp.dot(gathered, rows_part, preferred_element_type=jnp.float32)  12.5 us
  transfers between devices with their start and end apart: 9, of which 5 were waited for; matrix products, arithmetic and copies ran while one was open for 13% of the time, Pallas kernels for 0%

commit v1 on v0

v1 whole, which is shorter than its diff:
```python
import jax
import jax.numpy as jnp
from jax import lax
from jax.experimental import pallas as pl
from jax.experimental.pallas import tpu as pltpu
from jax.sharding import Mesh
from jax.sharding import PartitionSpec as P

HEAD_DIM = 64
STATE = 128
CONV = 4
BLOCK = 128
EPS = 1e-06
F32 = jnp.float32
BF16 = jnp.bfloat16
ALL = ("z", "x", "c", "y")

SMEM = pl.BlockSpec(memory_space=pltpu.SMEM)
VMEM = pl.BlockSpec(memory_space=pltpu.VMEM)


def cycle(count, step):
    return [(a, (a + step) % count) for a in range(count)]


def silu(v):
    return v / (1.0 + jnp.exp(-v))


def local_call(kernel, outs, ins, scalars=0, scratch=(), mib=16):
    return pl.pallas_call(
        kernel,
        out_shape=outs,
        in_specs=[SMEM] * scalars + [VMEM] * (len(ins) - scalars),
        out_specs=jax.tree.map(lambda _: VMEM, outs),
        scratch_shapes=list(scratch),
        compiler_params=pltpu.CompilerParams(vmem_limit_bytes=mib << 20),
    )(*ins)


def to_all(value, axis, copies):
    return lax.all_to_all(
        jnp.broadcast_to(value, (copies, *value.shape)), axis, 0, 0, tiled=True
    )


def rotate_kernel(at, *refs):
    *pieces, out = refs
    count = len(pieces)
    for k in range(count):
        slot = lax.rem(at[0] + count - k, count)
        out[:, pl.ds(slot, 1)] = pieces[k][...][:, None]


def placed(pieces, at):
    lead, *rest = pieces[0].shape
    out = jax.ShapeDtypeStruct((lead, len(pieces), *rest), pieces[0].dtype)
    return local_call(rotate_kernel, out, (at, *pieces), 1, mib=8)


def around(value, axis):
    count = lax.axis_size(axis)
    return [value] + [lax.ppermute(value, axis, cycle(count, k)) for k in range(1, count)]


def norm_kernel(at, gain, tail, *refs):
    *pieces, out = refs
    count = len(pieces)
    rows = pieces[0].shape[0]

    def normed(values):
        values = values.astype(F32)
        mean = jnp.mean(values * values, axis=-1, keepdims=True)
        return (values * lax.rsqrt(mean + EPS) * gain[...]).astype(BF16)

    out[count * rows :, :] = normed(tail[...])
    for k in range(count):
        first = lax.rem(at[0] + count - k, count) * rows

        def chunk(r, carry):
            to = pl.multiple_of(first + r * 16, 16)
            out[pl.ds(to, 16), :] = normed(pieces[k][pl.ds(pl.multiple_of(r * 16, 16), 16), :])
            return carry

        lax.fori_loop(0, rows // 16, chunk, 0, unroll=5)


def scan_kernel(
    core, own, other, step, rate, taps, y_out, c_out, reach_out, state_out, rows_seq, buf, state, offset
):
    length = step.shape[0]
    inner = y_out.shape[1] // 2
    heads = inner // HEAD_DIM
    rows_seq[pl.ds(core[0], 1)] = own[...][None]
    rows_seq[pl.ds(1 - core[0], 1)] = other[...][None]
    buf[:, 0:8, :] = rows_seq[:, length + 8 : length + 16, :].astype(F32)
    state[...] = jnp.zeros_like(state)
    offset[...] = jnp.zeros_like(offset)
    causal = lax.broadcasted_iota(jnp.int32, (BLOCK, BLOCK), 0) >= lax.broadcasted_iota(
        jnp.int32, (BLOCK, BLOCK), 1
    )
    lower = causal.astype(F32)

    def block(i, carry):
        here = pl.ds(i * BLOCK, BLOCK)
        steps = step[here, :]
        cum = jnp.dot(
            lower, -steps * rate[...], precision=lax.Precision.HIGHEST, preferred_element_type=F32
        )
        cum_t = cum.T
        total = cum[BLOCK - 1 : BLOCK, :]
        decay = jnp.exp(cum)
        tail_weight = jnp.exp(total - cum)
        total_decay = jnp.exp(total)
        reach_out[here, :] = jnp.exp(cum + offset[...])
        offset[...] = offset[...] + total
        for g in range(2):
            buf[g, 8 : 8 + BLOCK, :] = rows_seq[g, here, :].astype(F32)
            summed = taps[g, 0:1, :] * buf[g, 5 : 5 + BLOCK, :]
            for k in range(1, CONV):
                summed = summed + taps[g, k : k + 1, :] * buf[g, 5 + k : 5 + k + BLOCK, :]
            buf[g, 0:8, :] = buf[g, BLOCK : BLOCK + 8, :]
            mixed = silu(summed)
            xs = mixed[:, :inner]
            bs = mixed[:, inner : inner + STATE]
            cs = mixed[:, inner + STATE :].astype(BF16)
            scores = lax.dot_general(
                cs, bs.astype(BF16), (((1,), (1,)), ((), ())), preferred_element_type=F32
            )
            old = state[g]
            reached = jnp.dot(cs, old.astype(BF16), preferred_element_type=F32)
            tails, factors, ys = [], [], []
            for h in range(heads):
                cut = slice(h * HEAD_DIM, (h + 1) * HEAD_DIM)
                lane = slice(g * heads + h, g * heads + h + 1)
                scaled = xs[:, cut] * steps[:, lane]
                gap = cum[:, lane] - cum_t[lane, :]
                within = jnp.where(causal, jnp.exp(jnp.where(causal, gap, 0.0)), 0.0) * scores
                inside = jnp.dot(
                    within.astype(BF16), scaled.astype(BF16), preferred_element_type=F32
                )
                ys.append(inside + reached[:, cut] * decay[:, lane])
                tails.append(scaled * tail_weight[:, lane])
                factors.append(jnp.broadcast_to(total_decay[:, lane], (1, HEAD_DIM)))
            y_out[here, g * inner : (g + 1) * inner] = jnp.concatenate(ys, axis=1)
            c_out[here, g * STATE : (g + 1) * STATE] = cs
            fresh = jnp.dot(
                bs.T.astype(BF16),
                jnp.concatenate(tails, axis=1).astype(BF16),
                preferred_element_type=F32,
            )
            state[g] = old * jnp.concatenate(factors, axis=1) + fresh
        return carry

    lax.fori_loop(0, length // BLOCK, block, 0)
    share = STATE // state_out.shape[0]
    for part in range(state_out.shape[0]):
        rows = slice(part * share, (part + 1) * share)
        write_packed(
            state_out,
            part,
            jnp.concatenate([state[0, rows, :], state[1, rows, :]], axis=1),
            jnp.exp(offset[...]),
        )


def write_packed(out, part, states, factor):
    width = states.shape[1]
    high = factor.astype(BF16).astype(F32)
    low = factor - high
    pick = lax.broadcasted_iota(jnp.int32, (states.shape[0], factor.shape[1]), 0)
    extra = jnp.where(pick == 0, high, jnp.where(pick == 1, low, 0.0))
    out[part, :, 0:width] = states.astype(BF16)
    out[part, :, width:] = extra.astype(BF16)


def read_packed(ref, part):
    width = ref.shape[2] - 128
    extra = ref[part, :, width:].astype(F32)
    return extra[0:1, :] + extra[1:2, :], ref[part, :, 0:width].astype(F32)


def widened(factor, width):
    return jnp.concatenate(
        [
            jnp.broadcast_to(factor[:, h : h + 1], (factor.shape[0], HEAD_DIM))
            for h in range(width // HEAD_DIM)
        ],
        axis=1,
    )


def plane_kernel(pieces, out):
    factor, states = read_packed(pieces, 0)
    for k in range(1, pieces.shape[0]):
        next_factor, next_states = read_packed(pieces, k)
        states = states * widened(next_factor, states.shape[1]) + next_states
        factor = factor * next_factor
    for k in range(out.shape[0]):
        write_packed(out, k, states, factor)


def enter_kernel(at, pieces, planes, out):
    run = jnp.zeros(out.shape[1:], F32)
    for k in range(planes.shape[0]):
        factor, states = read_packed(planes, k)
        run = jnp.where(k < at[0], run * widened(factor, run.shape[1]) + states, run)
    for k in range(pieces.shape[0]):
        out[k] = run.astype(BF16)
        factor, states = read_packed(pieces, k)
        run = run * widened(factor, run.shape[1]) + states


def gate_kernel(core, y, cs, reach, entering, gate_own, gate_other, gain, out):
    inner = y.shape[1] // 2
    heads = inner // HEAD_DIM

    def block(i, carry):
        here = pl.ds(pl.multiple_of(i * BLOCK, BLOCK), BLOCK)
        weight = reach[here, :]
        own, other = (gate[here, :].astype(F32) for gate in (gate_own, gate_other))
        for g in range(2):
            cut = slice(g * inner, (g + 1) * inner)
            reached = jnp.dot(
                cs[here, g * STATE : (g + 1) * STATE],
                entering[:, cut],
                preferred_element_type=F32,
            )
            expanded = widened(weight[:, g * heads : (g + 1) * heads], inner)
            gates = jnp.where(core[0] == g, own, other)
            gated = (y[here, cut] + reached * expanded) * silu(gates)
            mean = jnp.mean(gated * gated, axis=-1, keepdims=True)
            out[here, cut] = (gated * lax.rsqrt(mean + EPS) * gain[:, cut]).astype(BF16)
        return carry

    lax.fori_loop(0, y.shape[0] // BLOCK, block, 0)


def dot(a, b):
    return jnp.dot(a, b, preferred_element_type=F32)


def dot_t(a, b):
    return lax.dot_general(a, b, (((1,), (1,)), ((), ())), preferred_element_type=F32)


def body(
    tokens, in_gain, w_x, w_z, w_b, w_c, w_dt, conv_x, conv_b, conv_c, dt_bias, a_log, out_gain, w_out
):
    x_at, c_at, y_at, z_at = (lax.axis_index(a) for a in ("x", "c", "y", "z"))
    x_one, c_one, y_one, z_one = (v.reshape(1) for v in (x_at, c_at, y_at, z_at))
    n_z, n_x, n_y = (lax.axis_size(a) for a in ("z", "x", "y"))
    rows, width = tokens.shape
    length = rows * n_y
    inner = w_x.shape[1] // 2
    state = w_b.shape[1] // 2
    heads = 2 * inner // HEAD_DIM
    cut = inner + 2 * state
    core_swap = cycle(2, 1)

    def halves_swapped(*arrays):
        def columns_of(core):
            return jnp.concatenate(
                [
                    lax.dynamic_slice_in_dim(w, core * (w.shape[1] // 2), w.shape[1] // 2, 1)
                    for w in arrays
                ],
                axis=1,
            )

        mine = columns_of(c_at)
        swapped = lax.ppermute(columns_of(1 - c_at), "c", core_swap)
        return jnp.where(
            c_at == 0,
            jnp.concatenate([mine, swapped], axis=0),
            jnp.concatenate([swapped, mine], axis=0),
        )

    first_source = halves_swapped(w_x, w_b, w_c)
    pieces = around(tokens, "y")
    first_z = to_all(first_source, "z", n_z)
    first_pieces = around(first_z, "x")
    second_source = halves_swapped(w_z, w_out.T)
    second_source, first_z = lax.optimization_barrier((second_source, first_z))
    second_z = to_all(second_source, "z", n_z)

    ends = lax.select_n(lax.rem(y_at + 1, n_y), *(piece[rows - 16 :] for piece in pieces))
    chain_steps = [(a, a + 1) for a in range(2 * n_z * n_x - 1)]
    tail = lax.ppermute(ends, ("z", "x", "c"), chain_steps)
    normed = local_call(
        norm_kernel,
        jax.ShapeDtypeStruct((length + 16, width), BF16),
        (y_one, in_gain.reshape(1, -1), tail, *pieces),
        1,
    )

    def here(v, size):
        return lax.dynamic_slice_in_dim(v, y_at * size, size, v.ndim - 1)

    lanes = 128
    dt_weight = jnp.pad(here(w_dt, heads), ((0, 0), (0, lanes - heads)))
    bias = jnp.pad(here(dt_bias, heads), (0, lanes - heads))
    rate = jnp.pad(jnp.exp(here(a_log, heads)), (0, lanes - heads)).reshape(1, lanes)
    step = jax.nn.softplus(dot(normed[:length], dt_weight) + bias)
    taps = jnp.concatenate(
        [
            here(v, 2 * size).reshape(CONV, 2, size).swapaxes(0, 1)
            for v, size in ((conv_x, inner), (conv_b, state), (conv_c, state))
        ],
        axis=2,
    )

    first_pieces, step = lax.optimization_barrier((first_pieces, step))
    first = placed(first_pieces, x_one).reshape(width, cut)
    first_other = lax.ppermute(first, "c", core_swap)
    second_pieces = around(second_z, "x")
    second = placed(second_pieces, x_one).reshape(width, 2 * inner)
    second_other = lax.ppermute(second, "c", core_swap)

    proj = [dot(normed, w).astype(BF16) for w in (first, first_other)]
    parts = 2 * n_x
    share = STATE // parts
    y_local, c_rows, reach, final = local_call(
        scan_kernel,
        (
            jax.ShapeDtypeStruct((length, 2 * inner), F32),
            jax.ShapeDtypeStruct((length, 2 * STATE), BF16),
            jax.ShapeDtypeStruct((length, lanes), F32),
            jax.ShapeDtypeStruct((parts, share, 2 * inner + lanes), BF16),
        ),
        (c_one, *proj, step, rate, taps),
        1,
        (
            pltpu.VMEM((2, length + 16, cut), BF16),
            pltpu.VMEM((2, BLOCK + 8, cut), F32),
            pltpu.VMEM((2, STATE, inner), F32),
            pltpu.VMEM((1, lanes), F32),
        ),
    )

    within_plane = lax.all_to_all(final, ("x", "c"), 0, 0, tiled=True)
    sent = local_call(
        plane_kernel, jax.ShapeDtypeStruct((n_z, share, 2 * inner + lanes), BF16), (within_plane,)
    )
    planes = lax.all_to_all(sent, "z", 0, 0, tiled=True)
    back = local_call(
        enter_kernel,
        jax.ShapeDtypeStruct((parts, share, 2 * inner), BF16),
        (z_one, within_plane, planes),
        1,
    )
    entering = lax.all_to_all(back, ("x", "c"), 0, 0, tiled=True).reshape(STATE, 2 * inner)

    gates = [dot(normed[:length], w[:, :inner]).astype(BF16) for w in (second, second_other)]
    halves = [w[:, inner:] for w in (second, second_other)]
    out_weight = jnp.where(
        c_at == 0, jnp.concatenate(halves, axis=1), jnp.concatenate(halves[::-1], axis=1)
    )
    mixed = local_call(
        gate_kernel,
        jax.ShapeDtypeStruct((length, 2 * inner), BF16),
        (c_one, y_local, c_rows, reach, entering, *gates, here(out_gain, 2 * inner).reshape(1, -1)),
        1,
    ).reshape(n_y, rows, 2 * inner)

    def partial(k):
        share_rows = lax.dynamic_index_in_dim(mixed, lax.rem(y_at + k, n_y), 0, keepdims=False)
        return dot_t(share_rows, out_weight).astype(BF16)

    received = [lax.ppermute(partial(k), "y", cycle(n_y, k)) for k in (2, 1, 3)]
    summed = partial(0).astype(F32)
    for piece in received:
        summed = summed + piece.astype(F32)
    return summed.astype(BF16)


def solution(mesh):
    split = Mesh(mesh.devices.reshape(16, 4, 2, mesh.shape["tp"]), ALL)
    sp = ("z", "x", "c")
    in_specs = (
        P(ALL, None), P(), P(sp, "y"), P(sp, "y"), P(sp, "y"), P(sp, "y"),
        P(), P(), P(), P(), P(), P(), P(), P("y", sp),
    )
    return jax.shard_map(
        body, mesh=split, in_specs=in_specs, out_specs=P(ALL, None), check_vma=False
    )
```

time: 425 us -> 254 us (0.60)
  the two profiles are of different devices: /device:TPU:4 before, /device:TPU:64 now
where the time goes in v1:
time: 254 us; the launch traced here: 252 us
  waiting for transfers between devices  95.8 us (38%)
  starting transfers between devices  90.9 us (36%)
  matrix products  21.9 us (9%)
  Pallas kernels  19.5 us (8%)
  local copies, waits for them, and re-layouts  11.9 us (5%)
  blocking collectives  10.9 us (4%)
    ppermute x9, starting transfers between devices, around(): lax.ppermute(value, axis, cycle(count, k))  33.3 us
    ppermute x9, waiting for transfers between devices, around(): lax.ppermute(value, axis, cycle(count, k))  27.3 us
    ppermute x3, waiting for transfers between devices, body(): received = [lax.ppermute(partial(k), 'y', cycle(n_y, k)) for k in (2, 1, 3)]  25.7 us
    all_to_all x2, starting transfers between devices, to_all(): lax.all_to_all(jnp.broadcast_to(value, (copies, *value.shape)), axis, 0,...  22.8 us
    pallas_call x7, Pallas kernels, local_call(): pl.pallas_call(kernel, out_shape=outs, in_specs=[SMEM] * scalars + [VMEM]...  19.5 us
    all_to_all x1, waiting for transfers between devices, body(): planes = lax.all_to_all(sent, 'z', 0, 0, tiled=True)  15.2 us
    dot_general x5, matrix products, dot(): return jnp.dot(a, b, preferred_element_type=F32)  13.6 us
    all_to_all x2, waiting for transfers between devices, to_all(): lax.all_to_all(jnp.broadcast_to(value, (copies, *value.shape)), axis, 0,...  13.5 us
  transfers between devices with their start and end apart: 21, of which 14 were waited for; matrix products, arithmetic and copies ran while one was open for 9% of the time, Pallas kernels for 6%

profile of v1, /device:TPU:64, one launch (start us, length us, event | category | flops | bytes accessed | tf_op | source)
XLA Modules:
  0.0 252.2 jit_solution(7395613181868532811)
XLA Ops:
  5.5 14.8 %all-to-all-start = ((bf16[16,32,512]{2,1,0:T(8,128)(2,1)}), bf16[16,32,512]{2,1,0:T(8,128)(2,1)S(1)}, u32[]{:S(2)}, u32[]{:S(2)}) async-start(bf16[16,32,512]{2,1,0:T(8,128)(2,1)} %broadcast_in_dim.7), calls=%async_computation | async-start | bytes 1048576 | tf_op jit(solution)/shard_map/all_to_all | solution.py:42
  20.3 4.9 %collective-permute-start.2 = (bf16[160,2048]{1,0:T(8,128)(2,1)}, bf16[160,2048]{1,0:T(8,128)(2,1)S(1)}, u32[]{:S(2)}, u32[]{:S(2)}) collective-permute-start(bf16[160,2048]{1,0:T(8,128)(2,1)} %refs_0_.1), channel_id=1, source_target_pairs={{0,3},{1,0},{2,1},{3,2},{4,7},{5,4},{6,5},{7,6},{8,11},{9,8},{10,9... | collective-permute-start | bytes 1966088 | tf_op jit(solution)/shard_map/ppermute | solution.py:63
  34.5 13.5 %all-to-all-done.refs_0_ = bf16[16,32,512]{2,1,0:T(8,128)(2,1)S(1)} async-done(((bf16[16,32,512]{2,1,0:T(8,128)(2,1)}), bf16[16,32,512]{2,1,0:T(8,128)(2,1)S(1)}, u32[]{:S(2)}, u32[]{:S(2)}) %all-to-all-start) | async-done | bytes 524320 | tf_op jit(solution)/shard_map/all_to_all | solution.py:42
  48.8 8.0 %all-to-all-start.4 = ((bf16[16,32,512]{2,1,0:T(8,128)(2,1)}), bf16[16,32,512]{2,1,0:T(8,128)(2,1)S(1)}, u32[]{:S(2)}, u32[]{:S(2)}) async-start(bf16[16,32,512]{2,1,0:T(8,128)(2,1)} %broadcast_in_dim.8), calls=%async_computation.4 | async-start | bytes 1048576 | tf_op jit(solution)/shard_map/all_to_all | solution.py:42
  61.7 3.4 %collective-permute-start.5 = (bf16[16,32,512]{2,1,0:T(8,128)(2,1)S(1)}, bf16[16,32,512]{2,1,0:T(8,128)(2,1)}, u32[]{:S(2)}, u32[]{:S(2)}) collective-permute-start(bf16[16,32,512]{2,1,0:T(8,128)(2,1)S(1)} %all-to-all-done.refs_0_), channel_id=1, source_target_pairs={{0,8},{8,16},{16,24},{24,0},{1,9},{9,17},{17,25},{25,1},{2,10},{10... | collective-permute-start | bytes 1572872 | tf_op jit(solution)/shard_map/ppermute | solution.py:63
  65.1 4.6 %collective-permute-start.6 = (bf16[16,32,512]{2,1,0:T(8,128)(2,1)S(1)}, bf16[16,32,512]{2,1,0:T(8,128)(2,1)}, u32[]{:S(2)}, u32[]{:S(2)}) collective-permute-start(bf16[16,32,512]{2,1,0:T(8,128)(2,1)S(1)} %all-to-all-done.refs_0_), channel_id=1, source_target_pairs={{0,16},{8,24},{16,0},{24,8},{1,17},{9,25},{17,1},{25,9},{2,18},{10... | collective-permute-start | bytes 1572872 | tf_op jit(solution)/shard_map/ppermute | solution.py:63
  69.8 3.3 %collective-permute-start.7 = (bf16[16,32,512]{2,1,0:T(8,128)(2,1)S(1)}, bf16[16,32,512]{2,1,0:T(8,128)(2,1)}, u32[]{:S(2)}, u32[]{:S(2)}) collective-permute-start(bf16[16,32,512]{2,1,0:T(8,128)(2,1)S(1)} %all-to-all-done.refs_0_), channel_id=1, source_target_pairs={{0,24},{8,0},{16,8},{24,16},{1,25},{9,1},{17,9},{25,17},{2,26},{10... | collective-permute-start | bytes 1572872 | tf_op jit(solution)/shard_map/ppermute | solution.py:63
  73.3 8.7 %collective-permute-done.3.tail = bf16[16,2048]{1,0:T(8,128)(2,1)S(1)} collective-permute-done((bf16[16,2048]{1,0:T(8,128)(2,1)S(1)}, bf16[16,2048]{1,0:T(8,128)(2,1)S(1)}, u32[]{:S(2)}, u32[]{:S(2)}) %collective-permute-start.3) | collective-permute-done | bytes 65568 | tf_op jit(solution)/shard_map/ppermute | solution.py:289
  86.1 5.6 %collective-permute-done.6.refs_2_ = bf16[16,32,512]{2,1,0:T(8,128)(2,1)} collective-permute-done((bf16[16,32,512]{2,1,0:T(8,128)(2,1)S(1)}, bf16[16,32,512]{2,1,0:T(8,128)(2,1)}, u32[]{:S(2)}, u32[]{:S(2)}) %collective-permute-start.6) | collective-permute-done | bytes 524320 | tf_op jit(solution)/shard_map/ppermute | solution.py:63
  98.4 4.6 %collective-permute-start.10 = (bf16[16,32,512]{2,1,0:T(8,128)(2,1)S(1)}, bf16[16,32,512]{2,1,0:T(8,128)(2,1)S(1)}, u32[]{:S(2)}, u32[]{:S(2)}) collective-permute-start(bf16[16,32,512]{2,1,0:T(8,128)(2,1)S(1)} %all-to-all-done.4.refs_0_), channel_id=1, source_target_pairs={{0,8},{8,16},{16,24},{24,0},{1,9},{9,17},{17,25},{25,1},{2,10},{10... | collective-permute-start | bytes 1572872 | tf_op jit(solution)/shard_map/ppermute | solution.py:63
  103.0 3.6 %collective-permute-start.11 = (bf16[16,32,512]{2,1,0:T(8,128)(2,1)S(1)}, bf16[16,32,512]{2,1,0:T(8,128)(2,1)S(1)}, u32[]{:S(2)}, u32[]{:S(2)}) collective-permute-start(bf16[16,32,512]{2,1,0:T(8,128)(2,1)S(1)} %all-to-all-done.4.refs_0_), channel_id=1, source_target_pairs={{0,16},{8,24},{16,0},{24,8},{1,17},{9,25},{17,1},{25,9},{2,18},{10... | collective-permute-start | bytes 1572872 | tf_op jit(solution)/shard_map/ppermute | solution.py:63
  106.6 3.4 %collective-permute-start.12 = (bf16[16,32,512]{2,1,0:T(8,128)(2,1)S(1)}, bf16[16,32,512]{2,1,0:T(8,128)(2,1)S(1)}, u32[]{:S(2)}, u32[]{:S(2)}) collective-permute-start(bf16[16,32,512]{2,1,0:T(8,128)(2,1)S(1)} %all-to-all-done.4.refs_0_), channel_id=1, source_target_pairs={{0,24},{8,0},{16,8},{24,16},{1,25},{9,1},{17,9},{25,17},{2,26},{10... | collective-permute-start | bytes 1572872 | tf_op jit(solution)/shard_map/ppermute | solution.py:63
  111.6 4.1 %collective-permute-done.10.refs_1_ = bf16[16,32,512]{2,1,0:T(8,128)(2,1)S(1)} collective-permute-done((bf16[16,32,512]{2,1,0:T(8,128)(2,1)S(1)}, bf16[16,32,512]{2,1,0:T(8,128)(2,1)S(1)}, u32[]{:S(2)}, u32[]{:S(2)}) %collective-permute-start.10) | collective-permute-done | bytes 524320 | tf_op jit(solution)/shard_map/ppermute | solution.py:63
  115.7 12.4 %collective-permute-done.11.refs_2_ = bf16[16,32,512]{2,1,0:T(8,128)(2,1)S(1)} collective-permute-done((bf16[16,32,512]{2,1,0:T(8,128)(2,1)S(1)}, bf16[16,32,512]{2,1,0:T(8,128)(2,1)S(1)}, u32[]{:S(2)}, u32[]{:S(2)}) %collective-permute-start.11) | collective-permute-done | bytes 524320 | tf_op jit(solution)/shard_map/ppermute | solution.py:63
  134.7 3.1 %convolution_convert_fusion.4.other = bf16[656,512]{1,0:T(8,128)(2,1)S(1)} fusion(bf16[656,2048]{1,0:T(8,128)(2,1)S(1)} %copy-done.2, bf16[2048,512]{1,0:T(8,128)(2,1)} %collective-permute-done.8), kind=kOutput, calls=%fused_computation.16 | convolution fusion | flops 1376067584 | bytes 5455872 | tf_op jit(solution)/shard_map/dot_general | solution.py:240
  137.9 8.2 %shard_map.138 = (f32[640,512]{1,0:T(8,128)S(1)}, bf16[640,256]{1,0:T(8,128)(2,1)S(1)}, f32[640,128]{1,0:T(8,128)S(1)}, bf16[8,16,640]{2,1,0:T(8,128)(2,1)S(1)}) custom-call(s32[1]{0:T(128)} %bitcast.core, bf16[656,512]{1,0:T(8,128)(2,1)S(1)} %convolution_convert_fusion.5.own, bf16[656,512]{1,0:T(8,128)(2,1)S(1)} %convolution_convert_fusion.4.other, ...), custom_call_target="tpu_custom_call" | custom-call | tf_op jit(solution)/shard_map/pallas_call | solution.py:31
  148.7 10.9 %all_to_all.25.pieces = bf16[8,16,640]{2,1,0:T(8,128)(2,1)S(1)} all-to-all(bf16[8,16,640]{2,1,0:T(8,128)(2,1)S(1)} %get-tuple-element.23), channel_id=1, replica_groups=mesh['z'=16,'x'=4,'c'=2,'y'=4] {'x','c'}, dimensions={0} | all-to-all | bytes 327680 | tf_op jit(solution)/shard_map/all_to_all | solution.py:341
  160.5 12.0 %all-to-all-start.2 = ((bf16[16,16,640]{2,1,0:T(8,128)(2,1)}), bf16[16,16,640]{2,1,0:T(8,128)(2,1)S(1)}, u32[]{:S(2)}, u32[]{:S(2)}) async-start(bf16[16,16,640]{2,1,0:T(8,128)(2,1)} %shard_map.139), calls=%async_computation.2 | async-start | bytes 655360 | tf_op jit(solution)/shard_map/all_to_all | solution.py:345
  174.4 3.4 %fusion.11.gate_own = bf16[640,256]{1,0:T(8,128)(2,1)} fusion(bf16[656,2048]{1,0:T(8,128)(2,1)} %copy-done.1, bf16[2048,512]{1,0:T(8,128)(2,1)S(1)} %bitcast.45), kind=kOutput, calls=%fused_computation.18 | convolution fusion | flops 671252480 | bytes 3997696 | tf_op jit(solution)/shard_map/dot_general | solution.py:240
  177.7 15.2 %all-to-all-done.2.planes = bf16[16,16,640]{2,1,0:T(8,128)(2,1)S(1)} async-done(((bf16[16,16,640]{2,1,0:T(8,128)(2,1)}), bf16[16,16,640]{2,1,0:T(8,128)(2,1)S(1)}, u32[]{:S(2)}, u32[]{:S(2)}) %all-to-all-start.2) | async-done | bytes 327712 | tf_op jit(solution)/shard_map/all_to_all | solution.py:345
  194.0 4.0 %all-to-all-start.3 = ((bf16[8,16,512]{2,1,0:T(8,128)(2,1)}), bf16[8,16,512]{2,1,0:T(8,128)(2,1)}, u32[]{:S(2)}, u32[]{:S(2)}) async-start(bf16[8,16,512]{2,1,0:T(8,128)(2,1)} %shard_map.140), calls=%async_computation.3 | async-start | bytes 262144 | tf_op jit(solution)/shard_map/all_to_all | solution.py:352
  204.1 3.7 %shard_map.142 = bf16[640,512]{1,0:T(8,128)(2,1)S(1)} custom-call(s32[1]{0:T(128)} %bitcast.core, f32[640,512]{1,0:T(8,128)S(1)} %copy-done.4, bf16[640,256]{1,0:T(8,128)(2,1)S(1)} %copy-done.7, f32[640,128]{1,0:T(8,128)S(1)} %copy-done.9, bf16[128,512]{1,0:T(8,128)(2,1)} %bitcast.13.entering, bf16[640,256]{1,0:T(8,128)(2,1)S(1)} %copy-done.10, ...), custom_call_target="tpu_custom_call" | custom-call | tf_op jit(solution)/shard_map/pallas_call | solution.py:31
  223.4 7.2 %collective-permute-done.16 = bf16[160,2048]{1,0:T(8,128)(2,1)S(1)} collective-permute-done((bf16[160,2048]{1,0:T(8,128)(2,1)}, bf16[160,2048]{1,0:T(8,128)(2,1)S(1)}, u32[]{:S(2)}, u32[]{:S(2)}) %collective-permute-start.16) | collective-permute-done | bytes 655392 | tf_op jit(solution)/shard_map/ppermute | solution.py:370
  230.6 18.5 %collective-permute-done.15 = bf16[160,2048]{1,0:T(8,128)(2,1)} collective-permute-done((bf16[160,2048]{1,0:T(8,128)(2,1)}, bf16[160,2048]{1,0:T(8,128)(2,1)}, u32[]{:S(2)}, u32[]{:S(2)}) %collective-permute-start.15) | collective-permute-done | bytes 655392 | tf_op jit(solution)/shard_map/ppermute | solution.py:370
  (88 shorter events, 70.4 us)
Async XLA Ops:
  0.0 73.1 %copy-start = (bf16[2048,32]{0,1:T(8,128)(2,1)S(1)}, bf16[2048,32]{0,1:T(8,128)(2,1)}, u32[]{:S(2)}) copy-start(bf16[2048,32]{0,1:T(8,128)(2,1)} %param.20) | copy-start | bytes 393220
  0.0 73.2 %copy-start.14 = (f32[32]{0:T(128)S(1)}, f32[32]{0:T(128)}, u32[]{:S(2)}) copy-start(f32[32]{0:T(128)} %param.24) | copy-start | bytes 388
  0.0 82.0 %copy-start.11 = (f32[2048]{0:T(1024)S(1)}, f32[2048]{0:T(1024)}, u32[]{:S(2)}) copy-start(f32[2048]{0:T(1024)} %param.15) | copy-start | bytes 24580
  1.6 3.1 %collective-permute-start.4 = (bf16[16,512]{1,0:T(8,128)(2,1)S(1)}, bf16[16,512]{1,0:T(8,128)(2,1)S(1)}, u32[]{:S(2)}, u32[]{:S(2)}) collective-permute-start(bf16[16,512]{1,0:T(8,128)(2,1)S(1)} %pad_maximum_fusion), channel_id=1, source_target_pairs={{0,4},{4,0},{1,5},{5,1},{2,6},{6,2},{3,7},{7,3},{8,12},{12,8},{9,1... | collective-permute-start | bytes 49160 | tf_op jit(solution)/shard_map/ppermute | solution.py:272
  5.5 42.5 %all-to-all-start = ((bf16[16,32,512]{2,1,0:T(8,128)(2,1)}), bf16[16,32,512]{2,1,0:T(8,128)(2,1)S(1)}, u32[]{:S(2)}, u32[]{:S(2)}) async-start(bf16[16,32,512]{2,1,0:T(8,128)(2,1)} %broadcast_in_dim.7), calls=%async_computation | async-start | bytes 1048576 | tf_op jit(solution)/shard_map/all_to_all | solution.py:42
  20.3 36.6 %collective-permute-start.2 = (bf16[160,2048]{1,0:T(8,128)(2,1)}, bf16[160,2048]{1,0:T(8,128)(2,1)S(1)}, u32[]{:S(2)}, u32[]{:S(2)}) collective-permute-start(bf16[160,2048]{1,0:T(8,128)(2,1)} %refs_0_.1), channel_id=1, source_target_pairs={{0,3},{1,0},{2,1},{3,2},{4,7},{5,4},{6,5},{7,6},{8,11},{9,8},{10,9... | collective-permute-start | bytes 1966088 | tf_op jit(solution)/shard_map/ppermute | solution.py:63
  25.2 31.7 %collective-permute-start.1 = (bf16[160,2048]{1,0:T(8,128)(2,1)}, bf16[160,2048]{1,0:T(8,128)(2,1)S(1)}, u32[]{:S(2)}, u32[]{:S(2)}) collective-permute-start(bf16[160,2048]{1,0:T(8,128)(2,1)} %refs_0_.1), channel_id=1, source_target_pairs={{0,2},{1,3},{2,0},{3,1},{4,6},{5,7},{6,4},{7,5},{8,10},{9,11},{10,... | collective-permute-start | bytes 1966088 | tf_op jit(solution)/shard_map/ppermute | solution.py:63
  27.8 31.2 %collective-permute-start = (bf16[160,2048]{1,0:T(8,128)(2,1)}, bf16[160,2048]{1,0:T(8,128)(2,1)}, u32[]{:S(2)}, u32[]{:S(2)}) collective-permute-start(bf16[160,2048]{1,0:T(8,128)(2,1)} %refs_0_.1), channel_id=1, source_target_pairs={{0,1},{1,2},{2,3},{3,0},{4,5},{5,6},{6,7},{7,4},{8,9},{9,10},{10,1... | collective-permute-start | bytes 1966088 | tf_op jit(solution)/shard_map/ppermute | solution.py:63
  31.4 3.1 %collective-permute-start.9 = (bf16[16,512]{1,0:T(8,128)(2,1)S(1)}, bf16[16,512]{1,0:T(8,128)(2,1)S(1)}, u32[]{:S(2)}, u32[]{:S(2)}) collective-permute-start(bf16[16,512]{1,0:T(8,128)(2,1)S(1)} %pad_maximum_fusion.2), channel_id=1, source_target_pairs={{0,4},{4,0},{1,5},{5,1},{2,6},{6,2},{3,7},{7,3},{8,12},{12,8},{9,1... | collective-permute-start | bytes 49160 | tf_op jit(solution)/shard_map/ppermute | solution.py:272
  48.8 49.5 %all-to-all-start.4 = ((bf16[16,32,512]{2,1,0:T(8,128)(2,1)}), bf16[16,32,512]{2,1,0:T(8,128)(2,1)S(1)}, u32[]{:S(2)}, u32[]{:S(2)}) async-start(bf16[16,32,512]{2,1,0:T(8,128)(2,1)} %broadcast_in_dim.8), calls=%async_computation.4 | async-start | bytes 1048576 | tf_op jit(solution)/shard_map/all_to_all | solution.py:42
  59.8 22.2 %collective-permute-start.3 = (bf16[16,2048]{1,0:T(8,128)(2,1)S(1)}, bf16[16,2048]{1,0:T(8,128)(2,1)S(1)}, u32[]{:S(2)}, u32[]{:S(2)}) collective-permute-start(bf16[16,2048]{1,0:T(8,128)(2,1)S(1)} %fusion.35), channel_id=1, source_target_pairs={{0,4},{4,8},{8,12},{12,16},{16,20},{20,24},{24,28},{28,32},{32,36}... | collective-permute-start | bytes 196616 | tf_op jit(solution)/shard_map/ppermute | solution.py:289
  61.7 24.4 %collective-permute-start.5 = (bf16[16,32,512]{2,1,0:T(8,128)(2,1)S(1)}, bf16[16,32,512]{2,1,0:T(8,128)(2,1)}, u32[]{:S(2)}, u32[]{:S(2)}) collective-permute-start(bf16[16,32,512]{2,1,0:T(8,128)(2,1)S(1)} %all-to-all-done.refs_0_), channel_id=1, source_target_pairs={{0,8},{8,16},{16,24},{24,0},{1,9},{9,17},{17,25},{25,1},{2,10},{10... | collective-permute-start | bytes 1572872 | tf_op jit(solution)/shard_map/ppermute | solution.py:63
  65.1 26.6 %collective-permute-start.6 = (bf16[16,32,512]{2,1,0:T(8,128)(2,1)S(1)}, bf16[16,32,512]{2,1,0:T(8,128)(2,1)}, u32[]{:S(2)}, u32[]{:S(2)}) collective-permute-start(bf16[16,32,512]{2,1,0:T(8,128)(2,1)S(1)} %all-to-all-done.refs_0_), channel_id=1, source_target_pairs={{0,16},{8,24},{16,0},{24,8},{1,17},{9,25},{17,1},{25,9},{2,18},{10... | collective-permute-start | bytes 1572872 | tf_op jit(solution)/shard_map/ppermute | solution.py:63
  69.8 23.7 %collective-permute-start.7 = (bf16[16,32,512]{2,1,0:T(8,128)(2,1)S(1)}, bf16[16,32,512]{2,1,0:T(8,128)(2,1)}, u32[]{:S(2)}, u32[]{:S(2)}) collective-permute-start(bf16[16,32,512]{2,1,0:T(8,128)(2,1)S(1)} %all-to-all-done.refs_0_), channel_id=1, source_target_pairs={{0,24},{8,0},{16,8},{24,16},{1,25},{9,1},{17,9},{25,17},{2,26},{10... | collective-permute-start | bytes 1572872 | tf_op jit(solution)/shard_map/ppermute | solution.py:63
  96.3 38.4 %collective-permute-start.8 = (bf16[2048,512]{1,0:T(8,128)(2,1)}, bf16[2048,512]{1,0:T(8,128)(2,1)}, u32[]{:S(2)}, u32[]{:S(2)}) collective-permute-start(bf16[2048,512]{1,0:T(8,128)(2,1)} %bitcast.4), channel_id=1, source_target_pairs={{0,4},{4,0},{1,5},{5,1},{2,6},{6,2},{3,7},{7,3},{8,12},{12,8},{9,1... | collective-permute-start | bytes 6291464 | tf_op jit(solution)/shard_map/ppermute | solution.py:315
  98.4 17.3 %collective-permute-start.10 = (bf16[16,32,512]{2,1,0:T(8,128)(2,1)S(1)}, bf16[16,32,512]{2,1,0:T(8,128)(2,1)S(1)}, u32[]{:S(2)}, u32[]{:S(2)}) collective-permute-start(bf16[16,32,512]{2,1,0:T(8,128)(2,1)S(1)} %all-to-all-done.4.refs_0_), channel_id=1, source_target_pairs={{0,8},{8,16},{16,24},{24,0},{1,9},{9,17},{17,25},{25,1},{2,10},{10... | collective-permute-start | bytes 1572872 | tf_op jit(solution)/shard_map/ppermute | solution.py:63
  103.0 25.1 %collective-permute-start.11 = (bf16[16,32,512]{2,1,0:T(8,128)(2,1)S(1)}, bf16[16,32,512]{2,1,0:T(8,128)(2,1)S(1)}, u32[]{:S(2)}, u32[]{:S(2)}) collective-permute-start(bf16[16,32,512]{2,1,0:T(8,128)(2,1)S(1)} %all-to-all-done.4.refs_0_), channel_id=1, source_target_pairs={{0,16},{8,24},{16,0},{24,8},{1,17},{9,25},{17,1},{25,9},{2,18},{10... | collective-permute-start | bytes 1572872 | tf_op jit(solution)/shard_map/ppermute | solution.py:63
  106.6 22.9 %collective-permute-start.12 = (bf16[16,32,512]{2,1,0:T(8,128)(2,1)S(1)}, bf16[16,32,512]{2,1,0:T(8,128)(2,1)S(1)}, u32[]{:S(2)}, u32[]{:S(2)}) collective-permute-start(bf16[16,32,512]{2,1,0:T(8,128)(2,1)S(1)} %all-to-all-done.4.refs_0_), channel_id=1, source_target_pairs={{0,24},{8,0},{16,8},{24,16},{1,25},{9,1},{17,9},{25,17},{2,26},{10... | collective-permute-start | bytes 1572872 | tf_op jit(solution)/shard_map/ppermute | solution.py:63
  129.6 68.4 %collective-permute-start.13 = (bf16[2048,512]{1,0:T(8,128)(2,1)S(1)}, bf16[2048,512]{1,0:T(8,128)(2,1)}, u32[]{:S(2)}, u32[]{:S(2)}) collective-permute-start(bf16[2048,512]{1,0:T(8,128)(2,1)S(1)} %bitcast.43), channel_id=1, source_target_pairs={{0,4},{4,0},{1,5},{5,1},{2,6},{6,2},{3,7},{7,3},{8,12},{12,8},{9,1... | collective-permute-start | bytes 6291464 | tf_op jit(solution)/shard_map/ppermute | solution.py:318
  160.5 32.4 %all-to-all-start.2 = ((bf16[16,16,640]{2,1,0:T(8,128)(2,1)}), bf16[16,16,640]{2,1,0:T(8,128)(2,1)S(1)}, u32[]{:S(2)}, u32[]{:S(2)}) async-start(bf16[16,16,640]{2,1,0:T(8,128)(2,1)} %shard_map.139), calls=%async_computation.2 | async-start | bytes 655360 | tf_op jit(solution)/shard_map/all_to_all | solution.py:345
  194.0 10.1 %all-to-all-start.3 = ((bf16[8,16,512]{2,1,0:T(8,128)(2,1)}), bf16[8,16,512]{2,1,0:T(8,128)(2,1)}, u32[]{:S(2)}, u32[]{:S(2)}) async-start(bf16[8,16,512]{2,1,0:T(8,128)(2,1)} %shard_map.140), calls=%async_computation.3 | async-start | bytes 262144 | tf_op jit(solution)/shard_map/all_to_all | solution.py:352
  210.9 19.7 %collective-permute-start.16 = (bf16[160,2048]{1,0:T(8,128)(2,1)}, bf16[160,2048]{1,0:T(8,128)(2,1)S(1)}, u32[]{:S(2)}, u32[]{:S(2)}) collective-permute-start(bf16[160,2048]{1,0:T(8,128)(2,1)} %convolution_convert_fusion), channel_id=1, source_target_pairs={{0,3},{1,0},{2,1},{3,2},{4,7},{5,4},{6,5},{7,6},{8,11},{9,8},{10,9... | collective-permute-start | bytes 1966088 | tf_op jit(solution)/shard_map/ppermute | solution.py:370
  215.5 33.6 %collective-permute-start.15 = (bf16[160,2048]{1,0:T(8,128)(2,1)}, bf16[160,2048]{1,0:T(8,128)(2,1)}, u32[]{:S(2)}, u32[]{:S(2)}) collective-permute-start(bf16[160,2048]{1,0:T(8,128)(2,1)} %convolution_convert_fusion.1), channel_id=1, source_target_pairs={{0,1},{1,2},{2,3},{3,0},{4,5},{5,6},{6,7},{7,4},{8,9},{9,10},{10,1... | collective-permute-start | bytes 1966088 | tf_op jit(solution)/shard_map/ppermute | solution.py:370
  220.4 28.7 %collective-permute-start.14 = (bf16[160,2048]{1,0:T(8,128)(2,1)}, bf16[160,2048]{1,0:T(8,128)(2,1)}, u32[]{:S(2)}, u32[]{:S(2)}) collective-permute-start(bf16[160,2048]{1,0:T(8,128)(2,1)} %convolution_convert_fusion.2), channel_id=1, source_target_pairs={{0,2},{1,3},{2,0},{3,1},{4,6},{5,7},{6,4},{7,5},{8,10},{9,11},{10,... | collective-permute-start | bytes 1966088 | tf_op jit(solution)/shard_map/ppermute | solution.py:370
  (13 other events, 162.5 us)

commit v2 on v1

--- a/solution.py
+++ b/solution.py
@@ -14,6 +14,7 @@
 F32 = jnp.float32
 BF16 = jnp.bfloat16
 ALL = ("z", "x", "c", "y")
+
 
 SMEM = pl.BlockSpec(memory_space=pltpu.SMEM)
 VMEM = pl.BlockSpec(memory_space=pltpu.VMEM)
@@ -279,6 +280,25 @@
     first_source = halves_swapped(w_x, w_b, w_c)
     pieces = around(tokens, "y")
     first_z = to_all(first_source, "z", n_z)
+
+    def here(v, size):
+        return lax.dynamic_slice_in_dim(v, y_at * size, size, v.ndim - 1)
+
+    lanes = 128
+    dt_weight = jnp.pad(here(w_dt, heads), ((0, 0), (0, lanes - heads)))
+    bias = jnp.pad(here(dt_bias, heads), (0, lanes - heads))
+    rate = jnp.pad(jnp.exp(here(a_log, heads)), (0, lanes - heads)).reshape(1, lanes)
+    taps = jnp.concatenate(
+        [
+            here(v, 2 * size).reshape(CONV, 2, size).swapaxes(0, 1)
+            for v, size in ((conv_x, inner), (conv_b, state), (conv_c, state))
+        ],
+        axis=2,
+    )
+    gain = here(out_gain, 2 * inner).reshape(1, -1)
+    first_z, taps, rate, bias, dt_weight, gain = lax.optimization_barrier(
+        (first_z, taps, rate, bias, dt_weight, gain)
+    )
     first_pieces = around(first_z, "x")
     second_source = halves_swapped(w_z, w_out.T)
     second_source, first_z = lax.optimization_barrier((second_source, first_z))
@@ -294,29 +314,10 @@
         1,
     )
 
-    def here(v, size):
-        return lax.dynamic_slice_in_dim(v, y_at * size, size, v.ndim - 1)
-
-    lanes = 128
-    dt_weight = jnp.pad(here(w_dt, heads), ((0, 0), (0, lanes - heads)))
-    bias = jnp.pad(here(dt_bias, heads), (0, lanes - heads))
-    rate = jnp.pad(jnp.exp(here(a_log, heads)), (0, lanes - heads)).reshape(1, lanes)
     step = jax.nn.softplus(dot(normed[:length], dt_weight) + bias)
-    taps = jnp.concatenate(
-        [
-            here(v, 2 * size).reshape(CONV, 2, size).swapaxes(0, 1)
-            for v, size in ((conv_x, inner), (conv_b, state), (conv_c, state))
-        ],
-        axis=2,
-    )
-
     first_pieces, step = lax.optimization_barrier((first_pieces, step))
     first = placed(first_pieces, x_one).reshape(width, cut)
     first_other = lax.ppermute(first, "c", core_swap)
-    second_pieces = around(second_z, "x")
-    second = placed(second_pieces, x_one).reshape(width, 2 * inner)
-    second_other = lax.ppermute(second, "c", core_swap)
-
     proj = [dot(normed, w).astype(BF16) for w in (first, first_other)]
     parts = 2 * n_x
     share = STATE // parts
@@ -338,6 +339,11 @@
         ),
     )
 
+    final, second_z = lax.optimization_barrier((final, second_z))
+    second_pieces = around(second_z, "x")
+    second = placed(second_pieces, x_one).reshape(width, 2 * inner)
+    second_other = lax.ppermute(second, "c", core_swap)
+
     within_plane = lax.all_to_all(final, ("x", "c"), 0, 0, tiled=True)
     sent = local_call(
         plane_kernel, jax.ShapeDtypeStruct((n_z, share, 2 * inner + lanes), BF16), (within_plane,)
@@ -359,19 +365,13 @@
     mixed = local_call(
         gate_kernel,
         jax.ShapeDtypeStruct((length, 2 * inner), BF16),
-        (c_one, y_local, c_rows, reach, entering, *gates, here(out_gain, 2 * inner).reshape(1, -1)),
+        (c_one, y_local, c_rows, reach, entering, *gates, gain),
         1,
-    ).reshape(n_y, rows, 2 * inner)
-
-    def partial(k):
-        share_rows = lax.dynamic_index_in_dim(mixed, lax.rem(y_at + k, n_y), 0, keepdims=False)
-        return dot_t(share_rows, out_weight).astype(BF16)
-
-    received = [lax.ppermute(partial(k), "y", cycle(n_y, k)) for k in (2, 1, 3)]
-    summed = partial(0).astype(F32)
-    for piece in received:
-        summed = summed + piece.astype(F32)
-    return summed.astype(BF16)
+    )
+
+    partial = dot_t(mixed, out_weight).astype(BF16).reshape(n_y, rows, width)
+    shares = lax.all_to_all(partial, "y", 0, 0, tiled=True)
+    return jnp.sum(shares.astype(F32), axis=0).astype(BF16)
 
 
 def solution(mesh):

time: 254 us -> 259 us (1.020)
  the two profiles are of different devices: /device:TPU:64 before, /device:TPU:1 now
where the time goes in v2:
time: 259 us; the launch traced here: 257 us
  starting transfers between devices  104 us (40%)
  waiting for transfers between devices  52 us (20%)
  blocking collectives  44.2 us (17%)
  local copies, waits for them, and re-layouts  19.6 us (8%)
  Pallas kernels  18.4 us (7%)
  matrix products  16.1 us (6%)
    all_to_all x1, blocking collectives, body(): shares = lax.all_to_all(partial, 'y', 0, 0, tiled=True)  34.9 us
    ppermute x9, starting transfers between devices, around(): lax.ppermute(value, axis, cycle(count, k))  31.4 us
    all_to_all x2, starting transfers between devices, to_all(): lax.all_to_all(jnp.broadcast_to(value, (copies, *value.shape)), axis, 0,...  24.4 us
    ppermute x9, waiting for transfers between devices, around(): lax.ppermute(value, axis, cycle(count, k))  20.1 us
    pallas_call x7, Pallas kernels, local_call(): pl.pallas_call(kernel, out_shape=outs, in_specs=[SMEM] * scalars + [VMEM]...  18.4 us
    dot_general x5, matrix products, dot(): return jnp.dot(a, b, preferred_element_type=F32)  14.3 us
    all_to_all x2, waiting for transfers between devices, to_all(): lax.all_to_all(jnp.broadcast_to(value, (copies, *value.shape)), axis, 0,...  14.1 us
    all_to_all x1, starting transfers between devices, body(): planes = lax.all_to_all(sent, 'z', 0, 0, tiled=True)  12.8 us
  transfers between devices with their start and end apart: 18, of which 12 were waited for; matrix products, arithmetic and copies ran while one was open for 8% of the time, Pallas kernels for 5%

profile of v2, /device:TPU:1, one launch (start us, length us, event | category | flops | bytes accessed | tf_op | source)
XLA Modules:
  0.0 257.1 jit_solution(11096207221840167989)
XLA Ops:
  1.5 8.7 %collective-permute-start.4 = (bf16[16,512]{1,0:T(8,128)(2,1)S(1)}, bf16[16,512]{1,0:T(8,128)(2,1)S(1)}, u32[]{:S(2)}, u32[]{:S(2)}) collective-permute-start(bf16[16,512]{1,0:T(8,128)(2,1)S(1)} %pad_maximum_fusion), channel_id=1, source_target_pairs={{0,4},{4,0},{1,5},{5,1},{2,6},{6,2},{3,7},{7,3},{8,12},{12,8},{9,1... | collective-permute-start | bytes 49160 | tf_op jit(solution)/shard_map/ppermute | solution.py:273
  12.0 9.6 %all-to-all-start = ((bf16[16,32,512]{2,1,0:T(8,128)(2,1)}), bf16[16,32,512]{2,1,0:T(8,128)(2,1)S(1)}, u32[]{:S(2)}, u32[]{:S(2)}) async-start(bf16[16,32,512]{2,1,0:T(8,128)(2,1)} %broadcast_in_dim.7), calls=%async_computation | async-start | bytes 1048576 | tf_op jit(solution)/shard_map/all_to_all | solution.py:43
  21.5 4.6 %collective-permute-start.2 = (bf16[160,2048]{1,0:T(8,128)(2,1)}, bf16[160,2048]{1,0:T(8,128)(2,1)S(1)}, u32[]{:S(2)}, u32[]{:S(2)}) collective-permute-start(bf16[160,2048]{1,0:T(8,128)(2,1)} %refs_0_.1), channel_id=1, source_target_pairs={{0,3},{1,0},{2,1},{3,2},{4,7},{5,4},{6,5},{7,6},{8,11},{9,8},{10,9... | collective-permute-start | bytes 1966088 | tf_op jit(solution)/shard_map/ppermute | solution.py:64
  35.6 8.6 %all-to-all-done.refs_0_ = bf16[16,32,512]{2,1,0:T(8,128)(2,1)S(1)} async-done(((bf16[16,32,512]{2,1,0:T(8,128)(2,1)}), bf16[16,32,512]{2,1,0:T(8,128)(2,1)S(1)}, u32[]{:S(2)}, u32[]{:S(2)}) %all-to-all-start) | async-done | bytes 524320 | tf_op jit(solution)/shard_map/all_to_all | solution.py:43
  44.3 3.1 %collective-permute-start.5 = (bf16[16,32,512]{2,1,0:T(8,128)(2,1)S(1)}, bf16[16,32,512]{2,1,0:T(8,128)(2,1)}, u32[]{:S(2)}, u32[]{:S(2)}) collective-permute-start(bf16[16,32,512]{2,1,0:T(8,128)(2,1)S(1)} %all-to-all-done.refs_0_), channel_id=1, source_target_pairs={{0,8},{8,16},{16,24},{24,0},{1,9},{9,17},{17,25},{25,1},{2,10},{10... | collective-permute-start | bytes 1572872 | tf_op jit(solution)/shard_map/ppermute | solution.py:64
  47.4 4.4 %collective-permute-start.6 = (bf16[16,32,512]{2,1,0:T(8,128)(2,1)S(1)}, bf16[16,32,512]{2,1,0:T(8,128)(2,1)}, u32[]{:S(2)}, u32[]{:S(2)}) collective-permute-start(bf16[16,32,512]{2,1,0:T(8,128)(2,1)S(1)} %all-to-all-done.refs_0_), channel_id=1, source_target_pairs={{0,16},{8,24},{16,0},{24,8},{1,17},{9,25},{17,1},{25,9},{2,18},{10... | collective-permute-start | bytes 1572872 | tf_op jit(solution)/shard_map/ppermute | solution.py:64
  53.8 4.4 %collective-permute-start.7 = (bf16[16,32,512]{2,1,0:T(8,128)(2,1)S(1)}, bf16[16,32,512]{2,1,0:T(8,128)(2,1)}, u32[]{:S(2)}, u32[]{:S(2)}) collective-permute-start(bf16[16,32,512]{2,1,0:T(8,128)(2,1)S(1)} %all-to-all-done.refs_0_), channel_id=1, source_target_pairs={{0,24},{8,0},{16,8},{24,16},{1,25},{9,1},{17,9},{25,17},{2,26},{10... | collective-permute-start | bytes 1572872 | tf_op jit(solution)/shard_map/ppermute | solution.py:64
  64.0 4.3 %collective-permute-start.3 = (bf16[16,2048]{1,0:T(8,128)(2,1)S(1)}, bf16[16,2048]{1,0:T(8,128)(2,1)S(1)}, u32[]{:S(2)}, u32[]{:S(2)}) collective-permute-start(bf16[16,2048]{1,0:T(8,128)(2,1)S(1)} %fusion.25), channel_id=1, source_target_pairs={{0,4},{4,8},{8,12},{12,16},{16,20},{20,24},{24,28},{28,32},{32,36}... | collective-permute-start | bytes 196616 | tf_op jit(solution)/shard_map/ppermute | solution.py:309
  87.8 14.9 %all-to-all-start.1 = ((bf16[16,32,512]{2,1,0:T(8,128)(2,1)}), bf16[16,32,512]{2,1,0:T(8,128)(2,1)S(1)}, u32[]{:S(2)}, u32[]{:S(2)}) async-start(bf16[16,32,512]{2,1,0:T(8,128)(2,1)} %broadcast_in_dim.8), calls=%async_computation.1 | async-start | bytes 1048576 | tf_op jit(solution)/shard_map/all_to_all | solution.py:43
  102.7 3.1 %convolution_convert_fusion.2.own = bf16[656,512]{1,0:T(8,128)(2,1)S(1)} fusion(bf16[656,2048]{1,0:T(8,128)(2,1)S(1)} %shard_map.136, bf16[2048,512]{1,0:T(8,128)(2,1)} %bitcast.12), kind=kOutput, calls=%fused_computation.15 | convolution fusion | flops 1376067584 | bytes 5455872 | tf_op jit(solution)/shard_map/dot_general | solution.py:241
  105.9 3.2 %convolution_convert_fusion.1.other = bf16[656,512]{1,0:T(8,128)(2,1)S(1)} fusion(bf16[656,2048]{1,0:T(8,128)(2,1)S(1)} %shard_map.136, bf16[2048,512]{1,0:T(8,128)(2,1)} %collective-permute-done.8), kind=kOutput, calls=%fused_computation.14 | convolution fusion | flops 1376067584 | bytes 5455872 | tf_op jit(solution)/shard_map/dot_general | solution.py:241
  109.0 8.3 %shard_map.138 = (f32[640,512]{1,0:T(8,128)S(1)}, bf16[640,256]{1,0:T(8,128)(2,1)S(1)}, f32[640,128]{1,0:T(8,128)S(1)}, bf16[8,16,640]{2,1,0:T(8,128)(2,1)S(1)}) custom-call(s32[1]{0:T(128)} %bitcast.core, bf16[656,512]{1,0:T(8,128)(2,1)S(1)} %convolution_convert_fusion.2.own, bf16[656,512]{1,0:T(8,128)(2,1)S(1)} %convolution_convert_fusion.1.other, ...), custom_call_target="tpu_custom_call" | custom-call | tf_op jit(solution)/shard_map/pallas_call | solution.py:32
  119.9 5.5 %all-to-all-done.1.refs_0_ = bf16[16,32,512]{2,1,0:T(8,128)(2,1)S(1)} async-done(((bf16[16,32,512]{2,1,0:T(8,128)(2,1)}), bf16[16,32,512]{2,1,0:T(8,128)(2,1)S(1)}, u32[]{:S(2)}, u32[]{:S(2)}) %all-to-all-start.1) | async-done | bytes 524320 | tf_op jit(solution)/shard_map/all_to_all | solution.py:43
  128.2 5.0 %collective-permute-start.11 = (bf16[16,32,512]{2,1,0:T(8,128)(2,1)S(1)}, bf16[16,32,512]{2,1,0:T(8,128)(2,1)S(1)}, u32[]{:S(2)}, u32[]{:S(2)}) collective-permute-start(bf16[16,32,512]{2,1,0:T(8,128)(2,1)S(1)} %all-to-all-done.1.refs_0_), channel_id=1, source_target_pairs={{0,16},{8,24},{16,0},{24,8},{1,17},{9,25},{17,1},{25,9},{2,18},{10... | collective-permute-start | bytes 1572872 | tf_op jit(solution)/shard_map/ppermute | solution.py:64
  136.6 10.4 %collective-permute-done.11.refs_2_ = bf16[16,32,512]{2,1,0:T(8,128)(2,1)S(1)} collective-permute-done((bf16[16,32,512]{2,1,0:T(8,128)(2,1)S(1)}, bf16[16,32,512]{2,1,0:T(8,128)(2,1)S(1)}, u32[]{:S(2)}, u32[]{:S(2)}) %collective-permute-start.11) | collective-permute-done | bytes 524320 | tf_op jit(solution)/shard_map/ppermute | solution.py:64
  147.0 4.2 %collective-permute-done.12.refs_3_ = bf16[16,32,512]{2,1,0:T(8,128)(2,1)S(1)} collective-permute-done((bf16[16,32,512]{2,1,0:T(8,128)(2,1)S(1)}, bf16[16,32,512]{2,1,0:T(8,128)(2,1)S(1)}, u32[]{:S(2)}, u32[]{:S(2)}) %collective-permute-start.12) | collective-permute-done | bytes 524320 | tf_op jit(solution)/shard_map/ppermute | solution.py:64
  151.3 7.4 %collective-permute-start.13 = (bf16[2048,512]{1,0:T(8,128)(2,1)S(1)}, bf16[2048,512]{1,0:T(8,128)(2,1)}, u32[]{:S(2)}, u32[]{:S(2)}) collective-permute-start(bf16[2048,512]{1,0:T(8,128)(2,1)S(1)} %bitcast.33), channel_id=1, source_target_pairs={{0,4},{4,0},{1,5},{5,1},{2,6},{6,2},{3,7},{7,3},{8,12},{12,8},{9,1... | collective-permute-start | bytes 6291464 | tf_op jit(solution)/shard_map/ppermute | solution.py:345
  158.8 9.3 %all_to_all.30.pieces = bf16[8,16,640]{2,1,0:T(8,128)(2,1)S(1)} all-to-all(bf16[8,16,640]{2,1,0:T(8,128)(2,1)S(1)} %get-tuple-element.38), channel_id=1, replica_groups=mesh['z'=16,'x'=4,'c'=2,'y'=4] {'x','c'}, dimensions={0} | all-to-all | bytes 327680 | tf_op jit(solution)/shard_map/all_to_all | solution.py:347
  169.0 12.8 %all-to-all-start.3 = ((bf16[16,16,640]{2,1,0:T(8,128)(2,1)}), bf16[16,16,640]{2,1,0:T(8,128)(2,1)S(1)}, u32[]{:S(2)}, u32[]{:S(2)}) async-start(bf16[16,16,640]{2,1,0:T(8,128)(2,1)} %shard_map.139), calls=%async_computation.3 | async-start | bytes 655360 | tf_op jit(solution)/shard_map/all_to_all | solution.py:351
  182.8 3.4 %fusion.12.gate_own = bf16[640,256]{1,0:T(8,128)(2,1)} fusion(bf16[656,2048]{1,0:T(8,128)(2,1)} %copy-done.1, bf16[2048,512]{1,0:T(8,128)(2,1)S(1)} %bitcast.35), kind=kOutput, calls=%fused_computation.16 | convolution fusion | flops 671252480 | bytes 3997696 | tf_op jit(solution)/shard_map/dot_general | solution.py:241
  186.2 10.7 %all-to-all-done.3.planes = bf16[16,16,640]{2,1,0:T(8,128)(2,1)S(1)} async-done(((bf16[16,16,640]{2,1,0:T(8,128)(2,1)}), bf16[16,16,640]{2,1,0:T(8,128)(2,1)S(1)}, u32[]{:S(2)}, u32[]{:S(2)}) %all-to-all-start.3) | async-done | bytes 327712 | tf_op jit(solution)/shard_map/all_to_all | solution.py:351
  197.9 10.5 %all-to-all-start.4 = ((bf16[8,16,512]{2,1,0:T(8,128)(2,1)}), bf16[8,16,512]{2,1,0:T(8,128)(2,1)}, u32[]{:S(2)}, u32[]{:S(2)}) async-start(bf16[8,16,512]{2,1,0:T(8,128)(2,1)} %shard_map.140), calls=%async_computation.4 | async-start | bytes 262144 | tf_op jit(solution)/shard_map/all_to_all | solution.py:358
  213.9 3.7 %shard_map.142 = bf16[640,512]{1,0:T(8,128)(2,1)S(1)} custom-call(s32[1]{0:T(128)} %bitcast.core, f32[640,512]{1,0:T(8,128)S(1)} %copy-done.3, bf16[640,256]{1,0:T(8,128)(2,1)S(1)} %copy-done.12, f32[640,128]{1,0:T(8,128)S(1)} %copy-done.14, bf16[128,512]{1,0:T(8,128)(2,1)} %bitcast.16.entering, bf16[640,256]{1,0:T(8,128)(2,1)S(1)} %copy-done.15, ...), custom_call_target="tpu_custom_call" | custom-call | tf_op jit(solution)/shard_map/pallas_call | solution.py:32
  220.7 34.9 %all_to_all.31 = bf16[4,160,2048]{2,1,0:T(8,128)(2,1)S(1)} all-to-all(bf16[4,160,2048]{2,1,0:T(8,128)(2,1)S(1)} %bitcast.38), channel_id=1, replica_groups=mesh['z'=16,'x'=4,'c'=2,'y'=4] {'y'}, dimensions={0} | all-to-all | bytes 5242880 | tf_op jit(solution)/shard_map/all_to_all | solution.py:373
  (92 shorter events, 61.7 us)
Async XLA Ops:
  0.0 31.1 %copy-start = (bf16[2048,32]{0,1:T(8,128)(2,1)S(1)}, bf16[2048,32]{0,1:T(8,128)(2,1)}, u32[]{:S(2)}) copy-start(bf16[2048,32]{0,1:T(8,128)(2,1)} %param.20) | copy-start | bytes 393220
  0.0 70.2 %copy-start.17 = (f32[2048]{0:T(1024)S(1)}, f32[2048]{0:T(1024)}, u32[]{:S(2)}) copy-start(f32[2048]{0:T(1024)} %param.15) | copy-start | bytes 24580
  1.5 9.6 %collective-permute-start.4 = (bf16[16,512]{1,0:T(8,128)(2,1)S(1)}, bf16[16,512]{1,0:T(8,128)(2,1)S(1)}, u32[]{:S(2)}, u32[]{:S(2)}) collective-permute-start(bf16[16,512]{1,0:T(8,128)(2,1)S(1)} %pad_maximum_fusion), channel_id=1, source_target_pairs={{0,4},{4,0},{1,5},{5,1},{2,6},{6,2},{3,7},{7,3},{8,12},{12,8},{9,1... | collective-permute-start | bytes 49160 | tf_op jit(solution)/shard_map/ppermute | solution.py:273
  12.0 32.3 %all-to-all-start = ((bf16[16,32,512]{2,1,0:T(8,128)(2,1)}), bf16[16,32,512]{2,1,0:T(8,128)(2,1)S(1)}, u32[]{:S(2)}, u32[]{:S(2)}) async-start(bf16[16,32,512]{2,1,0:T(8,128)(2,1)} %broadcast_in_dim.7), calls=%async_computation | async-start | bytes 1048576 | tf_op jit(solution)/shard_map/all_to_all | solution.py:43
  21.5 32.3 %collective-permute-start.2 = (bf16[160,2048]{1,0:T(8,128)(2,1)}, bf16[160,2048]{1,0:T(8,128)(2,1)S(1)}, u32[]{:S(2)}, u32[]{:S(2)}) collective-permute-start(bf16[160,2048]{1,0:T(8,128)(2,1)} %refs_0_.1), channel_id=1, source_target_pairs={{0,3},{1,0},{2,1},{3,2},{4,7},{5,4},{6,5},{7,6},{8,11},{9,8},{10,9... | collective-permute-start | bytes 1966088 | tf_op jit(solution)/shard_map/ppermute | solution.py:64
  26.2 32.0 %collective-permute-start.1 = (bf16[160,2048]{1,0:T(8,128)(2,1)}, bf16[160,2048]{1,0:T(8,128)(2,1)S(1)}, u32[]{:S(2)}, u32[]{:S(2)}) collective-permute-start(bf16[160,2048]{1,0:T(8,128)(2,1)} %refs_0_.1), channel_id=1, source_target_pairs={{0,2},{1,3},{2,0},{3,1},{4,6},{5,7},{6,4},{7,5},{8,10},{9,11},{10,... | collective-permute-start | bytes 1966088 | tf_op jit(solution)/shard_map/ppermute | solution.py:64
  28.4 32.1 %collective-permute-start = (bf16[160,2048]{1,0:T(8,128)(2,1)}, bf16[160,2048]{1,0:T(8,128)(2,1)S(1)}, u32[]{:S(2)}, u32[]{:S(2)}) collective-permute-start(bf16[160,2048]{1,0:T(8,128)(2,1)} %refs_0_.1), channel_id=1, source_target_pairs={{0,1},{1,2},{2,3},{3,0},{4,5},{5,6},{6,7},{7,4},{8,9},{9,10},{10,1... | collective-permute-start | bytes 1966088 | tf_op jit(solution)/shard_map/ppermute | solution.py:64
  44.3 33.4 %collective-permute-start.5 = (bf16[16,32,512]{2,1,0:T(8,128)(2,1)S(1)}, bf16[16,32,512]{2,1,0:T(8,128)(2,1)}, u32[]{:S(2)}, u32[]{:S(2)}) collective-permute-start(bf16[16,32,512]{2,1,0:T(8,128)(2,1)S(1)} %all-to-all-done.refs_0_), channel_id=1, source_target_pairs={{0,8},{8,16},{16,24},{24,0},{1,9},{9,17},{17,25},{25,1},{2,10},{10... | collective-permute-start | bytes 1572872 | tf_op jit(solution)/shard_map/ppermute | solution.py:64
  47.4 30.3 %collective-permute-start.6 = (bf16[16,32,512]{2,1,0:T(8,128)(2,1)S(1)}, bf16[16,32,512]{2,1,0:T(8,128)(2,1)}, u32[]{:S(2)}, u32[]{:S(2)}) collective-permute-start(bf16[16,32,512]{2,1,0:T(8,128)(2,1)S(1)} %all-to-all-done.refs_0_), channel_id=1, source_target_pairs={{0,16},{8,24},{16,0},{24,8},{1,17},{9,25},{17,1},{25,9},{2,18},{10... | collective-permute-start | bytes 1572872 | tf_op jit(solution)/shard_map/ppermute | solution.py:64
  53.8 23.9 %collective-permute-start.7 = (bf16[16,32,512]{2,1,0:T(8,128)(2,1)S(1)}, bf16[16,32,512]{2,1,0:T(8,128)(2,1)}, u32[]{:S(2)}, u32[]{:S(2)}) collective-permute-start(bf16[16,32,512]{2,1,0:T(8,128)(2,1)S(1)} %all-to-all-done.refs_0_), channel_id=1, source_target_pairs={{0,24},{8,0},{16,8},{24,16},{1,25},{9,1},{17,9},{25,17},{2,26},{10... | collective-permute-start | bytes 1572872 | tf_op jit(solution)/shard_map/ppermute | solution.py:64
  64.0 6.2 %collective-permute-start.3 = (bf16[16,2048]{1,0:T(8,128)(2,1)S(1)}, bf16[16,2048]{1,0:T(8,128)(2,1)S(1)}, u32[]{:S(2)}, u32[]{:S(2)}) collective-permute-start(bf16[16,2048]{1,0:T(8,128)(2,1)S(1)} %fusion.25), channel_id=1, source_target_pairs={{0,4},{4,8},{8,12},{12,16},{16,20},{20,24},{24,28},{28,32},{32,36}... | collective-permute-start | bytes 196616 | tf_op jit(solution)/shard_map/ppermute | solution.py:309
  76.0 29.8 %copy-start.1 = (bf16[656,2048]{1,0:T(8,128)(2,1)}, bf16[656,2048]{1,0:T(8,128)(2,1)S(1)}, u32[]{:S(2)}) copy-start(bf16[656,2048]{1,0:T(8,128)(2,1)S(1)} %shard_map.136) | copy-start | bytes 8060932
  80.6 25.3 %collective-permute-start.8 = (bf16[2048,512]{1,0:T(8,128)(2,1)}, bf16[2048,512]{1,0:T(8,128)(2,1)}, u32[]{:S(2)}, u32[]{:S(2)}) collective-permute-start(bf16[2048,512]{1,0:T(8,128)(2,1)} %bitcast.12), channel_id=1, source_target_pairs={{0,4},{4,0},{1,5},{5,1},{2,6},{6,2},{3,7},{7,3},{8,12},{12,8},{9,1... | collective-permute-start | bytes 6291464 | tf_op jit(solution)/shard_map/ppermute | solution.py:320
  82.5 4.4 %collective-permute-start.9 = (bf16[16,512]{1,0:T(8,128)(2,1)S(1)}, bf16[16,512]{1,0:T(8,128)(2,1)S(1)}, u32[]{:S(2)}, u32[]{:S(2)}) collective-permute-start(bf16[16,512]{1,0:T(8,128)(2,1)S(1)} %pad_maximum_fusion.2), channel_id=1, source_target_pairs={{0,4},{4,0},{1,5},{5,1},{2,6},{6,2},{3,7},{7,3},{8,12},{12,8},{9,1... | collective-permute-start | bytes 49160 | tf_op jit(solution)/shard_map/ppermute | solution.py:273
  87.8 37.6 %all-to-all-start.1 = ((bf16[16,32,512]{2,1,0:T(8,128)(2,1)}), bf16[16,32,512]{2,1,0:T(8,128)(2,1)S(1)}, u32[]{:S(2)}, u32[]{:S(2)}) async-start(bf16[16,32,512]{2,1,0:T(8,128)(2,1)} %broadcast_in_dim.8), calls=%async_computation.1 | async-start | bytes 1048576 | tf_op jit(solution)/shard_map/all_to_all | solution.py:43
  125.4 11.2 %collective-permute-start.10 = (bf16[16,32,512]{2,1,0:T(8,128)(2,1)S(1)}, bf16[16,32,512]{2,1,0:T(8,128)(2,1)S(1)}, u32[]{:S(2)}, u32[]{:S(2)}) collective-permute-start(bf16[16,32,512]{2,1,0:T(8,128)(2,1)S(1)} %all-to-all-done.1.refs_0_), channel_id=1, source_target_pairs={{0,8},{8,16},{16,24},{24,0},{1,9},{9,17},{17,25},{25,1},{2,10},{10... | collective-permute-start | bytes 1572872 | tf_op jit(solution)/shard_map/ppermute | solution.py:64
  128.2 18.9 %collective-permute-start.11 = (bf16[16,32,512]{2,1,0:T(8,128)(2,1)S(1)}, bf16[16,32,512]{2,1,0:T(8,128)(2,1)S(1)}, u32[]{:S(2)}, u32[]{:S(2)}) collective-permute-start(bf16[16,32,512]{2,1,0:T(8,128)(2,1)S(1)} %all-to-all-done.1.refs_0_), channel_id=1, source_target_pairs={{0,16},{8,24},{16,0},{24,8},{1,17},{9,25},{17,1},{25,9},{2,18},{10... | collective-permute-start | bytes 1572872 | tf_op jit(solution)/shard_map/ppermute | solution.py:64
  133.1 18.1 %collective-permute-start.12 = (bf16[16,32,512]{2,1,0:T(8,128)(2,1)S(1)}, bf16[16,32,512]{2,1,0:T(8,128)(2,1)S(1)}, u32[]{:S(2)}, u32[]{:S(2)}) collective-permute-start(bf16[16,32,512]{2,1,0:T(8,128)(2,1)S(1)} %all-to-all-done.1.refs_0_), channel_id=1, source_target_pairs={{0,24},{8,0},{16,8},{24,16},{1,25},{9,1},{17,9},{25,17},{2,26},{10... | collective-permute-start | bytes 1572872 | tf_op jit(solution)/shard_map/ppermute | solution.py:64
  151.3 57.1 %collective-permute-start.13 = (bf16[2048,512]{1,0:T(8,128)(2,1)S(1)}, bf16[2048,512]{1,0:T(8,128)(2,1)}, u32[]{:S(2)}, u32[]{:S(2)}) collective-permute-start(bf16[2048,512]{1,0:T(8,128)(2,1)S(1)} %bitcast.33), channel_id=1, source_target_pairs={{0,4},{4,0},{1,5},{5,1},{2,6},{6,2},{3,7},{7,3},{8,12},{12,8},{9,1... | collective-permute-start | bytes 6291464 | tf_op jit(solution)/shard_map/ppermute | solution.py:345
  169.0 27.9 %all-to-all-start.3 = ((bf16[16,16,640]{2,1,0:T(8,128)(2,1)}), bf16[16,16,640]{2,1,0:T(8,128)(2,1)S(1)}, u32[]{:S(2)}, u32[]{:S(2)}) async-start(bf16[16,16,640]{2,1,0:T(8,128)(2,1)} %shard_map.139), calls=%async_computation.3 | async-start | bytes 655360 | tf_op jit(solution)/shard_map/all_to_all | solution.py:351
  197.9 15.9 %all-to-all-start.4 = ((bf16[8,16,512]{2,1,0:T(8,128)(2,1)}), bf16[8,16,512]{2,1,0:T(8,128)(2,1)}, u32[]{:S(2)}, u32[]{:S(2)}) async-start(bf16[8,16,512]{2,1,0:T(8,128)(2,1)} %shard_map.140), calls=%async_computation.4 | async-start | bytes 262144 | tf_op jit(solution)/shard_map/all_to_all | solution.py:358
  208.4 5.4 %copy-start.3 = (f32[640,512]{1,0:T(8,128)S(1)}, f32[640,512]{1,0:T(8,128)}, u32[]{:S(2)}) copy-start(f32[640,512]{1,0:T(8,128)} %copy-done.2) | copy-start | bytes 3932164
  208.5 5.4 %copy-start.12 = (bf16[640,256]{1,0:T(8,128)(2,1)S(1)}, bf16[640,256]{1,0:T(8,128)(2,1)}, u32[]{:S(2)}) copy-start(bf16[640,256]{1,0:T(8,128)(2,1)} %copy-done.11) | copy-start | bytes 983044
  208.5 5.4 %copy-start.14 = (f32[640,128]{1,0:T(8,128)S(1)}, f32[640,128]{1,0:T(8,128)}, u32[]{:S(2)}) copy-start(f32[640,128]{1,0:T(8,128)} %copy-done.13) | copy-start | bytes 983044
  (15 other events, 29.4 us)

commit v3 on v2

--- a/solution.py
+++ b/solution.py
@@ -37,12 +37,6 @@
         scratch_shapes=list(scratch),
         compiler_params=pltpu.CompilerParams(vmem_limit_bytes=mib << 20),
     )(*ins)
-
-
-def to_all(value, axis, copies):
-    return lax.all_to_all(
-        jnp.broadcast_to(value, (copies, *value.shape)), axis, 0, 0, tiled=True
-    )
 
 
 def rotate_kernel(at, *refs):
@@ -259,27 +253,18 @@
     cut = inner + 2 * state
     core_swap = cycle(2, 1)
 
-    def halves_swapped(*arrays):
-        def columns_of(core):
-            return jnp.concatenate(
-                [
-                    lax.dynamic_slice_in_dim(w, core * (w.shape[1] // 2), w.shape[1] // 2, 1)
-                    for w in arrays
-                ],
-                axis=1,
-            )
-
-        mine = columns_of(c_at)
-        swapped = lax.ppermute(columns_of(1 - c_at), "c", core_swap)
-        return jnp.where(
-            c_at == 0,
-            jnp.concatenate([mine, swapped], axis=0),
-            jnp.concatenate([swapped, mine], axis=0),
-        )
-
-    first_source = halves_swapped(w_x, w_b, w_c)
+    def halves(*arrays):
+        parts = [a.reshape(a.shape[0], 2, -1).swapaxes(0, 1) for a in arrays]
+        return jnp.concatenate(parts, axis=2)
+
+    def along_z(source):
+        sent = jnp.broadcast_to(source, (n_z, *source.shape)).reshape(-1, *source.shape[1:])
+        got = lax.all_to_all(sent, ("z", "c"), 0, 0, tiled=True)
+        return got.reshape(n_z, -1, got.shape[-1])
+
+    first_source = halves(w_x, w_b, w_c)
     pieces = around(tokens, "y")
-    first_z = to_all(first_source, "z", n_z)
+    first_z = along_z(first_source)
 
     def here(v, size):
         return lax.dynamic_slice_in_dim(v, y_at * size, size, v.ndim - 1)
@@ -300,9 +285,9 @@
         (first_z, taps, rate, bias, dt_weight, gain)
     )
     first_pieces = around(first_z, "x")
-    second_source = halves_swapped(w_z, w_out.T)
+    second_source = halves(w_z, w_out.T)
     second_source, first_z = lax.optimization_barrier((second_source, first_z))
-    second_z = to_all(second_source, "z", n_z)
+    second_z = along_z(second_source)
 
     ends = lax.select_n(lax.rem(y_at + 1, n_y), *(piece[rows - 16 :] for piece in pieces))
     chain_steps = [(a, a + 1) for a in range(2 * n_z * n_x - 1)]
@@ -357,11 +342,13 @@
     )
     entering = lax.all_to_all(back, ("x", "c"), 0, 0, tiled=True).reshape(STATE, 2 * inner)
 
-    gates = [dot(normed[:length], w[:, :inner]).astype(BF16) for w in (second, second_other)]
-    halves = [w[:, inner:] for w in (second, second_other)]
+    gates = [dot(normed[:length], second[:, :inner]).astype(BF16)]
+    gates.append(dot(normed[:length], second_other[:, :inner]).astype(BF16))
+    ends = [w[:, inner:] for w in (second, second_other)]
     out_weight = jnp.where(
-        c_at == 0, jnp.concatenate(halves, axis=1), jnp.concatenate(halves[::-1], axis=1)
-    )
+        c_at == 0, jnp.concatenate(ends, axis=1), jnp.concatenate(ends[::-1], axis=1)
+    )
+    out_weight, entering = lax.optimization_barrier((out_weight, entering))
     mixed = local_call(
         gate_kernel,
         jax.ShapeDtypeStruct((length, 2 * inner), BF16),

time: 259 us -> 259 us (level)
  the two profiles are of different devices: /device:TPU:1 before, /device:TPU:32 now
where the time goes in v3:
time: 259 us; the launch traced here: 258 us
  waiting for transfers between devices  80.3 us (31%)
  starting transfers between devices  75.3 us (29%)
  blocking collectives  44.9 us (17%)
  local copies, waits for them, and re-layouts  20.7 us (8%)
  Pallas kernels  17.5 us (7%)
  matrix products  14.3 us (6%)
  other arithmetic  4.38 us (2%)
    all_to_all x1, blocking collectives, body(): shares = lax.all_to_all(partial, 'y', 0, 0, tiled=True)  36 us
    ppermute x9, starting transfers between devices, around(): lax.ppermute(value, axis, cycle(count, k))  33.8 us
    all_to_all x2, waiting for transfers between devices, along_z(): got = lax.all_to_all(sent, ('z', 'c'), 0, 0, tiled=True)  30.1 us
    ppermute x9, waiting for transfers between devices, around(): lax.ppermute(value, axis, cycle(count, k))  24.5 us
    all_to_all x2, starting transfers between devices, along_z(): got = lax.all_to_all(sent, ('z', 'c'), 0, 0, tiled=True)  22.7 us
    pallas_call x7, Pallas kernels, local_call(): pl.pallas_call(kernel, out_shape=outs, in_specs=[SMEM] * scalars + [VMEM]...  17.5 us
    all_to_all x1, waiting for transfers between devices, body(): planes = lax.all_to_all(sent, 'z', 0, 0, tiled=True)  17.3 us
    dot_general x5, matrix products, dot(): return jnp.dot(a, b, preferred_element_type=F32)  12.7 us
  transfers between devices with their start and end apart: 16, of which 8 were waited for; matrix products, arithmetic and copies ran while one was open for 8% of the time, Pallas kernels for 5%

profile of v3, /device:TPU:32, one launch (start us, length us, event | category | flops | bytes accessed | tf_op | source)
XLA Modules:
  0.0 257.7 jit_solution(8058662570979019848)
XLA Ops:
  3.1 15.4 %all-to-all-start = ((bf16[32,16,512]{2,1,0:T(8,128)(2,1)}), bf16[32,16,512]{2,1,0:T(8,128)(2,1)S(1)}, u32[]{:S(2)}, u32[]{:S(2)}) async-start(bf16[32,16,512]{2,1,0:T(8,128)(2,1)} %bitcast.7), calls=%async_computation | async-start | bytes 1048576 | tf_op jit(solution)/shard_map/all_to_all | solution.py:262
  18.4 5.1 %collective-permute-start.1 = (bf16[160,2048]{1,0:T(8,128)(2,1)}, bf16[160,2048]{1,0:T(8,128)(2,1)S(1)}, u32[]{:S(2)}, u32[]{:S(2)}) collective-permute-start(bf16[160,2048]{1,0:T(8,128)(2,1)} %refs_0_.1), channel_id=1, source_target_pairs={{0,2},{1,3},{2,0},{3,1},{4,6},{5,7},{6,4},{7,5},{8,10},{9,11},{10,... | collective-permute-start | bytes 1966088 | tf_op jit(solution)/shard_map/ppermute | solution.py:58
  26.2 4.5 %collective-permute-start.2 = (bf16[160,2048]{1,0:T(8,128)(2,1)}, bf16[160,2048]{1,0:T(8,128)(2,1)S(1)}, u32[]{:S(2)}, u32[]{:S(2)}) collective-permute-start(bf16[160,2048]{1,0:T(8,128)(2,1)} %refs_0_.1), channel_id=1, source_target_pairs={{0,3},{1,0},{2,1},{3,2},{4,7},{5,4},{6,5},{7,6},{8,11},{9,8},{10,9... | collective-permute-start | bytes 1966088 | tf_op jit(solution)/shard_map/ppermute | solution.py:58
  35.2 15.5 %all-to-all-done = bf16[32,16,512]{2,1,0:T(8,128)(2,1)S(1)} async-done(((bf16[32,16,512]{2,1,0:T(8,128)(2,1)}), bf16[32,16,512]{2,1,0:T(8,128)(2,1)S(1)}, u32[]{:S(2)}, u32[]{:S(2)}) %all-to-all-start) | async-done | bytes 524320 | tf_op jit(solution)/shard_map/all_to_all | solution.py:262
  50.6 4.7 %collective-permute-start.6 = (bf16[16,32,512]{2,1,0:T(8,128)(2,1)S(1)}, bf16[16,32,512]{2,1,0:T(8,128)(2,1)}, u32[]{:S(2)}, u32[]{:S(2)}) collective-permute-start(bf16[16,32,512]{2,1,0:T(8,128)(2,1)S(1)} %bitcast.43), channel_id=1, source_target_pairs={{0,24},{8,0},{16,8},{24,16},{1,25},{9,1},{17,9},{25,17},{2,26},{10... | collective-permute-start | bytes 1572872 | tf_op jit(solution)/shard_map/ppermute | solution.py:58
  58.0 2.8 %collective-permute-start.4 = (bf16[16,32,512]{2,1,0:T(8,128)(2,1)S(1)}, bf16[16,32,512]{2,1,0:T(8,128)(2,1)}, u32[]{:S(2)}, u32[]{:S(2)}) collective-permute-start(bf16[16,32,512]{2,1,0:T(8,128)(2,1)S(1)} %bitcast.45), channel_id=1, source_target_pairs={{0,8},{8,16},{16,24},{24,0},{1,9},{9,17},{17,25},{25,1},{2,10},{10... | collective-permute-start | bytes 1572872 | tf_op jit(solution)/shard_map/ppermute | solution.py:58
  66.2 6.1 %collective-permute-done.3.tail = bf16[16,2048]{1,0:T(8,128)(2,1)S(1)} collective-permute-done((bf16[16,2048]{1,0:T(8,128)(2,1)S(1)}, bf16[16,2048]{1,0:T(8,128)(2,1)S(1)}, u32[]{:S(2)}, u32[]{:S(2)}) %collective-permute-start.3) | collective-permute-done | bytes 65568 | tf_op jit(solution)/shard_map/ppermute | solution.py:294
  79.8 3.5 %collective-permute-done.4.refs_1_ = bf16[16,32,512]{2,1,0:T(8,128)(2,1)} collective-permute-done((bf16[16,32,512]{2,1,0:T(8,128)(2,1)S(1)}, bf16[16,32,512]{2,1,0:T(8,128)(2,1)}, u32[]{:S(2)}, u32[]{:S(2)}) %collective-permute-start.4) | collective-permute-done | bytes 524320 | tf_op jit(solution)/shard_map/ppermute | solution.py:58
  83.3 2.9 %shard_map.137 = bf16[16,4,32,512]{3,2,1,0:T(8,128)(2,1)} custom-call(s32[1]{0:T(128)} %bitcast.3.at, bf16[16,32,512]{2,1,0:T(8,128)(2,1)S(1)} %bitcast.46, bf16[16,32,512]{2,1,0:T(8,128)(2,1)} %collective-permute-done.4.refs_1_, bf16[16,32,512]{2,1,0:T(8,128)(2,1)} %collective-permute-done.5.refs_2_, bf16[16,32,512]{2,1,0:T(8,128)(2,1)} %collective-permute-done.6.refs_3_), custom_call_target="tpu_custom_call" | custom-call | tf_op jit(solution)/shard_map/pallas_call | solution.py:32
  86.2 4.8 %collective-permute-start.7 = (bf16[2048,512]{1,0:T(8,128)(2,1)}, bf16[2048,512]{1,0:T(8,128)(2,1)}, u32[]{:S(2)}, u32[]{:S(2)}) collective-permute-start(bf16[2048,512]{1,0:T(8,128)(2,1)} %bitcast.17), channel_id=1, source_target_pairs={{0,4},{4,0},{1,5},{5,1},{2,6},{6,2},{3,7},{7,3},{8,12},{12,8},{9,1... | collective-permute-start | bytes 6291464 | tf_op jit(solution)/shard_map/ppermute | solution.py:305
  91.9 7.4 %all-to-all-start.1 = ((bf16[32,16,512]{2,1,0:T(8,128)(2,1)}), bf16[32,16,512]{2,1,0:T(8,128)(2,1)S(1)}, u32[]{:S(2)}, u32[]{:S(2)}) async-start(bf16[32,16,512]{2,1,0:T(8,128)(2,1)} %bitcast.55), calls=%async_computation.1 | async-start | bytes 1048576 | tf_op jit(solution)/shard_map/all_to_all | solution.py:262
  99.3 3.1 %convolution_convert_fusion.2.own = bf16[656,512]{1,0:T(8,128)(2,1)S(1)} fusion(bf16[656,2048]{1,0:T(8,128)(2,1)S(1)} %shard_map.136, bf16[2048,512]{1,0:T(8,128)(2,1)} %bitcast.17), kind=kOutput, calls=%fused_computation.9 | convolution fusion | flops 1376067584 | bytes 5455872 | tf_op jit(solution)/shard_map/dot_general | solution.py:235
  102.5 3.2 %convolution_convert_fusion.1.other = bf16[656,512]{1,0:T(8,128)(2,1)S(1)} fusion(bf16[656,2048]{1,0:T(8,128)(2,1)S(1)} %shard_map.136, bf16[2048,512]{1,0:T(8,128)(2,1)} %collective-permute-done.7), kind=kOutput, calls=%fused_computation.8 | convolution fusion | flops 1376067584 | bytes 5455872 | tf_op jit(solution)/shard_map/dot_general | solution.py:235
  105.7 8.3 %shard_map.138 = (f32[640,512]{1,0:T(8,128)S(1)}, bf16[640,256]{1,0:T(8,128)(2,1)S(1)}, f32[640,128]{1,0:T(8,128)S(1)}, bf16[8,16,640]{2,1,0:T(8,128)(2,1)S(1)}) custom-call(s32[1]{0:T(128)} %bitcast.core, bf16[656,512]{1,0:T(8,128)(2,1)S(1)} %convolution_convert_fusion.2.own, bf16[656,512]{1,0:T(8,128)(2,1)S(1)} %convolution_convert_fusion.1.other, ...), custom_call_target="tpu_custom_call" | custom-call | tf_op jit(solution)/shard_map/pallas_call | solution.py:32
  116.6 14.6 %all-to-all-done.1 = bf16[32,16,512]{2,1,0:T(8,128)(2,1)S(1)} async-done(((bf16[32,16,512]{2,1,0:T(8,128)(2,1)}), bf16[32,16,512]{2,1,0:T(8,128)(2,1)S(1)}, u32[]{:S(2)}, u32[]{:S(2)}) %all-to-all-start.1) | async-done | bytes 524320 | tf_op jit(solution)/shard_map/all_to_all | solution.py:262
  131.2 5.5 %collective-permute-start.10 = (bf16[16,32,512]{2,1,0:T(8,128)(2,1)S(1)}, bf16[16,32,512]{2,1,0:T(8,128)(2,1)S(1)}, u32[]{:S(2)}, u32[]{:S(2)}) collective-permute-start(bf16[16,32,512]{2,1,0:T(8,128)(2,1)S(1)} %bitcast.47), channel_id=1, source_target_pairs={{0,24},{8,0},{16,8},{24,16},{1,25},{9,1},{17,9},{25,17},{2,26},{10... | collective-permute-start | bytes 1572872 | tf_op jit(solution)/shard_map/ppermute | solution.py:58
  139.5 3.3 %collective-permute-start.8 = (bf16[16,32,512]{2,1,0:T(8,128)(2,1)S(1)}, bf16[16,32,512]{2,1,0:T(8,128)(2,1)S(1)}, u32[]{:S(2)}, u32[]{:S(2)}) collective-permute-start(bf16[16,32,512]{2,1,0:T(8,128)(2,1)S(1)} %bitcast.49), channel_id=1, source_target_pairs={{0,8},{8,16},{16,24},{24,0},{1,9},{9,17},{17,25},{25,1},{2,10},{10... | collective-permute-start | bytes 1572872 | tf_op jit(solution)/shard_map/ppermute | solution.py:58
  142.8 15.4 %collective-permute-done.10.refs_3_ = bf16[16,32,512]{2,1,0:T(8,128)(2,1)S(1)} collective-permute-done((bf16[16,32,512]{2,1,0:T(8,128)(2,1)S(1)}, bf16[16,32,512]{2,1,0:T(8,128)(2,1)S(1)}, u32[]{:S(2)}, u32[]{:S(2)}) %collective-permute-start.10) | collective-permute-done | bytes 524320 | tf_op jit(solution)/shard_map/ppermute | solution.py:58
  158.2 5.6 %collective-permute-done.8.refs_1_ = bf16[16,32,512]{2,1,0:T(8,128)(2,1)S(1)} collective-permute-done((bf16[16,32,512]{2,1,0:T(8,128)(2,1)S(1)}, bf16[16,32,512]{2,1,0:T(8,128)(2,1)S(1)}, u32[]{:S(2)}, u32[]{:S(2)}) %collective-permute-start.8) | collective-permute-done | bytes 524320 | tf_op jit(solution)/shard_map/ppermute | solution.py:58
  165.9 8.8 %all_to_all.30.pieces = bf16[8,16,640]{2,1,0:T(8,128)(2,1)S(1)} all-to-all(bf16[8,16,640]{2,1,0:T(8,128)(2,1)S(1)} %get-tuple-element.41), channel_id=1, replica_groups=mesh['z'=16,'x'=4,'c'=2,'y'=4] {'x','c'}, dimensions={0} | all-to-all | bytes 327680 | tf_op jit(solution)/shard_map/all_to_all | solution.py:332
  175.6 6.6 %all-to-all-start.3 = ((bf16[16,16,640]{2,1,0:T(8,128)(2,1)}), bf16[16,16,640]{2,1,0:T(8,128)(2,1)S(1)}, u32[]{:S(2)}, u32[]{:S(2)}) async-start(bf16[16,16,640]{2,1,0:T(8,128)(2,1)} %shard_map.140), calls=%async_computation.3 | async-start | bytes 655360 | tf_op jit(solution)/shard_map/all_to_all | solution.py:336
  185.9 17.3 %all-to-all-done.3.planes = bf16[16,16,640]{2,1,0:T(8,128)(2,1)S(1)} async-done(((bf16[16,16,640]{2,1,0:T(8,128)(2,1)}), bf16[16,16,640]{2,1,0:T(8,128)(2,1)S(1)}, u32[]{:S(2)}, u32[]{:S(2)}) %all-to-all-start.3) | async-done | bytes 327712 | tf_op jit(solution)/shard_map/all_to_all | solution.py:336
  204.2 3.6 %all-to-all-start.4 = ((bf16[8,16,512]{2,1,0:T(8,128)(2,1)}), bf16[8,16,512]{2,1,0:T(8,128)(2,1)S(1)}, u32[]{:S(2)}, u32[]{:S(2)}) async-start(bf16[8,16,512]{2,1,0:T(8,128)(2,1)} %shard_map.141), calls=%async_computation.4 | async-start | bytes 262144 | tf_op jit(solution)/shard_map/all_to_all | solution.py:343
  220.2 36.0 %all_to_all.31 = bf16[4,160,2048]{2,1,0:T(8,128)(2,1)S(1)} all-to-all(bf16[4,160,2048]{2,1,0:T(8,128)(2,1)S(1)} %bitcast.54), channel_id=1, replica_groups=mesh['z'=16,'x'=4,'c'=2,'y'=4] {'y'}, dimensions={0} | all-to-all | bytes 5242880 | tf_op jit(solution)/shard_map/all_to_all | solution.py:360
  (95 shorter events, 53.6 us)
Async XLA Ops:
  0.0 30.6 %copy-start = (bf16[2048,32]{0,1:T(8,128)(2,1)S(1)}, bf16[2048,32]{0,1:T(8,128)(2,1)}, u32[]{:S(2)}) copy-start(bf16[2048,32]{0,1:T(8,128)(2,1)} %param.20) | copy-start | bytes 393220
  0.0 72.3 %copy-start.17 = (f32[2048]{0:T(1024)S(1)}, f32[2048]{0:T(1024)}, u32[]{:S(2)}) copy-start(f32[2048]{0:T(1024)} %param.15) | copy-start | bytes 24580
  3.1 47.5 %all-to-all-start = ((bf16[32,16,512]{2,1,0:T(8,128)(2,1)}), bf16[32,16,512]{2,1,0:T(8,128)(2,1)S(1)}, u32[]{:S(2)}, u32[]{:S(2)}) async-start(bf16[32,16,512]{2,1,0:T(8,128)(2,1)} %bitcast.7), calls=%async_computation | async-start | bytes 1048576 | tf_op jit(solution)/shard_map/all_to_all | solution.py:262
  18.4 39.6 %collective-permute-start.1 = (bf16[160,2048]{1,0:T(8,128)(2,1)}, bf16[160,2048]{1,0:T(8,128)(2,1)S(1)}, u32[]{:S(2)}, u32[]{:S(2)}) collective-permute-start(bf16[160,2048]{1,0:T(8,128)(2,1)} %refs_0_.1), channel_id=1, source_target_pairs={{0,2},{1,3},{2,0},{3,1},{4,6},{5,7},{6,4},{7,5},{8,10},{9,11},{10,... | collective-permute-start | bytes 1966088 | tf_op jit(solution)/shard_map/ppermute | solution.py:58
  23.6 37.3 %collective-permute-start = (bf16[160,2048]{1,0:T(8,128)(2,1)}, bf16[160,2048]{1,0:T(8,128)(2,1)S(1)}, u32[]{:S(2)}, u32[]{:S(2)}) collective-permute-start(bf16[160,2048]{1,0:T(8,128)(2,1)} %refs_0_.1), channel_id=1, source_target_pairs={{0,1},{1,2},{2,3},{3,0},{4,5},{5,6},{6,7},{7,4},{8,9},{9,10},{10,1... | collective-permute-start | bytes 1966088 | tf_op jit(solution)/shard_map/ppermute | solution.py:58
  26.2 34.7 %collective-permute-start.2 = (bf16[160,2048]{1,0:T(8,128)(2,1)}, bf16[160,2048]{1,0:T(8,128)(2,1)S(1)}, u32[]{:S(2)}, u32[]{:S(2)}) collective-permute-start(bf16[160,2048]{1,0:T(8,128)(2,1)} %refs_0_.1), channel_id=1, source_target_pairs={{0,3},{1,0},{2,1},{3,2},{4,7},{5,4},{6,5},{7,6},{8,11},{9,8},{10,9... | collective-permute-start | bytes 1966088 | tf_op jit(solution)/shard_map/ppermute | solution.py:58
  50.6 29.2 %collective-permute-start.6 = (bf16[16,32,512]{2,1,0:T(8,128)(2,1)S(1)}, bf16[16,32,512]{2,1,0:T(8,128)(2,1)}, u32[]{:S(2)}, u32[]{:S(2)}) collective-permute-start(bf16[16,32,512]{2,1,0:T(8,128)(2,1)S(1)} %bitcast.43), channel_id=1, source_target_pairs={{0,24},{8,0},{16,8},{24,16},{1,25},{9,1},{17,9},{25,17},{2,26},{10... | collective-permute-start | bytes 1572872 | tf_op jit(solution)/shard_map/ppermute | solution.py:58
  55.3 24.5 %collective-permute-start.5 = (bf16[16,32,512]{2,1,0:T(8,128)(2,1)S(1)}, bf16[16,32,512]{2,1,0:T(8,128)(2,1)}, u32[]{:S(2)}, u32[]{:S(2)}) collective-permute-start(bf16[16,32,512]{2,1,0:T(8,128)(2,1)S(1)} %bitcast.44), channel_id=1, source_target_pairs={{0,16},{8,24},{16,0},{24,8},{1,17},{9,25},{17,1},{25,9},{2,18},{10... | collective-permute-start | bytes 1572872 | tf_op jit(solution)/shard_map/ppermute | solution.py:58
  58.0 25.3 %collective-permute-start.4 = (bf16[16,32,512]{2,1,0:T(8,128)(2,1)S(1)}, bf16[16,32,512]{2,1,0:T(8,128)(2,1)}, u32[]{:S(2)}, u32[]{:S(2)}) collective-permute-start(bf16[16,32,512]{2,1,0:T(8,128)(2,1)S(1)} %bitcast.45), channel_id=1, source_target_pairs={{0,8},{8,16},{16,24},{24,0},{1,9},{9,17},{17,25},{25,1},{2,10},{10... | collective-permute-start | bytes 1572872 | tf_op jit(solution)/shard_map/ppermute | solution.py:58
  64.3 8.0 %collective-permute-start.3 = (bf16[16,2048]{1,0:T(8,128)(2,1)S(1)}, bf16[16,2048]{1,0:T(8,128)(2,1)S(1)}, u32[]{:S(2)}, u32[]{:S(2)}) collective-permute-start(bf16[16,2048]{1,0:T(8,128)(2,1)S(1)} %fusion.19), channel_id=1, source_target_pairs={{0,4},{4,8},{8,12},{12,16},{16,20},{20,24},{24,28},{28,32},{32,36}... | collective-permute-start | bytes 196616 | tf_op jit(solution)/shard_map/ppermute | solution.py:294
  78.2 24.3 %copy-start.1 = (bf16[656,2048]{1,0:T(8,128)(2,1)}, bf16[656,2048]{1,0:T(8,128)(2,1)S(1)}, u32[]{:S(2)}) copy-start(bf16[656,2048]{1,0:T(8,128)(2,1)S(1)} %shard_map.136) | copy-start | bytes 8060932
  79.8 11.1 %copy-start.21 = (bf16[16,512]{1,0:T(8,128)(2,1)S(1)}, bf16[16,512]{1,0:T(8,128)(2,1)}, u32[]{:S(2)}) copy-start(bf16[16,512]{1,0:T(8,128)(2,1)} %param.17) | copy-start | bytes 49156
  79.8 11.1 %copy-start.22 = (bf16[512,16]{0,1:T(8,128)(2,1)S(1)}, bf16[512,16]{0,1:T(8,128)(2,1)}, u32[]{:S(2)}) copy-start(bf16[512,16]{0,1:T(8,128)(2,1)} %param.27) | copy-start | bytes 49156
  86.2 16.3 %collective-permute-start.7 = (bf16[2048,512]{1,0:T(8,128)(2,1)}, bf16[2048,512]{1,0:T(8,128)(2,1)}, u32[]{:S(2)}, u32[]{:S(2)}) collective-permute-start(bf16[2048,512]{1,0:T(8,128)(2,1)} %bitcast.17), channel_id=1, source_target_pairs={{0,4},{4,0},{1,5},{5,1},{2,6},{6,2},{3,7},{7,3},{8,12},{12,8},{9,1... | collective-permute-start | bytes 6291464 | tf_op jit(solution)/shard_map/ppermute | solution.py:305
  91.9 39.3 %all-to-all-start.1 = ((bf16[32,16,512]{2,1,0:T(8,128)(2,1)}), bf16[32,16,512]{2,1,0:T(8,128)(2,1)S(1)}, u32[]{:S(2)}, u32[]{:S(2)}) async-start(bf16[32,16,512]{2,1,0:T(8,128)(2,1)} %bitcast.55), calls=%async_computation.1 | async-start | bytes 1048576 | tf_op jit(solution)/shard_map/all_to_all | solution.py:262
  102.4 3.2 %copy-start.16 = (f32[640,128]{1,0:T(8,128)S(1)}, f32[640,128]{1,0:T(8,128)}, u32[]{:S(2)}) copy-start(f32[640,128]{1,0:T(8,128)} %compare_select_fusion.step) | copy-start | bytes 983044
  131.2 27.0 %collective-permute-start.10 = (bf16[16,32,512]{2,1,0:T(8,128)(2,1)S(1)}, bf16[16,32,512]{2,1,0:T(8,128)(2,1)S(1)}, u32[]{:S(2)}, u32[]{:S(2)}) collective-permute-start(bf16[16,32,512]{2,1,0:T(8,128)(2,1)S(1)} %bitcast.47), channel_id=1, source_target_pairs={{0,24},{8,0},{16,8},{24,16},{1,25},{9,1},{17,9},{25,17},{2,26},{10... | collective-permute-start | bytes 1572872 | tf_op jit(solution)/shard_map/ppermute | solution.py:58
  136.8 21.4 %collective-permute-start.9 = (bf16[16,32,512]{2,1,0:T(8,128)(2,1)S(1)}, bf16[16,32,512]{2,1,0:T(8,128)(2,1)S(1)}, u32[]{:S(2)}, u32[]{:S(2)}) collective-permute-start(bf16[16,32,512]{2,1,0:T(8,128)(2,1)S(1)} %bitcast.48), channel_id=1, source_target_pairs={{0,16},{8,24},{16,0},{24,8},{1,17},{9,25},{17,1},{25,9},{2,18},{10... | collective-permute-start | bytes 1572872 | tf_op jit(solution)/shard_map/ppermute | solution.py:58
  139.5 24.3 %collective-permute-start.8 = (bf16[16,32,512]{2,1,0:T(8,128)(2,1)S(1)}, bf16[16,32,512]{2,1,0:T(8,128)(2,1)S(1)}, u32[]{:S(2)}, u32[]{:S(2)}) collective-permute-start(bf16[16,32,512]{2,1,0:T(8,128)(2,1)S(1)} %bitcast.49), channel_id=1, source_target_pairs={{0,8},{8,16},{16,24},{24,0},{1,9},{9,17},{17,25},{25,1},{2,10},{10... | collective-permute-start | bytes 1572872 | tf_op jit(solution)/shard_map/ppermute | solution.py:58
  163.9 43.8 %collective-permute-start.11 = (bf16[2048,512]{1,0:T(8,128)(2,1)S(1)}, bf16[2048,512]{1,0:T(8,128)(2,1)}, u32[]{:S(2)}, u32[]{:S(2)}) collective-permute-start(bf16[2048,512]{1,0:T(8,128)(2,1)S(1)} %bitcast.40), channel_id=1, source_target_pairs={{0,4},{4,0},{1,5},{5,1},{2,6},{6,2},{3,7},{7,3},{8,12},{12,8},{9,1... | collective-permute-start | bytes 6291464 | tf_op jit(solution)/shard_map/ppermute | solution.py:330
  175.6 27.5 %all-to-all-start.3 = ((bf16[16,16,640]{2,1,0:T(8,128)(2,1)}), bf16[16,16,640]{2,1,0:T(8,128)(2,1)S(1)}, u32[]{:S(2)}, u32[]{:S(2)}) async-start(bf16[16,16,640]{2,1,0:T(8,128)(2,1)} %shard_map.140), calls=%async_computation.3 | async-start | bytes 655360 | tf_op jit(solution)/shard_map/all_to_all | solution.py:336
  204.2 9.4 %all-to-all-start.4 = ((bf16[8,16,512]{2,1,0:T(8,128)(2,1)}), bf16[8,16,512]{2,1,0:T(8,128)(2,1)S(1)}, u32[]{:S(2)}, u32[]{:S(2)}) async-start(bf16[8,16,512]{2,1,0:T(8,128)(2,1)} %shard_map.141), calls=%async_computation.4 | async-start | bytes 262144 | tf_op jit(solution)/shard_map/all_to_all | solution.py:343
  209.3 4.3 %copy-start.2 = (bf16[656,2048]{1,0:T(8,128)(2,1)S(1)}, bf16[656,2048]{1,0:T(8,128)(2,1)}, u32[]{:S(2)}) copy-start(bf16[656,2048]{1,0:T(8,128)(2,1)} %copy-done.1) | copy-start | bytes 8060932
  215.8 2.8 %copy-start.19 = (bf16[2048,512]{1,0:T(8,128)(2,1)S(1)}, bf16[2048,512]{1,0:T(8,128)(2,1)}, u32[]{:S(2)}) copy-start(bf16[2048,512]{1,0:T(8,128)(2,1)} %maximum_select_fusion) | copy-start | bytes 6291460
  (15 other events, 19.4 us)

commit v4 on v2

--- a/solution.py
+++ b/solution.py
@@ -117,9 +117,11 @@
         offset[...] = offset[...] + total
         for g in range(2):
             buf[g, 8 : 8 + BLOCK, :] = rows_seq[g, here, :].astype(F32)
-            summed = taps[g, 0:1, :] * buf[g, 5 : 5 + BLOCK, :]
-            for k in range(1, CONV):
-                summed = summed + taps[g, k : k + 1, :] * buf[g, 5 + k : 5 + k + BLOCK, :]
+            window = buf[g]
+            summed = taps[g, CONV - 1 : CONV, :] * window[8:, :]
+            for k in range(CONV - 1):
+                behind = pltpu.roll(window, CONV - 1 - k, 0)
+                summed = summed + taps[g, k : k + 1, :] * behind[8:, :]
             buf[g, 0:8, :] = buf[g, BLOCK : BLOCK + 8, :]
             mixed = silu(summed)
             xs = mixed[:, :inner]
@@ -136,7 +138,7 @@
                 lane = slice(g * heads + h, g * heads + h + 1)
                 scaled = xs[:, cut] * steps[:, lane]
                 gap = cum[:, lane] - cum_t[lane, :]
-                within = jnp.where(causal, jnp.exp(jnp.where(causal, gap, 0.0)), 0.0) * scores
+                within = jnp.exp(jnp.where(causal, gap, -jnp.inf)) * scores
                 inside = jnp.dot(
                     within.astype(BF16), scaled.astype(BF16), preferred_element_type=F32
                 )
@@ -357,11 +359,13 @@
     )
     entering = lax.all_to_all(back, ("x", "c"), 0, 0, tiled=True).reshape(STATE, 2 * inner)
 
-    gates = [dot(normed[:length], w[:, :inner]).astype(BF16) for w in (second, second_other)]
-    halves = [w[:, inner:] for w in (second, second_other)]
+    gates = [dot(normed[:length], second[:, :inner]).astype(BF16)]
+    gates.append(dot(normed[:length], second_other[:, :inner]).astype(BF16))
+    ends = [w[:, inner:] for w in (second, second_other)]
     out_weight = jnp.where(
-        c_at == 0, jnp.concatenate(halves, axis=1), jnp.concatenate(halves[::-1], axis=1)
-    )
+        c_at == 0, jnp.concatenate(ends, axis=1), jnp.concatenate(ends[::-1], axis=1)
+    )
+    out_weight, entering = lax.optimization_barrier((out_weight, entering))
     mixed = local_call(
         gate_kernel,
         jax.ShapeDtypeStruct((length, 2 * inner), BF16),

time: 259 us -> 261 us (level)
  starting transfers between devices: 104 us -> 108 us
    ppermute x1, starting transfers between devices: 4.29 us -> 9.05 us  [body(): tail = lax.ppermute(ends, ('z', 'x', 'c'), chain_steps)]
    unnamed x42 -> x44, local copies, waits for them, and re-layouts: 9.53 us -> 9.73 us
  transfers between devices with their start and end apart: 18 -> 18, of which waited for: 12 -> 11; matrix products, arithmetic and copies ran while one was open for 8% -> 8% of each run, Pallas kernels for 5% -> 4%
where the time goes in v4:
time: 261 us; the launch traced here: 260 us
  starting transfers between devices  108 us (41%)
  waiting for transfers between devices  53 us (20%)
  blocking collectives  42.8 us (16%)
  local copies, waits for them, and re-layouts  19.9 us (8%)
  Pallas kernels  16.7 us (6%)
  matrix products  14.3 us (5%)
  other arithmetic  4.32 us (2%)
    all_to_all x1, blocking collectives, body(): shares = lax.all_to_all(partial, 'y', 0, 0, tiled=True)  34.9 us
    ppermute x9, starting transfers between devices, around(): lax.ppermute(value, axis, cycle(count, k))  31.3 us
    all_to_all x2, starting transfers between devices, to_all(): lax.all_to_all(jnp.broadcast_to(value, (copies, *value.shape)), axis, 0,...  26.4 us
    ppermute x9, waiting for transfers between devices, around(): lax.ppermute(value, axis, cycle(count, k))  21.9 us
    pallas_call x7, Pallas kernels, local_call(): pl.pallas_call(kernel, out_shape=outs, in_specs=[SMEM] * scalars + [VMEM]...  16.7 us
    all_to_all x2, waiting for transfers between devices, to_all(): lax.all_to_all(jnp.broadcast_to(value, (copies, *value.shape)), axis, 0,...  13.2 us
    all_to_all x1, starting transfers between devices, body(): planes = lax.all_to_all(sent, 'z', 0, 0, tiled=True)  12.8 us
    dot_general x5, matrix products, dot(): return jnp.dot(a, b, preferred_element_type=F32)  12.7 us
  transfers between devices with their start and end apart: 18, of which 11 were waited for; matrix products, arithmetic and copies ran while one was open for 8% of the time, Pallas kernels for 4%

profile of v4, /device:TPU:1, one launch (start us, length us, event | category | flops | bytes accessed | tf_op | source)
XLA Modules:
  0.0 259.9 jit_solution(4809087228792995194)
XLA Ops:
  1.5 8.7 %collective-permute-start.4 = (bf16[16,512]{1,0:T(8,128)(2,1)S(1)}, bf16[16,512]{1,0:T(8,128)(2,1)S(1)}, u32[]{:S(2)}, u32[]{:S(2)}) collective-permute-start(bf16[16,512]{1,0:T(8,128)(2,1)S(1)} %pad_maximum_fusion), channel_id=1, source_target_pairs={{0,4},{4,0},{1,5},{5,1},{2,6},{6,2},{3,7},{7,3},{8,12},{12,8},{9,1... | collective-permute-start | bytes 49160 | tf_op jit(solution)/shard_map/ppermute | solution.py:275
  12.0 9.6 %all-to-all-start = ((bf16[16,32,512]{2,1,0:T(8,128)(2,1)}), bf16[16,32,512]{2,1,0:T(8,128)(2,1)S(1)}, u32[]{:S(2)}, u32[]{:S(2)}) async-start(bf16[16,32,512]{2,1,0:T(8,128)(2,1)} %broadcast_in_dim.7), calls=%async_computation | async-start | bytes 1048576 | tf_op jit(solution)/shard_map/all_to_all | solution.py:43
  21.5 4.8 %collective-permute-start.1 = (bf16[160,2048]{1,0:T(8,128)(2,1)}, bf16[160,2048]{1,0:T(8,128)(2,1)S(1)}, u32[]{:S(2)}, u32[]{:S(2)}) collective-permute-start(bf16[160,2048]{1,0:T(8,128)(2,1)} %refs_0_.1), channel_id=1, source_target_pairs={{0,2},{1,3},{2,0},{3,1},{4,6},{5,7},{6,4},{7,5},{8,10},{9,11},{10,... | collective-permute-start | bytes 1966088 | tf_op jit(solution)/shard_map/ppermute | solution.py:64
  28.7 4.2 %collective-permute-start.2 = (bf16[160,2048]{1,0:T(8,128)(2,1)}, bf16[160,2048]{1,0:T(8,128)(2,1)S(1)}, u32[]{:S(2)}, u32[]{:S(2)}) collective-permute-start(bf16[160,2048]{1,0:T(8,128)(2,1)} %refs_0_.1), channel_id=1, source_target_pairs={{0,3},{1,0},{2,1},{3,2},{4,7},{5,4},{6,5},{7,6},{8,11},{9,8},{10,9... | collective-permute-start | bytes 1966088 | tf_op jit(solution)/shard_map/ppermute | solution.py:64
  37.4 6.8 %all-to-all-done.refs_0_ = bf16[16,32,512]{2,1,0:T(8,128)(2,1)S(1)} async-done(((bf16[16,32,512]{2,1,0:T(8,128)(2,1)}), bf16[16,32,512]{2,1,0:T(8,128)(2,1)S(1)}, u32[]{:S(2)}, u32[]{:S(2)}) %all-to-all-start) | async-done | bytes 524320 | tf_op jit(solution)/shard_map/all_to_all | solution.py:43
  44.3 4.4 %collective-permute-start.7 = (bf16[16,32,512]{2,1,0:T(8,128)(2,1)S(1)}, bf16[16,32,512]{2,1,0:T(8,128)(2,1)}, u32[]{:S(2)}, u32[]{:S(2)}) collective-permute-start(bf16[16,32,512]{2,1,0:T(8,128)(2,1)S(1)} %all-to-all-done.refs_0_), channel_id=1, source_target_pairs={{0,24},{8,0},{16,8},{24,16},{1,25},{9,1},{17,9},{25,17},{2,26},{10... | collective-permute-start | bytes 1572872 | tf_op jit(solution)/shard_map/ppermute | solution.py:64
  59.3 9.0 %collective-permute-start.3 = (bf16[16,2048]{1,0:T(8,128)(2,1)S(1)}, bf16[16,2048]{1,0:T(8,128)(2,1)S(1)}, u32[]{:S(2)}, u32[]{:S(2)}) collective-permute-start(bf16[16,2048]{1,0:T(8,128)(2,1)S(1)} %fusion.19), channel_id=1, source_target_pairs={{0,4},{4,8},{8,12},{12,16},{16,20},{20,24},{24,28},{28,32},{32,36}... | collective-permute-start | bytes 196616 | tf_op jit(solution)/shard_map/ppermute | solution.py:311
  77.7 2.9 %shard_map.137 = bf16[16,4,32,512]{3,2,1,0:T(8,128)(2,1)} custom-call(s32[1]{0:T(128)} %bitcast.3.at, bf16[16,32,512]{2,1,0:T(8,128)(2,1)S(1)} %all-to-all-done.refs_0_, bf16[16,32,512]{2,1,0:T(8,128)(2,1)} %collective-permute-done.5.refs_1_, bf16[16,32,512]{2,1,0:T(8,128)(2,1)} %collective-permute-done.6.refs_2_, ...), custom_call_target="tpu_custom_call" | custom-call | tf_op jit(solution)/shard_map/pallas_call | solution.py:32
  87.8 16.9 %all-to-all-start.1 = ((bf16[16,32,512]{2,1,0:T(8,128)(2,1)}), bf16[16,32,512]{2,1,0:T(8,128)(2,1)S(1)}, u32[]{:S(2)}, u32[]{:S(2)}) async-start(bf16[16,32,512]{2,1,0:T(8,128)(2,1)} %broadcast_in_dim.8), calls=%async_computation.1 | async-start | bytes 1048576 | tf_op jit(solution)/shard_map/all_to_all | solution.py:43
  104.7 3.1 %convolution_convert_fusion.2.own = bf16[656,512]{1,0:T(8,128)(2,1)S(1)} fusion(bf16[656,2048]{1,0:T(8,128)(2,1)S(1)} %shard_map.136, bf16[2048,512]{1,0:T(8,128)(2,1)} %bitcast.12), kind=kOutput, calls=%fused_computation.9 | convolution fusion | flops 1376067584 | bytes 5455872 | tf_op jit(solution)/shard_map/dot_general | solution.py:243
  107.9 3.2 %convolution_convert_fusion.1.other = bf16[656,512]{1,0:T(8,128)(2,1)S(1)} fusion(bf16[656,2048]{1,0:T(8,128)(2,1)S(1)} %shard_map.136, bf16[2048,512]{1,0:T(8,128)(2,1)} %collective-permute-done.8), kind=kOutput, calls=%fused_computation.8 | convolution fusion | flops 1376067584 | bytes 5455872 | tf_op jit(solution)/shard_map/dot_general | solution.py:243
  111.1 7.5 %shard_map.138 = (f32[640,512]{1,0:T(8,128)S(1)}, bf16[640,256]{1,0:T(8,128)(2,1)S(1)}, f32[640,128]{1,0:T(8,128)S(1)}, bf16[8,16,640]{2,1,0:T(8,128)(2,1)S(1)}) custom-call(s32[1]{0:T(128)} %bitcast.core, bf16[656,512]{1,0:T(8,128)(2,1)S(1)} %convolution_convert_fusion.2.own, bf16[656,512]{1,0:T(8,128)(2,1)S(1)} %convolution_convert_fusion.1.other, ...), custom_call_target="tpu_custom_call" | custom-call | tf_op jit(solution)/shard_map/pallas_call | solution.py:32
  121.3 6.4 %all-to-all-done.1.refs_0_ = bf16[16,32,512]{2,1,0:T(8,128)(2,1)S(1)} async-done(((bf16[16,32,512]{2,1,0:T(8,128)(2,1)}), bf16[16,32,512]{2,1,0:T(8,128)(2,1)S(1)}, u32[]{:S(2)}, u32[]{:S(2)}) %all-to-all-start.1) | async-done | bytes 524320 | tf_op jit(solution)/shard_map/all_to_all | solution.py:43
  127.6 5.2 %collective-permute-start.12 = (bf16[16,32,512]{2,1,0:T(8,128)(2,1)S(1)}, bf16[16,32,512]{2,1,0:T(8,128)(2,1)S(1)}, u32[]{:S(2)}, u32[]{:S(2)}) collective-permute-start(bf16[16,32,512]{2,1,0:T(8,128)(2,1)S(1)} %all-to-all-done.1.refs_0_), channel_id=1, source_target_pairs={{0,24},{8,0},{16,8},{24,16},{1,25},{9,1},{17,9},{25,17},{2,26},{10... | collective-permute-start | bytes 1572872 | tf_op jit(solution)/shard_map/ppermute | solution.py:64
  135.5 2.8 %collective-permute-start.10 = (bf16[16,32,512]{2,1,0:T(8,128)(2,1)S(1)}, bf16[16,32,512]{2,1,0:T(8,128)(2,1)S(1)}, u32[]{:S(2)}, u32[]{:S(2)}) collective-permute-start(bf16[16,32,512]{2,1,0:T(8,128)(2,1)S(1)} %all-to-all-done.1.refs_0_), channel_id=1, source_target_pairs={{0,8},{8,16},{16,24},{24,0},{1,9},{9,17},{17,25},{25,1},{2,10},{10... | collective-permute-start | bytes 1572872 | tf_op jit(solution)/shard_map/ppermute | solution.py:64
  138.3 4.5 %collective-permute-done.12.refs_3_ = bf16[16,32,512]{2,1,0:T(8,128)(2,1)S(1)} collective-permute-done((bf16[16,32,512]{2,1,0:T(8,128)(2,1)S(1)}, bf16[16,32,512]{2,1,0:T(8,128)(2,1)S(1)}, u32[]{:S(2)}, u32[]{:S(2)}) %collective-permute-start.12) | collective-permute-done | bytes 524320 | tf_op jit(solution)/shard_map/ppermute | solution.py:64
  144.4 13.6 %collective-permute-done.10.refs_1_ = bf16[16,32,512]{2,1,0:T(8,128)(2,1)S(1)} collective-permute-done((bf16[16,32,512]{2,1,0:T(8,128)(2,1)S(1)}, bf16[16,32,512]{2,1,0:T(8,128)(2,1)S(1)}, u32[]{:S(2)}, u32[]{:S(2)}) %collective-permute-start.10) | collective-permute-done | bytes 524320 | tf_op jit(solution)/shard_map/ppermute | solution.py:64
  158.1 5.8 %collective-permute-start.13 = (bf16[2048,512]{1,0:T(8,128)(2,1)S(1)}, bf16[2048,512]{1,0:T(8,128)(2,1)}, u32[]{:S(2)}, u32[]{:S(2)}) collective-permute-start(bf16[2048,512]{1,0:T(8,128)(2,1)S(1)} %bitcast.34), channel_id=1, source_target_pairs={{0,4},{4,0},{1,5},{5,1},{2,6},{6,2},{3,7},{7,3},{8,12},{12,8},{9,1... | collective-permute-start | bytes 6291464 | tf_op jit(solution)/shard_map/ppermute | solution.py:347
  163.9 7.9 %all_to_all.30.pieces = bf16[8,16,640]{2,1,0:T(8,128)(2,1)S(1)} all-to-all(bf16[8,16,640]{2,1,0:T(8,128)(2,1)S(1)} %get-tuple-element.41), channel_id=1, replica_groups=mesh['z'=16,'x'=4,'c'=2,'y'=4] {'x','c'}, dimensions={0} | all-to-all | bytes 327680 | tf_op jit(solution)/shard_map/all_to_all | solution.py:349
  172.8 12.8 %all-to-all-start.3 = ((bf16[16,16,640]{2,1,0:T(8,128)(2,1)}), bf16[16,16,640]{2,1,0:T(8,128)(2,1)S(1)}, u32[]{:S(2)}, u32[]{:S(2)}) async-start(bf16[16,16,640]{2,1,0:T(8,128)(2,1)} %shard_map.140), calls=%async_computation.3 | async-start | bytes 655360 | tf_op jit(solution)/shard_map/all_to_all | solution.py:353
  189.2 11.4 %all-to-all-done.3.planes = bf16[16,16,640]{2,1,0:T(8,128)(2,1)S(1)} async-done(((bf16[16,16,640]{2,1,0:T(8,128)(2,1)}), bf16[16,16,640]{2,1,0:T(8,128)(2,1)S(1)}, u32[]{:S(2)}, u32[]{:S(2)}) %all-to-all-start.3) | async-done | bytes 327712 | tf_op jit(solution)/shard_map/all_to_all | solution.py:353
  201.7 9.9 %all-to-all-start.4 = ((bf16[8,16,512]{2,1,0:T(8,128)(2,1)}), bf16[8,16,512]{2,1,0:T(8,128)(2,1)S(1)}, u32[]{:S(2)}, u32[]{:S(2)}) async-start(bf16[8,16,512]{2,1,0:T(8,128)(2,1)} %shard_map.141), calls=%async_computation.4 | async-start | bytes 262144 | tf_op jit(solution)/shard_map/all_to_all | solution.py:360
  219.1 2.8 %shard_map.142 = bf16[640,512]{1,0:T(8,128)(2,1)S(1)} custom-call(s32[1]{0:T(128)} %bitcast.core, f32[640,512]{1,0:T(8,128)S(1)} %copy-done.4, bf16[640,256]{1,0:T(8,128)(2,1)S(1)} %copy-done.13, f32[640,128]{1,0:T(8,128)S(1)} %copy-done.15, bf16[128,512]{1,0:T(8,128)(2,1)S(1)} %bitcast.37, bf16[640,256]{1,0:T(8,128)(2,1)S(1)} %fusion.6.gate_own, ...), custom_call_target="tpu_custom_call" | custom-call | tf_op jit(solution)/shard_map/pallas_call | solution.py:32
  223.5 34.9 %all_to_all.31 = bf16[4,160,2048]{2,1,0:T(8,128)(2,1)S(1)} all-to-all(bf16[4,160,2048]{2,1,0:T(8,128)(2,1)S(1)} %bitcast.40), channel_id=1, replica_groups=mesh['z'=16,'x'=4,'c'=2,'y'=4] {'y'}, dimensions={0} | all-to-all | bytes 5242880 | tf_op jit(solution)/shard_map/all_to_all | solution.py:377
  (95 shorter events, 60.4 us)
Async XLA Ops:
  0.0 32.9 %copy-start = (bf16[2048,32]{0,1:T(8,128)(2,1)S(1)}, bf16[2048,32]{0,1:T(8,128)(2,1)}, u32[]{:S(2)}) copy-start(bf16[2048,32]{0,1:T(8,128)(2,1)} %param.20) | copy-start | bytes 393220
  0.0 70.2 %copy-start.17 = (f32[2048]{0:T(1024)S(1)}, f32[2048]{0:T(1024)}, u32[]{:S(2)}) copy-start(f32[2048]{0:T(1024)} %param.15) | copy-start | bytes 24580
  1.5 9.6 %collective-permute-start.4 = (bf16[16,512]{1,0:T(8,128)(2,1)S(1)}, bf16[16,512]{1,0:T(8,128)(2,1)S(1)}, u32[]{:S(2)}, u32[]{:S(2)}) collective-permute-start(bf16[16,512]{1,0:T(8,128)(2,1)S(1)} %pad_maximum_fusion), channel_id=1, source_target_pairs={{0,4},{4,0},{1,5},{5,1},{2,6},{6,2},{3,7},{7,3},{8,12},{12,8},{9,1... | collective-permute-start | bytes 49160 | tf_op jit(solution)/shard_map/ppermute | solution.py:275
  12.0 32.3 %all-to-all-start = ((bf16[16,32,512]{2,1,0:T(8,128)(2,1)}), bf16[16,32,512]{2,1,0:T(8,128)(2,1)S(1)}, u32[]{:S(2)}, u32[]{:S(2)}) async-start(bf16[16,32,512]{2,1,0:T(8,128)(2,1)} %broadcast_in_dim.7), calls=%async_computation | async-start | bytes 1048576 | tf_op jit(solution)/shard_map/all_to_all | solution.py:43
  21.5 29.5 %collective-permute-start.1 = (bf16[160,2048]{1,0:T(8,128)(2,1)}, bf16[160,2048]{1,0:T(8,128)(2,1)S(1)}, u32[]{:S(2)}, u32[]{:S(2)}) collective-permute-start(bf16[160,2048]{1,0:T(8,128)(2,1)} %refs_0_.1), channel_id=1, source_target_pairs={{0,2},{1,3},{2,0},{3,1},{4,6},{5,7},{6,4},{7,5},{8,10},{9,11},{10,... | collective-permute-start | bytes 1966088 | tf_op jit(solution)/shard_map/ppermute | solution.py:64
  26.4 29.5 %collective-permute-start = (bf16[160,2048]{1,0:T(8,128)(2,1)}, bf16[160,2048]{1,0:T(8,128)(2,1)S(1)}, u32[]{:S(2)}, u32[]{:S(2)}) collective-permute-start(bf16[160,2048]{1,0:T(8,128)(2,1)} %refs_0_.1), channel_id=1, source_target_pairs={{0,1},{1,2},{2,3},{3,0},{4,5},{5,6},{6,7},{7,4},{8,9},{9,10},{10,1... | collective-permute-start | bytes 1966088 | tf_op jit(solution)/shard_map/ppermute | solution.py:64
  28.7 27.2 %collective-permute-start.2 = (bf16[160,2048]{1,0:T(8,128)(2,1)}, bf16[160,2048]{1,0:T(8,128)(2,1)S(1)}, u32[]{:S(2)}, u32[]{:S(2)}) collective-permute-start(bf16[160,2048]{1,0:T(8,128)(2,1)} %refs_0_.1), channel_id=1, source_target_pairs={{0,3},{1,0},{2,1},{3,2},{4,7},{5,4},{6,5},{7,6},{8,11},{9,8},{10,9... | collective-permute-start | bytes 1966088 | tf_op jit(solution)/shard_map/ppermute | solution.py:64
  44.3 33.5 %collective-permute-start.7 = (bf16[16,32,512]{2,1,0:T(8,128)(2,1)S(1)}, bf16[16,32,512]{2,1,0:T(8,128)(2,1)}, u32[]{:S(2)}, u32[]{:S(2)}) collective-permute-start(bf16[16,32,512]{2,1,0:T(8,128)(2,1)S(1)} %all-to-all-done.refs_0_), channel_id=1, source_target_pairs={{0,24},{8,0},{16,8},{24,16},{1,25},{9,1},{17,9},{25,17},{2,26},{10... | collective-permute-start | bytes 1572872 | tf_op jit(solution)/shard_map/ppermute | solution.py:64
  48.6 29.1 %collective-permute-start.6 = (bf16[16,32,512]{2,1,0:T(8,128)(2,1)S(1)}, bf16[16,32,512]{2,1,0:T(8,128)(2,1)}, u32[]{:S(2)}, u32[]{:S(2)}) collective-permute-start(bf16[16,32,512]{2,1,0:T(8,128)(2,1)S(1)} %all-to-all-done.refs_0_), channel_id=1, source_target_pairs={{0,16},{8,24},{16,0},{24,8},{1,17},{9,25},{17,1},{25,9},{2,18},{10... | collective-permute-start | bytes 1572872 | tf_op jit(solution)/shard_map/ppermute | solution.py:64
  51.1 26.6 %collective-permute-start.5 = (bf16[16,32,512]{2,1,0:T(8,128)(2,1)S(1)}, bf16[16,32,512]{2,1,0:T(8,128)(2,1)}, u32[]{:S(2)}, u32[]{:S(2)}) collective-permute-start(bf16[16,32,512]{2,1,0:T(8,128)(2,1)S(1)} %all-to-all-done.refs_0_), channel_id=1, source_target_pairs={{0,8},{8,16},{16,24},{24,0},{1,9},{9,17},{17,25},{25,1},{2,10},{10... | collective-permute-start | bytes 1572872 | tf_op jit(solution)/shard_map/ppermute | solution.py:64
  59.3 10.9 %collective-permute-start.3 = (bf16[16,2048]{1,0:T(8,128)(2,1)S(1)}, bf16[16,2048]{1,0:T(8,128)(2,1)S(1)}, u32[]{:S(2)}, u32[]{:S(2)}) collective-permute-start(bf16[16,2048]{1,0:T(8,128)(2,1)S(1)} %fusion.19), channel_id=1, source_target_pairs={{0,4},{4,8},{8,12},{12,16},{16,20},{20,24},{24,28},{28,32},{32,36}... | collective-permute-start | bytes 196616 | tf_op jit(solution)/shard_map/ppermute | solution.py:311
  76.1 31.8 %copy-start.1 = (bf16[656,2048]{1,0:T(8,128)(2,1)}, bf16[656,2048]{1,0:T(8,128)(2,1)S(1)}, u32[]{:S(2)}) copy-start(bf16[656,2048]{1,0:T(8,128)(2,1)S(1)} %shard_map.136) | copy-start | bytes 8060932
  77.7 4.8 %copy-start.21 = (bf16[512,16]{0,1:T(8,128)(2,1)S(1)}, bf16[512,16]{0,1:T(8,128)(2,1)}, u32[]{:S(2)}) copy-start(bf16[512,16]{0,1:T(8,128)(2,1)} %param.27) | copy-start | bytes 49156
  80.6 27.3 %collective-permute-start.8 = (bf16[2048,512]{1,0:T(8,128)(2,1)}, bf16[2048,512]{1,0:T(8,128)(2,1)}, u32[]{:S(2)}, u32[]{:S(2)}) collective-permute-start(bf16[2048,512]{1,0:T(8,128)(2,1)} %bitcast.12), channel_id=1, source_target_pairs={{0,4},{4,0},{1,5},{5,1},{2,6},{6,2},{3,7},{7,3},{8,12},{12,8},{9,1... | collective-permute-start | bytes 6291464 | tf_op jit(solution)/shard_map/ppermute | solution.py:322
  82.5 4.4 %collective-permute-start.9 = (bf16[16,512]{1,0:T(8,128)(2,1)S(1)}, bf16[16,512]{1,0:T(8,128)(2,1)S(1)}, u32[]{:S(2)}, u32[]{:S(2)}) collective-permute-start(bf16[16,512]{1,0:T(8,128)(2,1)S(1)} %pad_maximum_fusion.2), channel_id=1, source_target_pairs={{0,4},{4,0},{1,5},{5,1},{2,6},{6,2},{3,7},{7,3},{8,12},{12,8},{9,1... | collective-permute-start | bytes 49160 | tf_op jit(solution)/shard_map/ppermute | solution.py:275
  87.8 39.8 %all-to-all-start.1 = ((bf16[16,32,512]{2,1,0:T(8,128)(2,1)}), bf16[16,32,512]{2,1,0:T(8,128)(2,1)S(1)}, u32[]{:S(2)}, u32[]{:S(2)}) async-start(bf16[16,32,512]{2,1,0:T(8,128)(2,1)} %broadcast_in_dim.8), calls=%async_computation.1 | async-start | bytes 1048576 | tf_op jit(solution)/shard_map/all_to_all | solution.py:43
  107.9 3.2 %copy-start.16 = (f32[640,128]{1,0:T(8,128)S(1)}, f32[640,128]{1,0:T(8,128)}, u32[]{:S(2)}) copy-start(f32[640,128]{1,0:T(8,128)} %compare_select_fusion.step) | copy-start | bytes 983044
  127.6 15.1 %collective-permute-start.12 = (bf16[16,32,512]{2,1,0:T(8,128)(2,1)S(1)}, bf16[16,32,512]{2,1,0:T(8,128)(2,1)S(1)}, u32[]{:S(2)}, u32[]{:S(2)}) collective-permute-start(bf16[16,32,512]{2,1,0:T(8,128)(2,1)S(1)} %all-to-all-done.1.refs_0_), channel_id=1, source_target_pairs={{0,24},{8,0},{16,8},{24,16},{1,25},{9,1},{17,9},{25,17},{2,26},{10... | collective-permute-start | bytes 1572872 | tf_op jit(solution)/shard_map/ppermute | solution.py:64
  132.9 11.5 %collective-permute-start.11 = (bf16[16,32,512]{2,1,0:T(8,128)(2,1)S(1)}, bf16[16,32,512]{2,1,0:T(8,128)(2,1)S(1)}, u32[]{:S(2)}, u32[]{:S(2)}) collective-permute-start(bf16[16,32,512]{2,1,0:T(8,128)(2,1)S(1)} %all-to-all-done.1.refs_0_), channel_id=1, source_target_pairs={{0,16},{8,24},{16,0},{24,8},{1,17},{9,25},{17,1},{25,9},{2,18},{10... | collective-permute-start | bytes 1572872 | tf_op jit(solution)/shard_map/ppermute | solution.py:64
  135.5 22.5 %collective-permute-start.10 = (bf16[16,32,512]{2,1,0:T(8,128)(2,1)S(1)}, bf16[16,32,512]{2,1,0:T(8,128)(2,1)S(1)}, u32[]{:S(2)}, u32[]{:S(2)}) collective-permute-start(bf16[16,32,512]{2,1,0:T(8,128)(2,1)S(1)} %all-to-all-done.1.refs_0_), channel_id=1, source_target_pairs={{0,8},{8,16},{16,24},{24,0},{1,9},{9,17},{17,25},{25,1},{2,10},{10... | collective-permute-start | bytes 1572872 | tf_op jit(solution)/shard_map/ppermute | solution.py:64
  158.1 53.5 %collective-permute-start.13 = (bf16[2048,512]{1,0:T(8,128)(2,1)S(1)}, bf16[2048,512]{1,0:T(8,128)(2,1)}, u32[]{:S(2)}, u32[]{:S(2)}) collective-permute-start(bf16[2048,512]{1,0:T(8,128)(2,1)S(1)} %bitcast.34), channel_id=1, source_target_pairs={{0,4},{4,0},{1,5},{5,1},{2,6},{6,2},{3,7},{7,3},{8,12},{12,8},{9,1... | collective-permute-start | bytes 6291464 | tf_op jit(solution)/shard_map/ppermute | solution.py:347
  172.8 27.9 %all-to-all-start.3 = ((bf16[16,16,640]{2,1,0:T(8,128)(2,1)}), bf16[16,16,640]{2,1,0:T(8,128)(2,1)S(1)}, u32[]{:S(2)}, u32[]{:S(2)}) async-start(bf16[16,16,640]{2,1,0:T(8,128)(2,1)} %shard_map.140), calls=%async_computation.3 | async-start | bytes 655360 | tf_op jit(solution)/shard_map/all_to_all | solution.py:353
  201.7 15.2 %all-to-all-start.4 = ((bf16[8,16,512]{2,1,0:T(8,128)(2,1)}), bf16[8,16,512]{2,1,0:T(8,128)(2,1)S(1)}, u32[]{:S(2)}, u32[]{:S(2)}) async-start(bf16[8,16,512]{2,1,0:T(8,128)(2,1)} %shard_map.141), calls=%async_computation.4 | async-start | bytes 262144 | tf_op jit(solution)/shard_map/all_to_all | solution.py:360
  213.1 3.7 %copy-start.2 = (bf16[656,2048]{1,0:T(8,128)(2,1)S(1)}, bf16[656,2048]{1,0:T(8,128)(2,1)}, u32[]{:S(2)}) copy-start(bf16[656,2048]{1,0:T(8,128)(2,1)} %copy-done.1) | copy-start | bytes 8060932
  (16 other events, 22.1 us)

commit v5 on v4

--- a/solution.py
+++ b/solution.py
@@ -87,10 +87,10 @@
 
 
 def scan_kernel(
-    core, own, other, step, rate, taps, y_out, c_out, reach_out, state_out, rows_seq, buf, state, offset
+    core, own, other, step, rate, taps, rows_out, reach_out, state_out, rows_seq, buf, state, offset
 ):
     length = step.shape[0]
-    inner = y_out.shape[1] // 2
+    inner = state.shape[2]
     heads = inner // HEAD_DIM
     rows_seq[pl.ds(core[0], 1)] = own[...][None]
     rows_seq[pl.ds(1 - core[0], 1)] = other[...][None]
@@ -145,8 +145,8 @@
                 ys.append(inside + reached[:, cut] * decay[:, lane])
                 tails.append(scaled * tail_weight[:, lane])
                 factors.append(jnp.broadcast_to(total_decay[:, lane], (1, HEAD_DIM)))
-            y_out[here, g * inner : (g + 1) * inner] = jnp.concatenate(ys, axis=1)
-            c_out[here, g * STATE : (g + 1) * STATE] = cs
+            rows_out[here, g * inner : (g + 1) * inner] = jnp.concatenate(ys, axis=1).astype(BF16)
+            rows_out[here, 2 * inner + g * STATE : 2 * inner + (g + 1) * STATE] = cs
             fresh = jnp.dot(
                 bs.T.astype(BF16),
                 jnp.concatenate(tails, axis=1).astype(BF16),
@@ -214,8 +214,8 @@
         run = run * widened(factor, run.shape[1]) + states
 
 
-def gate_kernel(core, y, cs, reach, entering, gate_own, gate_other, gain, out):
-    inner = y.shape[1] // 2
+def gate_kernel(core, local, reach, entering, gate_own, gate_other, gain, out):
+    inner = entering.shape[1] // 2
     heads = inner // HEAD_DIM
 
     def block(i, carry):
@@ -225,18 +225,18 @@
         for g in range(2):
             cut = slice(g * inner, (g + 1) * inner)
             reached = jnp.dot(
-                cs[here, g * STATE : (g + 1) * STATE],
+                local[here, 2 * inner + g * STATE : 2 * inner + (g + 1) * STATE],
                 entering[:, cut],
                 preferred_element_type=F32,
             )
             expanded = widened(weight[:, g * heads : (g + 1) * heads], inner)
             gates = jnp.where(core[0] == g, own, other)
-            gated = (y[here, cut] + reached * expanded) * silu(gates)
+            gated = (local[here, cut].astype(F32) + reached * expanded) * silu(gates)
             mean = jnp.mean(gated * gated, axis=-1, keepdims=True)
             out[here, cut] = (gated * lax.rsqrt(mean + EPS) * gain[:, cut]).astype(BF16)
         return carry
 
-    lax.fori_loop(0, y.shape[0] // BLOCK, block, 0)
+    lax.fori_loop(0, local.shape[0] // BLOCK, block, 0)
 
 
 def dot(a, b):
@@ -323,11 +323,10 @@
     proj = [dot(normed, w).astype(BF16) for w in (first, first_other)]
     parts = 2 * n_x
     share = STATE // parts
-    y_local, c_rows, reach, final = local_call(
+    local, reach, final = local_call(
         scan_kernel,
         (
-            jax.ShapeDtypeStruct((length, 2 * inner), F32),
-            jax.ShapeDtypeStruct((length, 2 * STATE), BF16),
+            jax.ShapeDtypeStruct((length, 2 * inner + 2 * STATE), BF16),
             jax.ShapeDtypeStruct((length, lanes), F32),
             jax.ShapeDtypeStruct((parts, share, 2 * inner + lanes), BF16),
         ),
@@ -369,7 +368,7 @@
     mixed = local_call(
         gate_kernel,
         jax.ShapeDtypeStruct((length, 2 * inner), BF16),
-        (c_one, y_local, c_rows, reach, entering, *gates, gain),
+        (c_one, local, reach, entering, *gates, gain),
         1,
     )
 

time: 261 us -> 261 us (level)
    unnamed x44 -> x40, local copies, waits for them, and re-layouts: 9.73 us -> 8.77 us
where the time goes in v5:
time: 261 us; the launch traced here: 260 us
  starting transfers between devices  108 us (41%)
  waiting for transfers between devices  54 us (21%)
  blocking collectives  42.8 us (16%)
  local copies, waits for them, and re-layouts  19 us (7%)
  Pallas kernels  16.6 us (6%)
  matrix products  14.3 us (5%)
  other arithmetic  4.32 us (2%)
    all_to_all x1, blocking collectives, body(): shares = lax.all_to_all(partial, 'y', 0, 0, tiled=True)  34.9 us
    ppermute x9, starting transfers between devices, around(): lax.ppermute(value, axis, cycle(count, k))  31.3 us
    all_to_all x2, starting transfers between devices, to_all(): lax.all_to_all(jnp.broadcast_to(value, (copies, *value.shape)), axis, 0,...  26.5 us
    ppermute x9, waiting for transfers between devices, around(): lax.ppermute(value, axis, cycle(count, k))  21.9 us
    pallas_call x7, Pallas kernels, local_call(): pl.pallas_call(kernel, out_shape=outs, in_specs=[SMEM] * scalars + [VMEM]...  16.6 us
    all_to_all x2, waiting for transfers between devices, to_all(): lax.all_to_all(jnp.broadcast_to(value, (copies, *value.shape)), axis, 0,...  14.2 us
    all_to_all x1, starting transfers between devices, body(): planes = lax.all_to_all(sent, 'z', 0, 0, tiled=True)  12.8 us
    dot_general x5, matrix products, dot(): return jnp.dot(a, b, preferred_element_type=F32)  12.7 us
  transfers between devices with their start and end apart: 18, of which 11 were waited for; matrix products, arithmetic and copies ran while one was open for 8% of the time, Pallas kernels for 4%

profile of v5, /device:TPU:1, one launch (start us, length us, event | category | flops | bytes accessed | tf_op | source)
XLA Modules:
  0.0 259.8 jit_solution(8689134691016995697)
XLA Ops:
  1.5 8.7 %collective-permute-start.4 = (bf16[16,512]{1,0:T(8,128)(2,1)S(1)}, bf16[16,512]{1,0:T(8,128)(2,1)S(1)}, u32[]{:S(2)}, u32[]{:S(2)}) collective-permute-start(bf16[16,512]{1,0:T(8,128)(2,1)S(1)} %pad_maximum_fusion), channel_id=1, source_target_pairs={{0,4},{4,0},{1,5},{5,1},{2,6},{6,2},{3,7},{7,3},{8,12},{12,8},{9,1... | collective-permute-start | bytes 49160 | tf_op jit(solution)/shard_map/ppermute | solution.py:275
  12.0 9.6 %all-to-all-start = ((bf16[16,32,512]{2,1,0:T(8,128)(2,1)}), bf16[16,32,512]{2,1,0:T(8,128)(2,1)S(1)}, u32[]{:S(2)}, u32[]{:S(2)}) async-start(bf16[16,32,512]{2,1,0:T(8,128)(2,1)} %broadcast_in_dim.7), calls=%async_computation | async-start | bytes 1048576 | tf_op jit(solution)/shard_map/all_to_all | solution.py:43
  21.5 4.8 %collective-permute-start.1 = (bf16[160,2048]{1,0:T(8,128)(2,1)}, bf16[160,2048]{1,0:T(8,128)(2,1)S(1)}, u32[]{:S(2)}, u32[]{:S(2)}) collective-permute-start(bf16[160,2048]{1,0:T(8,128)(2,1)} %refs_0_.1), channel_id=1, source_target_pairs={{0,2},{1,3},{2,0},{3,1},{4,6},{5,7},{6,4},{7,5},{8,10},{9,11},{10,... | collective-permute-start | bytes 1966088 | tf_op jit(solution)/shard_map/ppermute | solution.py:64
  28.7 4.2 %collective-permute-start.2 = (bf16[160,2048]{1,0:T(8,128)(2,1)}, bf16[160,2048]{1,0:T(8,128)(2,1)S(1)}, u32[]{:S(2)}, u32[]{:S(2)}) collective-permute-start(bf16[160,2048]{1,0:T(8,128)(2,1)} %refs_0_.1), channel_id=1, source_target_pairs={{0,3},{1,0},{2,1},{3,2},{4,7},{5,4},{6,5},{7,6},{8,11},{9,8},{10,9... | collective-permute-start | bytes 1966088 | tf_op jit(solution)/shard_map/ppermute | solution.py:64
  37.4 6.8 %all-to-all-done.refs_0_ = bf16[16,32,512]{2,1,0:T(8,128)(2,1)S(1)} async-done(((bf16[16,32,512]{2,1,0:T(8,128)(2,1)}), bf16[16,32,512]{2,1,0:T(8,128)(2,1)S(1)}, u32[]{:S(2)}, u32[]{:S(2)}) %all-to-all-start) | async-done | bytes 524320 | tf_op jit(solution)/shard_map/all_to_all | solution.py:43
  44.3 4.4 %collective-permute-start.7 = (bf16[16,32,512]{2,1,0:T(8,128)(2,1)S(1)}, bf16[16,32,512]{2,1,0:T(8,128)(2,1)}, u32[]{:S(2)}, u32[]{:S(2)}) collective-permute-start(bf16[16,32,512]{2,1,0:T(8,128)(2,1)S(1)} %all-to-all-done.refs_0_), channel_id=1, source_target_pairs={{0,24},{8,0},{16,8},{24,16},{1,25},{9,1},{17,9},{25,17},{2,26},{10... | collective-permute-start | bytes 1572872 | tf_op jit(solution)/shard_map/ppermute | solution.py:64
  59.2 9.0 %collective-permute-start.3 = (bf16[16,2048]{1,0:T(8,128)(2,1)S(1)}, bf16[16,2048]{1,0:T(8,128)(2,1)S(1)}, u32[]{:S(2)}, u32[]{:S(2)}) collective-permute-start(bf16[16,2048]{1,0:T(8,128)(2,1)S(1)} %fusion.19), channel_id=1, source_target_pairs={{0,4},{4,8},{8,12},{12,16},{16,20},{20,24},{24,28},{28,32},{32,36}... | collective-permute-start | bytes 196616 | tf_op jit(solution)/shard_map/ppermute | solution.py:311
  77.7 2.9 %shard_map.137 = bf16[16,4,32,512]{3,2,1,0:T(8,128)(2,1)} custom-call(s32[1]{0:T(128)} %bitcast.3.at, bf16[16,32,512]{2,1,0:T(8,128)(2,1)S(1)} %all-to-all-done.refs_0_, bf16[16,32,512]{2,1,0:T(8,128)(2,1)} %collective-permute-done.5.refs_1_, bf16[16,32,512]{2,1,0:T(8,128)(2,1)} %collective-permute-done.6.refs_2_, ...), custom_call_target="tpu_custom_call" | custom-call | tf_op jit(solution)/shard_map/pallas_call | solution.py:32
  87.8 16.9 %all-to-all-start.1 = ((bf16[16,32,512]{2,1,0:T(8,128)(2,1)}), bf16[16,32,512]{2,1,0:T(8,128)(2,1)S(1)}, u32[]{:S(2)}, u32[]{:S(2)}) async-start(bf16[16,32,512]{2,1,0:T(8,128)(2,1)} %broadcast_in_dim.8), calls=%async_computation.1 | async-start | bytes 1048576 | tf_op jit(solution)/shard_map/all_to_all | solution.py:43
  104.7 3.1 %convolution_convert_fusion.2.own = bf16[656,512]{1,0:T(8,128)(2,1)S(1)} fusion(bf16[656,2048]{1,0:T(8,128)(2,1)S(1)} %shard_map.136, bf16[2048,512]{1,0:T(8,128)(2,1)} %bitcast.12), kind=kOutput, calls=%fused_computation.9 | convolution fusion | flops 1376067584 | bytes 5455872 | tf_op jit(solution)/shard_map/dot_general | solution.py:243
  107.9 3.2 %convolution_convert_fusion.1.other = bf16[656,512]{1,0:T(8,128)(2,1)S(1)} fusion(bf16[656,2048]{1,0:T(8,128)(2,1)S(1)} %shard_map.136, bf16[2048,512]{1,0:T(8,128)(2,1)} %collective-permute-done.8), kind=kOutput, calls=%fused_computation.8 | convolution fusion | flops 1376067584 | bytes 5455872 | tf_op jit(solution)/shard_map/dot_general | solution.py:243
  111.1 7.5 %shard_map.138 = (bf16[640,768]{1,0:T(8,128)(2,1)S(1)}, f32[640,128]{1,0:T(8,128)S(1)}, bf16[8,16,640]{2,1,0:T(8,128)(2,1)S(1)}) custom-call(s32[1]{0:T(128)} %bitcast.core, bf16[656,512]{1,0:T(8,128)(2,1)S(1)} %convolution_convert_fusion.2.own, bf16[656,512]{1,0:T(8,128)(2,1)S(1)} %convolution_convert_fusion.1.other, f32[640,128]{1,0:T(8,128)S(1)} %copy-done.12, ...), custom_call_target="tpu_custom_call" | custom-call | tf_op jit(solution)/shard_map/pallas_call | solution.py:32
  120.3 7.4 %all-to-all-done.1.refs_0_ = bf16[16,32,512]{2,1,0:T(8,128)(2,1)S(1)} async-done(((bf16[16,32,512]{2,1,0:T(8,128)(2,1)}), bf16[16,32,512]{2,1,0:T(8,128)(2,1)S(1)}, u32[]{:S(2)}, u32[]{:S(2)}) %all-to-all-start.1) | async-done | bytes 524320 | tf_op jit(solution)/shard_map/all_to_all | solution.py:43
  127.6 5.2 %collective-permute-start.12 = (bf16[16,32,512]{2,1,0:T(8,128)(2,1)S(1)}, bf16[16,32,512]{2,1,0:T(8,128)(2,1)S(1)}, u32[]{:S(2)}, u32[]{:S(2)}) collective-permute-start(bf16[16,32,512]{2,1,0:T(8,128)(2,1)S(1)} %all-to-all-done.1.refs_0_), channel_id=1, source_target_pairs={{0,24},{8,0},{16,8},{24,16},{1,25},{9,1},{17,9},{25,17},{2,26},{10... | collective-permute-start | bytes 1572872 | tf_op jit(solution)/shard_map/ppermute | solution.py:64
  135.5 2.8 %collective-permute-start.10 = (bf16[16,32,512]{2,1,0:T(8,128)(2,1)S(1)}, bf16[16,32,512]{2,1,0:T(8,128)(2,1)S(1)}, u32[]{:S(2)}, u32[]{:S(2)}) collective-permute-start(bf16[16,32,512]{2,1,0:T(8,128)(2,1)S(1)} %all-to-all-done.1.refs_0_), channel_id=1, source_target_pairs={{0,8},{8,16},{16,24},{24,0},{1,9},{9,17},{17,25},{25,1},{2,10},{10... | collective-permute-start | bytes 1572872 | tf_op jit(solution)/shard_map/ppermute | solution.py:64
  138.3 4.5 %collective-permute-done.12.refs_3_ = bf16[16,32,512]{2,1,0:T(8,128)(2,1)S(1)} collective-permute-done((bf16[16,32,512]{2,1,0:T(8,128)(2,1)S(1)}, bf16[16,32,512]{2,1,0:T(8,128)(2,1)S(1)}, u32[]{:S(2)}, u32[]{:S(2)}) %collective-permute-start.12) | collective-permute-done | bytes 524320 | tf_op jit(solution)/shard_map/ppermute | solution.py:64
  144.4 13.6 %collective-permute-done.10.refs_1_ = bf16[16,32,512]{2,1,0:T(8,128)(2,1)S(1)} collective-permute-done((bf16[16,32,512]{2,1,0:T(8,128)(2,1)S(1)}, bf16[16,32,512]{2,1,0:T(8,128)(2,1)S(1)}, u32[]{:S(2)}, u32[]{:S(2)}) %collective-permute-start.10) | collective-permute-done | bytes 524320 | tf_op jit(solution)/shard_map/ppermute | solution.py:64
  158.1 5.8 %collective-permute-start.13 = (bf16[2048,512]{1,0:T(8,128)(2,1)S(1)}, bf16[2048,512]{1,0:T(8,128)(2,1)}, u32[]{:S(2)}, u32[]{:S(2)}) collective-permute-start(bf16[2048,512]{1,0:T(8,128)(2,1)S(1)} %bitcast.34), channel_id=1, source_target_pairs={{0,4},{4,0},{1,5},{5,1},{2,6},{6,2},{3,7},{7,3},{8,12},{12,8},{9,1... | collective-permute-start | bytes 6291464 | tf_op jit(solution)/shard_map/ppermute | solution.py:346
  163.9 7.9 %all_to_all.30.pieces = bf16[8,16,640]{2,1,0:T(8,128)(2,1)S(1)} all-to-all(bf16[8,16,640]{2,1,0:T(8,128)(2,1)S(1)} %get-tuple-element.39), channel_id=1, replica_groups=mesh['z'=16,'x'=4,'c'=2,'y'=4] {'x','c'}, dimensions={0} | all-to-all | bytes 327680 | tf_op jit(solution)/shard_map/all_to_all | solution.py:348
  172.8 12.8 %all-to-all-start.3 = ((bf16[16,16,640]{2,1,0:T(8,128)(2,1)}), bf16[16,16,640]{2,1,0:T(8,128)(2,1)S(1)}, u32[]{:S(2)}, u32[]{:S(2)}) async-start(bf16[16,16,640]{2,1,0:T(8,128)(2,1)} %shard_map.140), calls=%async_computation.3 | async-start | bytes 655360 | tf_op jit(solution)/shard_map/all_to_all | solution.py:352
  189.2 11.4 %all-to-all-done.3.planes = bf16[16,16,640]{2,1,0:T(8,128)(2,1)S(1)} async-done(((bf16[16,16,640]{2,1,0:T(8,128)(2,1)}), bf16[16,16,640]{2,1,0:T(8,128)(2,1)S(1)}, u32[]{:S(2)}, u32[]{:S(2)}) %all-to-all-start.3) | async-done | bytes 327712 | tf_op jit(solution)/shard_map/all_to_all | solution.py:352
  201.7 9.9 %all-to-all-start.4 = ((bf16[8,16,512]{2,1,0:T(8,128)(2,1)}), bf16[8,16,512]{2,1,0:T(8,128)(2,1)S(1)}, u32[]{:S(2)}, u32[]{:S(2)}) async-start(bf16[8,16,512]{2,1,0:T(8,128)(2,1)} %shard_map.141), calls=%async_computation.4 | async-start | bytes 262144 | tf_op jit(solution)/shard_map/all_to_all | solution.py:359
  219.1 2.7 %shard_map.142 = bf16[640,512]{1,0:T(8,128)(2,1)S(1)} custom-call(s32[1]{0:T(128)} %bitcast.core, bf16[640,768]{1,0:T(8,128)(2,1)S(1)} %copy-done.4, f32[640,128]{1,0:T(8,128)S(1)} %copy-done.14, bf16[128,512]{1,0:T(8,128)(2,1)S(1)} %bitcast.37, bf16[640,256]{1,0:T(8,128)(2,1)S(1)} %fusion.6.gate_own, bf16[640,256]{1,0:T(8,128)(2,1)S(1)} %fusion.9.gate_other, ...), custom_call_target="tpu_custom_call" | custom-call | tf_op jit(solution)/shard_map/pallas_call | solution.py:32
  223.4 34.9 %all_to_all.31 = bf16[4,160,2048]{2,1,0:T(8,128)(2,1)S(1)} all-to-all(bf16[4,160,2048]{2,1,0:T(8,128)(2,1)S(1)} %bitcast.40), channel_id=1, replica_groups=mesh['z'=16,'x'=4,'c'=2,'y'=4] {'y'}, dimensions={0} | all-to-all | bytes 5242880 | tf_op jit(solution)/shard_map/all_to_all | solution.py:376
  (91 shorter events, 59.4 us)
Async XLA Ops:
  0.0 32.9 %copy-start = (bf16[2048,32]{0,1:T(8,128)(2,1)S(1)}, bf16[2048,32]{0,1:T(8,128)(2,1)}, u32[]{:S(2)}) copy-start(bf16[2048,32]{0,1:T(8,128)(2,1)} %param.20) | copy-start | bytes 393220
  0.0 70.2 %copy-start.15 = (f32[2048]{0:T(1024)S(1)}, f32[2048]{0:T(1024)}, u32[]{:S(2)}) copy-start(f32[2048]{0:T(1024)} %param.15) | copy-start | bytes 24580
  1.5 9.6 %collective-permute-start.4 = (bf16[16,512]{1,0:T(8,128)(2,1)S(1)}, bf16[16,512]{1,0:T(8,128)(2,1)S(1)}, u32[]{:S(2)}, u32[]{:S(2)}) collective-permute-start(bf16[16,512]{1,0:T(8,128)(2,1)S(1)} %pad_maximum_fusion), channel_id=1, source_target_pairs={{0,4},{4,0},{1,5},{5,1},{2,6},{6,2},{3,7},{7,3},{8,12},{12,8},{9,1... | collective-permute-start | bytes 49160 | tf_op jit(solution)/shard_map/ppermute | solution.py:275
  12.0 32.3 %all-to-all-start = ((bf16[16,32,512]{2,1,0:T(8,128)(2,1)}), bf16[16,32,512]{2,1,0:T(8,128)(2,1)S(1)}, u32[]{:S(2)}, u32[]{:S(2)}) async-start(bf16[16,32,512]{2,1,0:T(8,128)(2,1)} %broadcast_in_dim.7), calls=%async_computation | async-start | bytes 1048576 | tf_op jit(solution)/shard_map/all_to_all | solution.py:43
  21.5 29.5 %collective-permute-start.1 = (bf16[160,2048]{1,0:T(8,128)(2,1)}, bf16[160,2048]{1,0:T(8,128)(2,1)S(1)}, u32[]{:S(2)}, u32[]{:S(2)}) collective-permute-start(bf16[160,2048]{1,0:T(8,128)(2,1)} %refs_0_.1), channel_id=1, source_target_pairs={{0,2},{1,3},{2,0},{3,1},{4,6},{5,7},{6,4},{7,5},{8,10},{9,11},{10,... | collective-permute-start | bytes 1966088 | tf_op jit(solution)/shard_map/ppermute | solution.py:64
  26.4 29.5 %collective-permute-start = (bf16[160,2048]{1,0:T(8,128)(2,1)}, bf16[160,2048]{1,0:T(8,128)(2,1)S(1)}, u32[]{:S(2)}, u32[]{:S(2)}) collective-permute-start(bf16[160,2048]{1,0:T(8,128)(2,1)} %refs_0_.1), channel_id=1, source_target_pairs={{0,1},{1,2},{2,3},{3,0},{4,5},{5,6},{6,7},{7,4},{8,9},{9,10},{10,1... | collective-permute-start | bytes 1966088 | tf_op jit(solution)/shard_map/ppermute | solution.py:64
  28.7 27.2 %collective-permute-start.2 = (bf16[160,2048]{1,0:T(8,128)(2,1)}, bf16[160,2048]{1,0:T(8,128)(2,1)S(1)}, u32[]{:S(2)}, u32[]{:S(2)}) collective-permute-start(bf16[160,2048]{1,0:T(8,128)(2,1)} %refs_0_.1), channel_id=1, source_target_pairs={{0,3},{1,0},{2,1},{3,2},{4,7},{5,4},{6,5},{7,6},{8,11},{9,8},{10,9... | collective-permute-start | bytes 1966088 | tf_op jit(solution)/shard_map/ppermute | solution.py:64
  44.3 33.4 %collective-permute-start.7 = (bf16[16,32,512]{2,1,0:T(8,128)(2,1)S(1)}, bf16[16,32,512]{2,1,0:T(8,128)(2,1)}, u32[]{:S(2)}, u32[]{:S(2)}) collective-permute-start(bf16[16,32,512]{2,1,0:T(8,128)(2,1)S(1)} %all-to-all-done.refs_0_), channel_id=1, source_target_pairs={{0,24},{8,0},{16,8},{24,16},{1,25},{9,1},{17,9},{25,17},{2,26},{10... | collective-permute-start | bytes 1572872 | tf_op jit(solution)/shard_map/ppermute | solution.py:64
  48.6 29.1 %collective-permute-start.6 = (bf16[16,32,512]{2,1,0:T(8,128)(2,1)S(1)}, bf16[16,32,512]{2,1,0:T(8,128)(2,1)}, u32[]{:S(2)}, u32[]{:S(2)}) collective-permute-start(bf16[16,32,512]{2,1,0:T(8,128)(2,1)S(1)} %all-to-all-done.refs_0_), channel_id=1, source_target_pairs={{0,16},{8,24},{16,0},{24,8},{1,17},{9,25},{17,1},{25,9},{2,18},{10... | collective-permute-start | bytes 1572872 | tf_op jit(solution)/shard_map/ppermute | solution.py:64
  51.1 26.6 %collective-permute-start.5 = (bf16[16,32,512]{2,1,0:T(8,128)(2,1)S(1)}, bf16[16,32,512]{2,1,0:T(8,128)(2,1)}, u32[]{:S(2)}, u32[]{:S(2)}) collective-permute-start(bf16[16,32,512]{2,1,0:T(8,128)(2,1)S(1)} %all-to-all-done.refs_0_), channel_id=1, source_target_pairs={{0,8},{8,16},{16,24},{24,0},{1,9},{9,17},{17,25},{25,1},{2,10},{10... | collective-permute-start | bytes 1572872 | tf_op jit(solution)/shard_map/ppermute | solution.py:64
  59.2 10.9 %collective-permute-start.3 = (bf16[16,2048]{1,0:T(8,128)(2,1)S(1)}, bf16[16,2048]{1,0:T(8,128)(2,1)S(1)}, u32[]{:S(2)}, u32[]{:S(2)}) collective-permute-start(bf16[16,2048]{1,0:T(8,128)(2,1)S(1)} %fusion.19), channel_id=1, source_target_pairs={{0,4},{4,8},{8,12},{12,16},{16,20},{20,24},{24,28},{28,32},{32,36}... | collective-permute-start | bytes 196616 | tf_op jit(solution)/shard_map/ppermute | solution.py:311
  76.0 31.9 %copy-start.1 = (bf16[656,2048]{1,0:T(8,128)(2,1)}, bf16[656,2048]{1,0:T(8,128)(2,1)S(1)}, u32[]{:S(2)}) copy-start(bf16[656,2048]{1,0:T(8,128)(2,1)S(1)} %shard_map.136) | copy-start | bytes 8060932
  77.7 4.8 %copy-start.19 = (bf16[512,16]{0,1:T(8,128)(2,1)S(1)}, bf16[512,16]{0,1:T(8,128)(2,1)}, u32[]{:S(2)}) copy-start(bf16[512,16]{0,1:T(8,128)(2,1)} %param.27) | copy-start | bytes 49156
  80.6 27.3 %collective-permute-start.8 = (bf16[2048,512]{1,0:T(8,128)(2,1)}, bf16[2048,512]{1,0:T(8,128)(2,1)}, u32[]{:S(2)}, u32[]{:S(2)}) collective-permute-start(bf16[2048,512]{1,0:T(8,128)(2,1)} %bitcast.12), channel_id=1, source_target_pairs={{0,4},{4,0},{1,5},{5,1},{2,6},{6,2},{3,7},{7,3},{8,12},{12,8},{9,1... | collective-permute-start | bytes 6291464 | tf_op jit(solution)/shard_map/ppermute | solution.py:322
  82.5 4.4 %collective-permute-start.9 = (bf16[16,512]{1,0:T(8,128)(2,1)S(1)}, bf16[16,512]{1,0:T(8,128)(2,1)S(1)}, u32[]{:S(2)}, u32[]{:S(2)}) collective-permute-start(bf16[16,512]{1,0:T(8,128)(2,1)S(1)} %pad_maximum_fusion.2), channel_id=1, source_target_pairs={{0,4},{4,0},{1,5},{5,1},{2,6},{6,2},{3,7},{7,3},{8,12},{12,8},{9,1... | collective-permute-start | bytes 49160 | tf_op jit(solution)/shard_map/ppermute | solution.py:275
  87.8 39.8 %all-to-all-start.1 = ((bf16[16,32,512]{2,1,0:T(8,128)(2,1)}), bf16[16,32,512]{2,1,0:T(8,128)(2,1)S(1)}, u32[]{:S(2)}, u32[]{:S(2)}) async-start(bf16[16,32,512]{2,1,0:T(8,128)(2,1)} %broadcast_in_dim.8), calls=%async_computation.1 | async-start | bytes 1048576 | tf_op jit(solution)/shard_map/all_to_all | solution.py:43
  107.9 3.2 %copy-start.12 = (f32[640,128]{1,0:T(8,128)S(1)}, f32[640,128]{1,0:T(8,128)}, u32[]{:S(2)}) copy-start(f32[640,128]{1,0:T(8,128)} %compare_select_fusion.step) | copy-start | bytes 983044
  127.6 15.1 %collective-permute-start.12 = (bf16[16,32,512]{2,1,0:T(8,128)(2,1)S(1)}, bf16[16,32,512]{2,1,0:T(8,128)(2,1)S(1)}, u32[]{:S(2)}, u32[]{:S(2)}) collective-permute-start(bf16[16,32,512]{2,1,0:T(8,128)(2,1)S(1)} %all-to-all-done.1.refs_0_), channel_id=1, source_target_pairs={{0,24},{8,0},{16,8},{24,16},{1,25},{9,1},{17,9},{25,17},{2,26},{10... | collective-permute-start | bytes 1572872 | tf_op jit(solution)/shard_map/ppermute | solution.py:64
  132.9 11.5 %collective-permute-start.11 = (bf16[16,32,512]{2,1,0:T(8,128)(2,1)S(1)}, bf16[16,32,512]{2,1,0:T(8,128)(2,1)S(1)}, u32[]{:S(2)}, u32[]{:S(2)}) collective-permute-start(bf16[16,32,512]{2,1,0:T(8,128)(2,1)S(1)} %all-to-all-done.1.refs_0_), channel_id=1, source_target_pairs={{0,16},{8,24},{16,0},{24,8},{1,17},{9,25},{17,1},{25,9},{2,18},{10... | collective-permute-start | bytes 1572872 | tf_op jit(solution)/shard_map/ppermute | solution.py:64
  135.5 22.5 %collective-permute-start.10 = (bf16[16,32,512]{2,1,0:T(8,128)(2,1)S(1)}, bf16[16,32,512]{2,1,0:T(8,128)(2,1)S(1)}, u32[]{:S(2)}, u32[]{:S(2)}) collective-permute-start(bf16[16,32,512]{2,1,0:T(8,128)(2,1)S(1)} %all-to-all-done.1.refs_0_), channel_id=1, source_target_pairs={{0,8},{8,16},{16,24},{24,0},{1,9},{9,17},{17,25},{25,1},{2,10},{10... | collective-permute-start | bytes 1572872 | tf_op jit(solution)/shard_map/ppermute | solution.py:64
  158.1 53.5 %collective-permute-start.13 = (bf16[2048,512]{1,0:T(8,128)(2,1)S(1)}, bf16[2048,512]{1,0:T(8,128)(2,1)}, u32[]{:S(2)}, u32[]{:S(2)}) collective-permute-start(bf16[2048,512]{1,0:T(8,128)(2,1)S(1)} %bitcast.34), channel_id=1, source_target_pairs={{0,4},{4,0},{1,5},{5,1},{2,6},{6,2},{3,7},{7,3},{8,12},{12,8},{9,1... | collective-permute-start | bytes 6291464 | tf_op jit(solution)/shard_map/ppermute | solution.py:346
  172.8 27.9 %all-to-all-start.3 = ((bf16[16,16,640]{2,1,0:T(8,128)(2,1)}), bf16[16,16,640]{2,1,0:T(8,128)(2,1)S(1)}, u32[]{:S(2)}, u32[]{:S(2)}) async-start(bf16[16,16,640]{2,1,0:T(8,128)(2,1)} %shard_map.140), calls=%async_computation.3 | async-start | bytes 655360 | tf_op jit(solution)/shard_map/all_to_all | solution.py:352
  201.7 15.2 %all-to-all-start.4 = ((bf16[8,16,512]{2,1,0:T(8,128)(2,1)}), bf16[8,16,512]{2,1,0:T(8,128)(2,1)S(1)}, u32[]{:S(2)}, u32[]{:S(2)}) async-start(bf16[8,16,512]{2,1,0:T(8,128)(2,1)} %shard_map.141), calls=%async_computation.4 | async-start | bytes 262144 | tf_op jit(solution)/shard_map/all_to_all | solution.py:359
  213.2 3.7 %copy-start.2 = (bf16[656,2048]{1,0:T(8,128)(2,1)S(1)}, bf16[656,2048]{1,0:T(8,128)(2,1)}, u32[]{:S(2)}) copy-start(bf16[656,2048]{1,0:T(8,128)(2,1)} %copy-done.1) | copy-start | bytes 8060932
  (14 other events, 18.8 us)
